TPU v7x, 32 devices: a whole 2x2x4 slice. The times are simulated.
32 devices in a mesh: ep: 4 (over y, x), tp: 8 (over z, core).
Axes of the slice: x: 2, y: 2, z: 4, core: 2. Of those that a mesh axis runs over, the one named last changes fastest.
Arguments:
- query_heads_rows: bfloat16 [2048, 2048], P('ep', 'tp'), may hold values from -9 to 9
- key_heads_rows: bfloat16 [2048, 2048], P('ep', 'tp'), may hold values from -9 to 9
- value_heads_rows: bfloat16 [2048, 2048], P('ep', 'tp'), may hold values from -6 to 6
- write_strength_logit: bfloat16 [16, 2048], P('tp', 'ep'), may hold values from -3.5 to -1
- decay_preactivation: bfloat16 [16, 2048], P('tp', 'ep'), may hold values from -5 to 5
- head_decay_logarithm: float32 [16], P('tp'), may hold values from -20 to -3
- extra_log_decay: float32 [16, 2048], P('tp', 'ep'), may hold values from -0.7 to 0
- output_weight: bfloat16 [2048, 2048], P('tp'), may hold values from -2 to 2
- second_batch_tokens: bfloat16 [4096, 2048], P(('ep', 'tp')), may hold values from -6 to 6
- expert_norm_scale: float32 [2048], replicated, may hold values from 0.1 to 1.9
- expert_choice_index: int32 [4096, 2], P(('ep', 'tp')), may hold values from 0 to 15, as said below
- group_router_weight: float32 [4096], P(('ep', 'tp')), may hold values from 0.25 to 1
- expert_logit_difference: float32 [4096], P(('ep', 'tp')), may hold values from -8 to 8
- expert_gate_weight: bfloat16 [16, 1024, 2048], P('ep', 'tp'), may hold values from -0.125 to 0.125
- expert_up_weight: bfloat16 [16, 1024, 2048], P('ep', 'tp'), may hold values from -0.125 to 0.125
- expert_down_weight: bfloat16 [16, 1024, 2048], P('ep', 'tp'), may hold values from -0.375 to 0.375
Outputs:
- mixer_output_first: bfloat16 [2048, 2048], P(('ep', 'tp'))
- expert_out: bfloat16 [4096, 2048], P(('ep', 'tp'))
Inputs may be any that keep to these rules, and one draw needn't show every extreme that they name: `expert_choice_index`: each row names two different experts of one group, the experts a * 4 to a * 4 + 3 for some a. In the rows of one device (aligned blocks of 128 rows) no expert is named more than 32 times, and in every device's rows some expert is named exactly 32 times.
All inputs are finite; a program needn't handle non-finite values.
Results may differ from a plain program's by a relative error of at most 0.018.
Values may be sent and summed in bfloat16 or wider, within the bound.
No kernel may reach another device: no remote copies, remote signals or barrier semaphores. Data moves between devices by JAX's collectives and lax.ppermute only.
A program may use at most 128 MiB of HBM per device.

v0:
```python
import functools

import jax
import jax.numpy as jnp
from jax import lax
from jax.experimental import pallas as pl
from jax.experimental.pallas import tpu as pltpu
from jax.sharding import PartitionSpec as P


DK = 128
DV = 128
CAP = 32
EXPERTS = 16
EPG = 4
TOPK = 2
CORES = 2
META = 128
CHUNK = 128
NORM_EPS = 1e-06


F32 = jnp.float32
BF16 = jnp.bfloat16
EXACT = lax.Precision.HIGHEST
VMEM = pl.BlockSpec(memory_space=pltpu.VMEM)
HBM = pl.BlockSpec(memory_space=pltpu.HBM)
SMEM = pl.BlockSpec(memory_space=pltpu.SMEM)


def room(mib):
    return pltpu.CompilerParams(vmem_limit_bytes=mib * 2**20)


def cost(flops, moved):
    return pl.CostEstimate(flops=int(flops), bytes_accessed=int(moved), transcendentals=0)


def mm(a, b):
    return jnp.dot(a, b, precision=EXACT, preferred_element_type=F32)


def mixer_kernel(head, rate_ref, q_ref, k_ref, v_ref, write_ref, decay_ref, extra_ref, local_ref, proj_ref, joint_ref):
    length = q_ref.shape[0]
    chunks = length // CHUNK
    i = lax.broadcasted_iota(jnp.int32, (CHUNK, CHUNK), 0)
    j = lax.broadcasted_iota(jnp.int32, (CHUNK, CHUNK), 1)
    every = range(chunks)
    spans = [slice(c * CHUNK, (c + 1) * CHUNK) for c in every]

    def unit(ref, n):
        x = ref[spans[n], :].astype(F32)
        return x * lax.rsqrt(jnp.sum(x * x, axis=-1, keepdims=True) + NORM_EPS)

    q = [unit(q_ref, n) * DK**-0.5 for n in every]
    k = [unit(k_ref, n) for n in every]
    kt = [jnp.transpose(x) for x in k]
    v = [v_ref[spans[n], :].astype(F32) for n in every]
    raised = decay_ref[head : head + 1, :].astype(F32)
    soft = jnp.maximum(raised, 0.0) + jnp.log(1.0 + jnp.exp(-jnp.abs(raised)))
    rate = jnp.exp(jnp.full((1, length), rate_ref[head], F32))
    drops = extra_ref[head : head + 1, :] - rate * soft
    writes = jax.nn.sigmoid(write_ref[head : head + 1, :].astype(F32))
    drops = jnp.concatenate([drops[:, x] for x in spans], axis=0)
    writes = jnp.concatenate([writes[:, x] for x in spans], axis=0)
    summed = mm(drops, jnp.where(i <= j, 1.0, 0.0))
    columns = jnp.transpose(jnp.concatenate([summed, writes], axis=0))
    row = [summed[n : n + 1, :] for n in every]
    col = [columns[:, n : n + 1] for n in every]
    beta = [columns[:, len(every) + n : len(every) + n + 1] for n in every]
    last = [r[:, CHUNK - 1 :] for r in row]
    decay = [jnp.where(i >= j, jnp.exp(jnp.where(i >= j, col[n] - row[n], 0.0)), 0.0) for n in every]
    gram = [mm(k[n], kt[n]) for n in every]
    lower = [jnp.where(i > j, gram[n] * decay[n] * beta[n], 0.0) for n in every]
    scores = [mm(q[n], kt[n]) * decay[n] for n in every]
    eye = jnp.where(i == j, 1.0, 0.0)
    small = 16
    near = (i // small) == (j // small)
    power = [jnp.where(near, x, 0.0) for x in lower]
    inverse = [eye - x for x in power]
    reach = 2
    while reach < small:
        power = [mm(x, x) for x in power]
        inverse = [x + mm(x, y) for x, y in zip(inverse, power)]
        reach *= 2
    while small < CHUNK:
        band = ((i // (2 * small)) == (j // (2 * small))) & ((i // small) != (j // small))
        half = [mm(jnp.where(band, x, 0.0), y) for x, y in zip(lower, inverse)]
        inverse = [y - mm(y, x) for x, y in zip(half, inverse)]
        small *= 2
    grown = [jnp.exp(x) for x in col]
    rhs = [jnp.concatenate([v[n] * beta[n], k[n] * (beta[n] * grown[n])], axis=1) for n in every]
    solved = [mm(inverse[n], rhs[n]) for n in every]
    blank = jnp.zeros((CHUNK, DK), F32)
    start = jnp.concatenate([jnp.zeros((DK, DV), F32), eye], axis=1)
    joint = start
    for n in every:
        update = jnp.concatenate([solved[n][:, :DV], blank], axis=1) - mm(solved[n][:, DV:], joint)
        out = mm(q[n] * grown[n], joint) + mm(scores[n], update)
        joint = joint * jnp.exp(last[n]) + mm(kt[n] * jnp.exp(last[n] - row[n]), update)
        local_ref[spans[n], :] = out[:, :DV]
        proj_ref[spans[n], :] = out[:, DV:]
    joint_ref[...] = joint


def mixer_local(head, rates, queries, keys, values, write, decay, extra):
    length = queries.shape[0]
    tall = pl.BlockSpec((length, DK), lambda x: (0, head))
    gate = pl.BlockSpec(write.shape, lambda x: (0, 0))
    flat = pl.BlockSpec((length, DK), lambda x: (0, 0))
    return pl.pallas_call(
        functools.partial(mixer_kernel, head),
        grid=(1,),
        in_specs=[SMEM] + [tall] * 3 + [gate] * 3,
        out_specs=[flat, flat, pl.BlockSpec((DK, DV + DK), lambda x: (0, 0))],
        out_shape=[
            jax.ShapeDtypeStruct((length, DV), F32),
            jax.ShapeDtypeStruct((length, DK), F32),
            jax.ShapeDtypeStruct((DK, DV + DK), F32),
        ],
        cost_estimate=cost(length // CHUNK * 26 * 6 * 2 * 128**3, length * DK * 14),
        name="mixer_local",
    )(rates, queries, keys, values, write, decay, extra)


def join_kernel(late_ref, own_ref, got_ref, inner_ref, own_out, inner_out):
    late = late_ref[0] > 0
    for h in range(own_ref.shape[0]):
        own, got, inner = own_ref[h], got_ref[h], inner_ref[h]
        first, second = jnp.where(late, got, own), jnp.where(late, own, got)
        blank = jnp.zeros_like(own[:, DV:])
        keep = lambda x: jnp.concatenate([x[:, :DV], blank], axis=1)
        own_out[h] = mm(second[:, DV:], first) + keep(second)
        inner_out[h] = jnp.where(late, mm(inner[:, DV:], got) + keep(inner), inner)


def join(late, own, got, inner):
    shape = jax.ShapeDtypeStruct(own.shape, F32)
    return pl.pallas_call(
        join_kernel,
        in_specs=[SMEM] + [VMEM] * 3,
        out_specs=[VMEM] * 2,
        out_shape=[shape, shape],
        compiler_params=room(8),
        cost_estimate=cost(own.size * 24 * DK, own.size * 20),
        name="join",
    )(late, own, got, inner)


def attend_kernel(heads, late_ref, core_ref, *refs):
    local_refs, proj_refs = refs[:heads], refs[heads : 2 * heads]
    got_ref, inner_ref, mine_ref, other_ref = refs[2 * heads :]
    late = late_ref[0] > 0
    states = []
    for h in range(heads):
        inner = inner_ref[h]
        state = mm(inner[:, DV:], got_ref[h]) + inner[:, :DV]
        states.append(jnp.where(late, state, inner[:, :DV]))
    depth, rows = mine_ref.shape[0], mine_ref.shape[1]
    for out_ref, shift in ((mine_ref, core_ref[0]), (other_ref, 1 - core_ref[0])):
        for z in range(depth):
            span = pl.ds(pl.multiple_of((z * CORES + shift) * rows, rows), rows)
            for h in range(heads):
                out = local_refs[h][span, :] + mm(proj_refs[h][span, :], states[h])
                out_ref[z, :, h * DV : (h + 1) * DV] = out.astype(BF16)


def attend(depth, late, core, local, proj, got, inner):
    heads = len(local)
    length, width = local[0].shape
    half = jax.ShapeDtypeStruct((depth, length // depth // CORES, heads * width), BF16)
    full = lambda *shape: pl.BlockSpec(shape, lambda x: (0,) * len(shape))
    return pl.pallas_call(
        functools.partial(attend_kernel, heads),
        grid=(1,),
        in_specs=[SMEM] * 2 + [full(length, width)] * (2 * heads) + [full(*got.shape), full(*inner.shape)],
        out_specs=[full(*half.shape)] * 2,
        out_shape=[half, half],
        compiler_params=room(8),
        cost_estimate=cost(6 * 2 * length * width * DK * heads, length * width * 10 * heads),
        name="attend",
    )(late, core, *local, *proj, got, inner)


def project_kernel(mine_ref, theirs_ref, own_ref, pair_ref, out_ref):
    depth, rows, width = mine_ref.shape
    left = jnp.concatenate(
        [x[...].reshape(depth * rows, width) for x in (mine_ref, theirs_ref)], axis=1
    )
    tile = 512

    def body(step, carry):
        span = pl.ds(pl.multiple_of(step * tile, tile), tile)
        right = jnp.concatenate([own_ref[:, span], pair_ref[:, span]], axis=0)
        part = jnp.dot(left, right, preferred_element_type=F32).astype(BF16)
        out_ref[:, :, span] = part.reshape(depth, rows, tile)
        return carry

    lax.fori_loop(0, out_ref.shape[2] // tile, body, 0)


def project(mine, theirs, own, pair):
    depth, rows, width = mine.shape
    wide = own.shape[1]
    return pl.pallas_call(
        project_kernel,
        in_specs=[VMEM] * 4,
        out_specs=VMEM,
        out_shape=jax.ShapeDtypeStruct((depth, rows, wide), BF16),
        compiler_params=room(8),
        cost_estimate=cost(4 * depth * rows * width * wide, 4 * width * wide + 2 * depth * rows * wide),
        name="project",
    )(mine, theirs, own, pair)


def prepare_kernel(own, peers, slots, me_ref, x_ref, scale_ref, index_ref, gain_ref, block_ref, *out_refs):
    rows, width = x_ref.shape
    x = x_ref[...].astype(F32)
    inv = lax.rsqrt(jnp.mean(x * x, axis=-1, keepdims=True) + NORM_EPS)
    block_ref[:, :width] = (x * inv * scale_ref[...]).astype(BF16)
    shift = own.bit_length() - 1
    names = jnp.transpose(jnp.concatenate([index_ref[...].astype(F32), gain_ref[...]], axis=0))
    picks = [names[:, n : n + 1].astype(jnp.int32) for n in range(TOPK)]
    gain, logit = names[:, TOPK : TOPK + 1], names[:, TOPK + 1 : TOPK + 2]
    home = [lax.shift_right_logical(x, jnp.full_like(x, shift)) for x in picks]
    place = [x & (own - 1) for x in picks]
    lane = lax.broadcasted_iota(jnp.int32, (rows, META), 1)
    member = jnp.where((lane == home[0]) | (lane == home[1]), 1.0, 0.0).astype(BF16)
    ti = lax.broadcasted_iota(jnp.int32, (rows, rows), 0)
    tj = lax.broadcasted_iota(jnp.int32, (rows, rows), 1)
    before = jnp.where(ti > tj, 1.0, 0.0).astype(BF16)
    count = jnp.dot(before, member, preferred_element_type=F32)
    rank = [jnp.sum(jnp.where(lane == x, count, 0.0), axis=1, keepdims=True) for x in home]
    lead = jax.nn.sigmoid(logit)
    mixing = [gain * lead, gain * (1.0 - lead)]
    high = [x.astype(BF16).astype(F32) for x in mixing]
    low = [x - y for x, y in zip(mixing, high)]
    columns = [x.astype(F32) for x in home] + rank + [x.astype(F32) for x in place] + high + low
    meta = jnp.zeros((rows, META), F32)
    for number, column in enumerate(columns):
        meta = jnp.where(lane == number, column, meta)
    block_ref[:, width:] = meta.astype(BF16)
    dispatch_kernel(peers, slots, me_ref, block_ref, *out_refs)


def prepare(own, peers, slots, me, tokens, scale, index, weight, logit):
    rows, width = tokens.shape
    gains = jnp.stack([weight, logit] + [jnp.zeros_like(weight)] * 4)
    inputs = (tokens, scale.reshape(1, -1), index.T, gains)
    full = lambda *shape: pl.BlockSpec(shape, lambda x: (0,) * len(shape))
    block = jax.ShapeDtypeStruct((rows, width + META), BF16)
    return pl.pallas_call(
        functools.partial(prepare_kernel, own, peers, slots),
        grid=(1,),
        in_specs=[SMEM] + [full(*x.shape) for x in inputs],
        out_specs=[full(rows, width + META)] + [full(slots, width + META)] * peers,
        out_shape=[block] + [jax.ShapeDtypeStruct((slots, width + META), BF16)] * peers,
        cost_estimate=cost(2 * peers * slots * rows * width, rows * width * 8),
        name="prepare",
    )(me, *inputs)


def placement(me, meta, total, slots):
    rows = meta.shape[0]
    lane = lax.broadcasted_iota(jnp.int32, (rows, total), 1)
    home = [meta[:, x : x + 1].astype(jnp.int32) for x in (0, 1)]
    rank = [meta[:, x : x + 1].astype(jnp.int32) for x in (2, 3)]
    spot = [(x ^ me) * slots + y for x, y in zip(home, rank)]
    return jnp.where((lane == spot[0]) | (lane == spot[1]), 1.0, 0.0)


def dispatch_kernel(peers, slots, me_ref, block_ref, *out_refs):
    width = block_ref.shape[1] - META
    meta = block_ref[:, width:].astype(F32)
    pick = jnp.transpose(placement(me_ref[0], meta, peers * slots, slots)).astype(BF16)
    for number, out_ref in enumerate(out_refs):
        part = pick[number * slots : (number + 1) * slots, :]
        out_ref[...] = jnp.dot(part, block_ref[...], preferred_element_type=F32).astype(BF16)


def dispatch(peers, slots, me, block):
    rows, width = block.shape
    return pl.pallas_call(
        functools.partial(dispatch_kernel, peers, slots),
        in_specs=[SMEM, VMEM],
        out_specs=[VMEM] * peers,
        out_shape=[jax.ShapeDtypeStruct((slots, width), BF16)] * peers,
        compiler_params=room(8),
        cost_estimate=cost(2 * peers * slots * rows * width, (rows + peers * slots) * width * 2),
        name="dispatch",
    )(me, block)


def expert_kernel(peers, slots, me_ref, *refs):
    x_refs, sources, refs = refs[:peers], refs[peers : peers + 6], refs[peers + 6 :]
    out_refs, (x_all, hidden, *kept, ready) = refs[:peers], refs[peers:]
    gate_a, gate_b, up_a, up_b, down_a, down_b = kept
    own, half, width = gate_a.shape
    units = 2 * half
    rows = peers * slots
    tile = 256

    def fetch(which, expert):
        return pltpu.make_async_copy(
            sources[which].at[expert], kept[which].at[expert], ready.at[which, expert]
        )

    for expert in range(own):
        for which in range(4):
            fetch(which, expert).start()
    for expert in range(own):
        for which in (4, 5):
            fetch(which, expert).start()
    for number, x_ref in enumerate(x_refs):
        x_all[number * slots : (number + 1) * slots, :] = x_ref[...]
    meta = x_all[:, width:].astype(F32)
    me = me_ref[0].astype(F32)

    def inward(expert, carry):
        for which in range(4):
            fetch(which, expert).wait()
        here = expert.astype(F32)
        weight = jnp.zeros((rows, 1), F32)
        for choice in range(TOPK):
            fits = (meta[:, choice : choice + 1] == me) & (meta[:, 4 + choice : 5 + choice] == here)
            value = meta[:, 6 + choice : 7 + choice] + meta[:, 8 + choice : 9 + choice]
            weight = weight + jnp.where(fits, value, 0.0)
        inner = jnp.concatenate([gate_a[expert], gate_b[expert], up_a[expert], up_b[expert]], axis=0)
        both = lax.dot_general(
            x_all[:, :width], inner, (((1,), (1,)), ((), ())), preferred_element_type=F32
        )
        gating, upward = both[:, :units], both[:, units:]
        hidden[expert] = (gating / (1.0 + jnp.exp(-gating)) * upward * weight).astype(BF16)
        return carry

    lax.fori_loop(0, own, inward, 0)
    for expert in range(own):
        for which in (4, 5):
            fetch(which, expert).wait()

    def outward(step, carry):
        span = pl.ds(pl.multiple_of(step * tile, tile), tile)
        left = jnp.concatenate([hidden[x] for x in range(own)], axis=1)
        right = jnp.concatenate(
            [y for x in range(own) for y in (down_a[x, :, span], down_b[x, :, span])], axis=0
        )
        part = jnp.dot(left, right, preferred_element_type=F32).astype(BF16)
        for number, out_ref in enumerate(out_refs):
            out_ref[:, span] = part[number * slots : (number + 1) * slots, :]
        return carry

    lax.fori_loop(0, width // tile, outward, 0)


def expert_part(peers, slots, me, arrived, weights):
    own, units, width = weights[0].shape
    rows = peers * slots
    return pl.pallas_call(
        functools.partial(expert_kernel, peers, slots),
        in_specs=[SMEM] + [VMEM] * peers + [HBM] * 6,
        out_specs=[VMEM] * peers,
        out_shape=[jax.ShapeDtypeStruct((slots, width), BF16)] * peers,
        scratch_shapes=[pltpu.VMEM((rows, width + META), BF16), pltpu.VMEM((own, rows, 2 * units), BF16)]
        + [pltpu.VMEM((own, units, width), BF16)] * 6
        + [pltpu.SemaphoreType.DMA((6, own))],
        compiler_params=room(28),
        cost_estimate=cost(12 * own * units * rows * width, 12 * own * units * width + 4 * rows * width),
        name="expert_part",
    )(me, *arrived, *weights)


def collect_kernel(peers, slots, me_ref, meta_ref, *refs):
    pick = placement(me_ref[0], meta_ref[...].astype(F32), peers * slots, slots).astype(BF16)
    back = jnp.concatenate([x[...] for x in refs[:peers]], axis=0)
    found = jnp.dot(pick, back, preferred_element_type=F32)
    for extra in refs[peers:-1]:
        found = found + extra[...].astype(F32)
    refs[-1][...] = found.astype(BF16)


def collect(peers, slots, me, block, returned, extra):
    rows = block.shape[0]
    width = block.shape[1] - META
    full = lambda *shape: pl.BlockSpec(shape, lambda x: (0,) * len(shape))
    return pl.pallas_call(
        functools.partial(collect_kernel, peers, slots),
        grid=(1,),
        in_specs=[SMEM, pl.BlockSpec((rows, META), lambda x: (0, width // META))]
        + [full(slots, width)] * peers
        + [full(rows, width)] * len(extra),
        out_specs=full(rows, width),
        out_shape=jax.ShapeDtypeStruct((rows, width), BF16),
        compiler_params=room(8),
        cost_estimate=cost(2 * rows * peers * slots * width, (2 * rows + peers * slots) * width * 2),
        name="collect",
    )(me, block, *returned, *extra)


def shards(
    query_heads_rows,
    key_heads_rows,
    value_heads_rows,
    write_strength_logit,
    decay_preactivation,
    head_decay_logarithm,
    extra_log_decay,
    output_weight,
    second_batch_tokens,
    expert_norm_scale,
    expert_choice_index,
    group_router_weight,
    expert_logit_difference,
    expert_gate_weight,
    expert_up_weight,
    expert_down_weight,
):
    ep, tp = lax.axis_size("ep"), lax.axis_size("tp")
    depth = tp // CORES
    me = lax.axis_index("ep")
    rank = lax.axis_index("tp")
    level, core = rank // CORES, rank % CORES
    pair = [(x, x ^ 1) for x in range(tp)]

    def swap(x):
        return lax.ppermute(x, "tp", pair)

    def send(x, chips):
        return lax.ppermute(x, "tp", [(y, (y + chips * CORES) % tp) for y in range(tp)])

    def trade(x, distance):
        return lax.ppermute(x, "ep", [(y, y ^ distance) for y in range(ep)])

    def scalar(x):
        return x.astype(jnp.int32).reshape(1)

    me1 = scalar(me)
    own = EXPERTS // ep
    tokens = second_batch_tokens.shape[0]
    slots = own * CAP // TOPK if own % EPG == 0 else min(own * CAP, tokens)

    block, *sent = prepare(
        own,
        ep,
        slots,
        me1,
        second_batch_tokens,
        expert_norm_scale,
        expert_choice_index,
        group_router_weight,
        expert_logit_difference,
    )
    blocks, arrived = [block], []

    def move(hop):
        return send(blocks[hop - 1], 1)

    def exchange(sent):
        return [sent[0]] + [trade(sent[x], x) for x in range(1, ep)]

    def give_back(produced):
        return [produced[0]] + [trade(produced[x], x) for x in range(1, ep)]

    weights = []
    for shard in (expert_gate_weight, expert_up_weight, expert_down_weight):
        weights += [shard, swap(shard)]
    out_pair = swap(output_weight)

    for hop in range(depth):
        if hop > 0:
            blocks.append(move(hop))
            sent = dispatch(ep, slots, me1, blocks[hop])
        arrived.append(exchange(sent))

    heads = head_decay_logarithm.shape[0]
    local, proj, ends = [], [], []
    for head in range(heads):
        x, y, end = mixer_local(
            head,
            head_decay_logarithm,
            query_heads_rows,
            key_heads_rows,
            value_heads_rows,
            write_strength_logit,
            decay_preactivation,
            extra_log_decay,
        )
        local.append(x)
        proj.append(y)
        ends.append(end)
    joint = jnp.stack(ends)
    joint, weights = lax.optimization_barrier((joint, weights))
    eye = jnp.concatenate([jnp.zeros((DK, DV), F32), jnp.eye(DK, dtype=F32)], axis=1)
    inner = jnp.broadcast_to(eye, joint.shape)
    span = 1
    while True:
        late = scalar((me // span) % 2)
        final = 2 * span >= ep
        got = trade(joint[..., :DV] if final else joint, span)
        if final:
            break
        joint, inner = join(late, joint, got, inner)
        span *= 2
    mine, other = attend(depth, late, scalar(core), local, proj, got, inner)
    theirs = swap(other)
    partial = project(mine, theirs, output_weight, out_pair)

    def piece(hop):
        at = (level + depth - hop) % depth
        return lax.dynamic_index_in_dim(partial, at, 0, keepdims=False)

    mixed = piece(0).astype(F32)
    for hop in range(1, depth):
        mixed = mixed + send(piece(hop), -hop).astype(F32)

    found = []
    for hop in range(depth):
        produced = expert_part(ep, slots, me1, arrived[hop], weights)
        found.append(give_back(produced))
    running, near = [], []
    for hop in range(1, depth):
        total = collect(ep, slots, me1, blocks[hop], found[hop], running)
        if hop == 1:
            near = [send(total, -1)]
        else:
            running = [send(total, 1)]
    expert_out = collect(ep, slots, me1, blocks[0], found[0], near + running)
    return (mixed.astype(BF16), expert_out)


def solution(mesh):
    in_specs = (
        P("ep", "tp"),
        P("ep", "tp"),
        P("ep", "tp"),
        P("tp", "ep"),
        P("tp", "ep"),
        P("tp"),
        P("tp", "ep"),
        P("tp", None),
        P(("ep", "tp"), None),
        P(),
        P(("ep", "tp"), None),
        P(("ep", "tp")),
        P(("ep", "tp")),
        P("ep", "tp", None),
        P("ep", "tp", None),
        P("ep", "tp", None),
    )
    out_specs = (P(("ep", "tp"), None), P(("ep", "tp"), None))

    return jax.shard_map(shards, mesh=mesh, in_specs=in_specs, out_specs=out_specs, check_vma=False)
```

profile of v0, /device:TPU:10, one launch (start us, length us, event | category | flops | bytes accessed | tf_op | source)
XLA Modules:
  0.0 230.8 jit_solution(14964561647741489642)
XLA Ops:
  1.4 1.3 maximum_maximum_fusion.gain_ref
  2.7 3.2 %prepare.1 = (bf16[128,2176]{1,0:T(8,128)(2,1)}, bf16[64,2176]{1,0:T(8,128)(2,1)}, bf16[64,2176]{1,0:T(8,128)(2,1)}, bf16[64,2176]{1,0:T(8,128)(2,1)}, bf16[64,2176]{1,0:T(8,128)(2,1)}) custom-call(s32[1]{0:T(128)} %bitcast.9.me_ref, bf16[128,2048]{1,0:T(8,128)(2,1)} %x_ref.1, f32[1,2048]{1,0:T(1,128)} %bitcast.21, s32[2,128]{1,0:T(2,128)} %bitcast.22, ...), custom_call_target="tpu_custom_call" | custom-call | flops 134217728 | bytes 2097152 | tf_op jit(solution)/shard_map/prepare/pallas_call | solution.py:252
  5.9 1.6 collective-permute-start.16
  7.4 13.6 %collective-permute-done.16.block_ref.meta_ref = bf16[128,2176]{1,0:T(8,128)(2,1)S(1)} collective-permute-done((bf16[128,2176]{1,0:T(8,128)(2,1)}, bf16[128,2176]{1,0:T(8,128)(2,1)S(1)}, u32[]{:S(2)}, u32[]{:S(2)}) %collective-permute-start.16) | collective-permute-done | bytes 557088 | tf_op jit(solution)/shard_map/ppermute | solution.py:428
  21.0 1.6 collective-permute-start.24
  22.6 13.3 %collective-permute-done.24.block_ref.meta_ref = bf16[128,2176]{1,0:T(8,128)(2,1)} collective-permute-done((bf16[128,2176]{1,0:T(8,128)(2,1)S(1)}, bf16[128,2176]{1,0:T(8,128)(2,1)}, u32[]{:S(2)}, u32[]{:S(2)}) %collective-permute-start.24) | collective-permute-done | bytes 557088 | tf_op jit(solution)/shard_map/ppermute | solution.py:428
  35.9 1.0 collective-permute-start.25
  36.8 8.7 %mixer_local.2 = (f32[512,128]{1,0:T(8,128)}, f32[512,128]{1,0:T(8,128)}, f32[128,256]{1,0:T(8,128)}) custom-call(f32[2]{0:T(128)} %rate_ref.3, bf16[512,256]{1,0:T(8,128)(2,1)} %q_ref.3, bf16[512,256]{1,0:T(8,128)(2,1)} %k_ref.3, bf16[512,256]{1,0:T(8,128)(2,1)} %v_ref.3, bf16[2,512]{1,0:T(2,128)(2,1)} %write_ref.3, bf16[2,512]{1,0:T(2,128)(2,1)} %decay_ref.3, ...), custom_call_target="tpu_custom_call" | custom-call | flops 2617245696 | bytes 917504 | tf_op jit(solution)/shard_map/mixer_local/pallas_call | solution.py:111
  45.5 1.4 dispatch.3
  48.2 2.9 %collective-permute-done.25.block_ref.meta_ref = bf16[128,2176]{1,0:T(8,128)(2,1)S(1)} collective-permute-done((bf16[128,2176]{1,0:T(8,128)(2,1)}, bf16[128,2176]{1,0:T(8,128)(2,1)S(1)}, u32[]{:S(2)}, u32[]{:S(2)}) %collective-permute-start.25) | collective-permute-done | bytes 557088 | tf_op jit(solution)/shard_map/ppermute | solution.py:428
  51.2 1.5 collective-permute-start.18
  52.7 1.3 copy-done.7
  55.0 9.1 %mixer_local.3 = (f32[512,128]{1,0:T(8,128)}, f32[512,128]{1,0:T(8,128)}, f32[128,256]{1,0:T(8,128)}) custom-call(f32[2]{0:T(128)} %rate_ref.3, bf16[512,256]{1,0:T(8,128)(2,1)} %q_ref.3, bf16[512,256]{1,0:T(8,128)(2,1)} %k_ref.3, bf16[512,256]{1,0:T(8,128)(2,1)} %v_ref.3, bf16[2,512]{1,0:T(2,128)(2,1)} %write_ref.3, bf16[2,512]{1,0:T(2,128)(2,1)} %decay_ref.3, ...), custom_call_target="tpu_custom_call" | custom-call | flops 2617245696 | bytes 917504 | tf_op jit(solution)/shard_map/mixer_local/pallas_call | solution.py:111
  64.0 1.0 pad_maximum_fusion.own_ref
  65.0 1.7 dispatch.5
  66.8 1.4 dispatch.4
  68.9 1.1 collective-permute-start.32
  69.9 1.5 collective-permute-start.33
  72.4 1.0 collective-permute-start.26
  73.4 1.6 copy-done.1
  75.0 1.6 copy-done.4
  76.6 1.6 copy-done.8
  78.2 1.0 copy-done.21
  79.2 8.9 %expert_part.5 = (bf16[64,2048]{1,0:T(8,128)(2,1)S(1)}, bf16[64,2048]{1,0:T(8,128)(2,1)}, bf16[64,2048]{1,0:T(8,128)(2,1)}, bf16[64,2048]{1,0:T(8,128)(2,1)S(1)}) custom-call(s32[1]{0:T(128)} %bitcast.9.me_ref, bf16[64,2176]{1,0:T(8,128)(2,1)S(1)} %copy-done.21, bf16[64,2176]{1,0:T(8,128)(2,1)} %collective-permute-done.17.refs_1_, ...), custom_call_target="tpu_custom_call" | custom-call | flops 3221225472 | bytes 14680064 | tf_op jit(solution)/shard_map/expert_part/pallas_call | solution.py:358
  88.8 1.5 collective-permute-start.27
  91.3 1.0 collective-permute-start.3
  92.3 7.7 %expert_part.7 = (bf16[64,2048]{1,0:T(8,128)(2,1)S(1)}, bf16[64,2048]{1,0:T(8,128)(2,1)}, bf16[64,2048]{1,0:T(8,128)(2,1)S(1)}, bf16[64,2048]{1,0:T(8,128)(2,1)S(1)}) custom-call(s32[1]{0:T(128)} %bitcast.9.me_ref, bf16[64,2176]{1,0:T(8,128)(2,1)S(1)} %get-tuple-element.94.refs_0_, bf16[64,2176]{1,0:T(8,128)(2,1)S(1)} %collective-permute-done.32.refs_1_, ...), custom_call_target="tpu_custom_call" | custom-call | flops 3221225472 | bytes 14680064 | tf_op jit(solution)/shard_map/expert_part/pallas_call | solution.py:358
  102.8 1.0 collective-permute-start.20
  104.5 1.0 collective-permute-start.21
  106.3 1.5 collective-permute-start.35
  110.1 1.0 collective-permute-start.22
  111.2 1.1 collective-permute-done.20.refs_1_
  112.3 1.5 collective-permute-start.36
  114.5 3.4 %collective-permute-done.35.refs_1_ = bf16[64,2048]{1,0:T(8,128)(2,1)} collective-permute-done((bf16[64,2048]{1,0:T(8,128)(2,1)}, bf16[64,2048]{1,0:T(8,128)(2,1)}, u32[]{:S(2)}, u32[]{:S(2)}) %collective-permute-start.35) | collective-permute-done | bytes 262176 | tf_op jit(solution)/shard_map/ppermute | solution.py:431
  117.9 1.5 collective-permute-start.4
  119.5 1.6 copy-done.2
  121.0 1.6 copy-done.5
  122.6 1.6 copy-done.9
  124.2 1.0 copy-done.15
  125.2 1.0 copy-done.17
  126.1 1.0 copy-done.19
  127.1 8.8 %expert_part.6 = (bf16[64,2048]{1,0:T(8,128)(2,1)S(1)}, bf16[64,2048]{1,0:T(8,128)(2,1)}, bf16[64,2048]{1,0:T(8,128)(2,1)}, bf16[64,2048]{1,0:T(8,128)(2,1)S(1)}) custom-call(s32[1]{0:T(128)} %bitcast.9.me_ref, bf16[64,2176]{1,0:T(8,128)(2,1)S(1)} %copy-done.15, bf16[64,2176]{1,0:T(8,128)(2,1)S(1)} %copy-done.17, bf16[64,2176]{1,0:T(8,128)(2,1)S(1)} %copy-done.19, ...), custom_call_target="tpu_custom_call" | custom-call | flops 3221225472 | bytes 14680064 | tf_op jit(solution)/shard_map/expert_part/pallas_call | solution.py:358
  137.8 2.2 collect.5
  140.7 0.9 copy-done.26
  142.6 0.9 copy-done.28
  143.6 0.9 copy-done.29
  146.4 1.9 attend.1
  148.9 1.7 collect.4
  150.6 1.3 collective-permute-start.10
  152.0 1.5 collective-permute-start.11
  154.2 2.3 collective-permute-start.31
  156.5 2.7 %project.1 = bf16[4,64,2048]{2,1,0:T(8,128)(2,1)S(1)} custom-call(bf16[4,64,256]{2,1,0:T(8,128)(2,1)S(1)} %copy-done.39, bf16[4,64,256]{2,1,0:T(8,128)(2,1)} %collective-permute-done.5.theirs_ref, bf16[256,2048]{1,0:T(8,128)(2,1)S(1)} %copy-done.11, bf16[256,2048]{1,0:T(8,128)(2,1)} %collective-permute-done.6.pair_ref), custom_call_target="tpu_custom_call" | custom-call | flops 536870912 | bytes 3145728 | tf_op jit(solution)/shard_map/project/pallas_call | solution.py:205
  159.3 13.1 %collective-permute-done.31.refs_3_ = bf16[64,2048]{1,0:T(8,128)(2,1)S(1)} collective-permute-done((bf16[64,2048]{1,0:T(8,128)(2,1)S(1)}, bf16[64,2048]{1,0:T(8,128)(2,1)S(1)}, u32[]{:S(2)}, u32[]{:S(2)}) %collective-permute-start.31) | collective-permute-done | bytes 262176 | tf_op jit(solution)/shard_map/ppermute | solution.py:431
  172.4 3.5 %collective-permute-start.23 = (bf16[128,2048]{1,0:T(8,128)(2,1)S(1)}, bf16[128,2048]{1,0:T(8,128)(2,1)S(1)}, u32[]{:S(2)}, u32[]{:S(2)}) collective-permute-start(bf16[128,2048]{1,0:T(8,128)(2,1)S(1)} %collect.4), channel_id=1, source_target_pairs={{0,6},{1,7},{2,0},{3,1},{4,2},{5,3},{6,4},{7,5},{8,14},{9,15},{10,... | collective-permute-start | bytes 1572872 | tf_op jit(solution)/shard_map/ppermute | solution.py:428
  175.9 1.7 collect.6
  177.6 6.2 %collective-permute-start.8 = (bf16[64,2048]{1,0:T(8,128)(2,1)S(1)}, bf16[64,2048]{1,0:T(8,128)(2,1)S(1)}, u32[]{:S(2)}, u32[]{:S(2)}) collective-permute-start(bf16[64,2048]{1,0:T(8,128)(2,1)S(1)} %get-tuple-element.104), channel_id=1, source_target_pairs={{0,4},{1,5},{2,6},{3,7},{4,0},{5,1},{6,2},{7,3},{8,12},{9,13},{10,... | collective-permute-start | bytes 786440 | tf_op jit(solution)/shard_map/ppermute | solution.py:428
  183.8 2.0 collective-permute-start.39
  185.9 7.1 %expert_part.4 = (bf16[64,2048]{1,0:T(8,128)(2,1)S(1)}, bf16[64,2048]{1,0:T(8,128)(2,1)S(1)}, bf16[64,2048]{1,0:T(8,128)(2,1)S(1)}, bf16[64,2048]{1,0:T(8,128)(2,1)S(1)}) custom-call(s32[1]{0:T(128)} %bitcast.9.me_ref, bf16[64,2176]{1,0:T(8,128)(2,1)S(1)} %copy-done.13, bf16[64,2176]{1,0:T(8,128)(2,1)S(1)} %collective-permute-done.10.refs_1_, ...), custom_call_target="tpu_custom_call" | custom-call | flops 3221225472 | bytes 14680064 | tf_op jit(solution)/shard_map/expert_part/pallas_call | solution.py:358
  192.9 5.2 %collective-permute-done.9 = bf16[64,2048]{1,0:T(8,128)(2,1)S(1)} collective-permute-done((bf16[64,2048]{1,0:T(8,128)(2,1)S(1)}, bf16[64,2048]{1,0:T(8,128)(2,1)S(1)}, u32[]{:S(2)}, u32[]{:S(2)}) %collective-permute-start.9) | collective-permute-done | bytes 262176 | tf_op jit(solution)/shard_map/ppermute | solution.py:428
  198.1 1.5 collective-permute-start.13
  199.6 11.2 %collective-permute-done.8 = bf16[64,2048]{1,0:T(8,128)(2,1)S(1)} collective-permute-done((bf16[64,2048]{1,0:T(8,128)(2,1)S(1)}, bf16[64,2048]{1,0:T(8,128)(2,1)S(1)}, u32[]{:S(2)}, u32[]{:S(2)}) %collective-permute-start.8) | collective-permute-done | bytes 262176 | tf_op jit(solution)/shard_map/ppermute | solution.py:428
  211.5 9.9 %collective-permute-done.7 = bf16[64,2048]{1,0:T(8,128)(2,1)S(1)} collective-permute-done((bf16[64,2048]{1,0:T(8,128)(2,1)S(1)}, bf16[64,2048]{1,0:T(8,128)(2,1)S(1)}, u32[]{:S(2)}, u32[]{:S(2)}) %collective-permute-start.7) | collective-permute-done | bytes 262176 | tf_op jit(solution)/shard_map/ppermute | solution.py:428
  222.5 7.1 %collective-permute-done.15.refs_3_ = bf16[64,2048]{1,0:T(8,128)(2,1)S(1)} collective-permute-done((bf16[64,2048]{1,0:T(8,128)(2,1)S(1)}, bf16[64,2048]{1,0:T(8,128)(2,1)S(1)}, u32[]{:S(2)}, u32[]{:S(2)}) %collective-permute-start.15) | collective-permute-done | bytes 262176 | tf_op jit(solution)/shard_map/ppermute | solution.py:431
  229.5 1.3 collect.7
  (137 shorter events, 22.2 us)
Async XLA Ops:
  0.6 52.1 %collective-permute-start = (bf16[4,128,2048]{2,1,0:T(8,128)(2,1)}, bf16[4,128,2048]{2,1,0:T(8,128)(2,1)S(1)}, u32[]{:S(2)}, u32[]{:S(2)}) collective-permute-start(bf16[4,128,2048]{2,1,0:T(8,128)(2,1)} %refs_4_.3), channel_id=1, source_target_pairs={{0,1},{1,0},{2,3},{3,2},{4,5},{5,4},{6,7},{7,6},{8,9},{9,8},{10,11... | collective-permute-start | bytes 6291464 | tf_op jit(solution)/shard_map/ppermute | solution.py:425
  0.7 68.1 %collective-permute-start.1 = (bf16[4,128,2048]{2,1,0:T(8,128)(2,1)}, bf16[4,128,2048]{2,1,0:T(8,128)(2,1)}, u32[]{:S(2)}, u32[]{:S(2)}) collective-permute-start(bf16[4,128,2048]{2,1,0:T(8,128)(2,1)} %refs_6_.3), channel_id=1, source_target_pairs={{0,1},{1,0},{2,3},{3,2},{4,5},{5,4},{6,7},{7,6},{8,9},{9,8},{10,11... | collective-permute-start | bytes 6291464 | tf_op jit(solution)/shard_map/ppermute | solution.py:425
  1.2 67.7 %collective-permute-start.2 = (bf16[4,128,2048]{2,1,0:T(8,128)(2,1)}, bf16[4,128,2048]{2,1,0:T(8,128)(2,1)}, u32[]{:S(2)}, u32[]{:S(2)}) collective-permute-start(bf16[4,128,2048]{2,1,0:T(8,128)(2,1)} %refs_8_.3), channel_id=1, source_target_pairs={{0,1},{1,0},{2,3},{3,2},{4,5},{5,4},{6,7},{7,6},{8,9},{9,8},{10,11... | collective-permute-start | bytes 6291464 | tf_op jit(solution)/shard_map/ppermute | solution.py:425
  5.9 15.2 %collective-permute-start.16 = (bf16[128,2176]{1,0:T(8,128)(2,1)}, bf16[128,2176]{1,0:T(8,128)(2,1)S(1)}, u32[]{:S(2)}, u32[]{:S(2)}) collective-permute-start(bf16[128,2176]{1,0:T(8,128)(2,1)} %get-tuple-element.63.meta_ref), channel_id=1, source_target_pairs={{0,2},{1,3},{2,4},{3,5},{4,6},{5,7},{6,0},{7,1},{8,10},{9,11},{10,... | collective-permute-start | bytes 1671176 | tf_op jit(solution)/shard_map/ppermute | solution.py:428
  21.0 14.8 %collective-permute-start.24 = (bf16[128,2176]{1,0:T(8,128)(2,1)S(1)}, bf16[128,2176]{1,0:T(8,128)(2,1)}, u32[]{:S(2)}, u32[]{:S(2)}) collective-permute-start(bf16[128,2176]{1,0:T(8,128)(2,1)S(1)} %collective-permute-done.16.block_ref.meta_ref), channel_id=1, source_target_pairs={{0,2},{1,3},{2,4},{3,5},{4,6},{5,7},{6,0},{7,1},{8,10},{9,11},{10,... | collective-permute-start | bytes 1671176 | tf_op jit(solution)/shard_map/ppermute | solution.py:428
  35.9 15.3 %collective-permute-start.25 = (bf16[128,2176]{1,0:T(8,128)(2,1)}, bf16[128,2176]{1,0:T(8,128)(2,1)S(1)}, u32[]{:S(2)}, u32[]{:S(2)}) collective-permute-start(bf16[128,2176]{1,0:T(8,128)(2,1)} %collective-permute-done.24.block_ref.meta_ref), channel_id=1, source_target_pairs={{0,2},{1,3},{2,4},{3,5},{4,6},{5,7},{6,0},{7,1},{8,10},{9,11},{10,... | collective-permute-start | bytes 1671176 | tf_op jit(solution)/shard_map/ppermute | solution.py:428
  47.7 22.2 %collective-permute-start.17 = (bf16[64,2176]{1,0:T(8,128)(2,1)}, bf16[64,2176]{1,0:T(8,128)(2,1)}, u32[]{:S(2)}, u32[]{:S(2)}) collective-permute-start(bf16[64,2176]{1,0:T(8,128)(2,1)} %get-tuple-element.79), channel_id=1, source_target_pairs={{0,8},{8,0},{16,24},{24,16},{1,9},{9,1},{17,25},{25,17},{2,10},{10... | collective-permute-start | bytes 835592 | tf_op jit(solution)/shard_map/ppermute | solution.py:431
  51.2 20.3 %collective-permute-start.18 = (bf16[64,2176]{1,0:T(8,128)(2,1)}, bf16[64,2176]{1,0:T(8,128)(2,1)}, u32[]{:S(2)}, u32[]{:S(2)}) collective-permute-start(bf16[64,2176]{1,0:T(8,128)(2,1)} %get-tuple-element.80), channel_id=1, source_target_pairs={{0,16},{8,24},{16,0},{24,8},{1,17},{9,25},{17,1},{25,9},{2,18},{10... | collective-permute-start | bytes 835592 | tf_op jit(solution)/shard_map/ppermute | solution.py:431
  52.7 1.3 copy-start.7
  54.0 18.4 %collective-permute-start.19 = (bf16[64,2176]{1,0:T(8,128)(2,1)}, bf16[64,2176]{1,0:T(8,128)(2,1)}, u32[]{:S(2)}, u32[]{:S(2)}) collective-permute-start(bf16[64,2176]{1,0:T(8,128)(2,1)} %get-tuple-element.81), channel_id=1, source_target_pairs={{0,24},{8,16},{16,8},{24,0},{1,25},{9,17},{17,9},{25,1},{2,26},{10... | collective-permute-start | bytes 835592 | tf_op jit(solution)/shard_map/ppermute | solution.py:431
  55.0 18.5 %copy-start = (bf16[4,128,2048]{2,1,0:T(8,128)(2,1)S(1)}, bf16[4,128,2048]{2,1,0:T(8,128)(2,1)}, u32[]{:S(2)}) copy-start(bf16[4,128,2048]{2,1,0:T(8,128)(2,1)} %refs_4_.3) | copy-start | bytes 6291460
  68.9 81.8 %collective-permute-start.6 = (bf16[256,2048]{1,0:T(8,128)(2,1)}, bf16[256,2048]{1,0:T(8,128)(2,1)}, u32[]{:S(2)}, u32[]{:S(2)}) collective-permute-start(bf16[256,2048]{1,0:T(8,128)(2,1)} %own_ref.1), channel_id=1, source_target_pairs={{0,1},{1,0},{2,3},{3,2},{4,5},{5,4},{6,7},{7,6},{8,9},{9,8},{10,11... | collective-permute-start | bytes 3145736 | tf_op jit(solution)/shard_map/ppermute | solution.py:425
  68.9 19.9 %collective-permute-start.32 = (bf16[64,2176]{1,0:T(8,128)(2,1)S(1)}, bf16[64,2176]{1,0:T(8,128)(2,1)S(1)}, u32[]{:S(2)}, u32[]{:S(2)}) collective-permute-start(bf16[64,2176]{1,0:T(8,128)(2,1)S(1)} %get-tuple-element.95), channel_id=1, source_target_pairs={{0,8},{8,0},{16,24},{24,16},{1,9},{9,1},{17,25},{25,17},{2,10},{10... | collective-permute-start | bytes 835592 | tf_op jit(solution)/shard_map/ppermute | solution.py:431
  69.9 20.4 %collective-permute-start.33 = (bf16[64,2176]{1,0:T(8,128)(2,1)S(1)}, bf16[64,2176]{1,0:T(8,128)(2,1)S(1)}, u32[]{:S(2)}, u32[]{:S(2)}) collective-permute-start(bf16[64,2176]{1,0:T(8,128)(2,1)S(1)} %get-tuple-element.96), channel_id=1, source_target_pairs={{0,16},{8,24},{16,0},{24,8},{1,17},{9,25},{17,1},{25,9},{2,18},{10... | collective-permute-start | bytes 835592 | tf_op jit(solution)/shard_map/ppermute | solution.py:431
  71.5 19.8 %collective-permute-start.34 = (bf16[64,2176]{1,0:T(8,128)(2,1)S(1)}, bf16[64,2176]{1,0:T(8,128)(2,1)S(1)}, u32[]{:S(2)}, u32[]{:S(2)}) collective-permute-start(bf16[64,2176]{1,0:T(8,128)(2,1)S(1)} %get-tuple-element.97), channel_id=1, source_target_pairs={{0,24},{8,16},{16,8},{24,0},{1,25},{9,17},{17,9},{25,1},{2,26},{10... | collective-permute-start | bytes 835592 | tf_op jit(solution)/shard_map/ppermute | solution.py:431
  72.4 29.7 %collective-permute-start.26 = (bf16[64,2176]{1,0:T(8,128)(2,1)S(1)}, bf16[64,2176]{1,0:T(8,128)(2,1)S(1)}, u32[]{:S(2)}, u32[]{:S(2)}) collective-permute-start(bf16[64,2176]{1,0:T(8,128)(2,1)S(1)} %get-tuple-element.87), channel_id=1, source_target_pairs={{0,8},{8,0},{16,24},{24,16},{1,9},{9,1},{17,25},{25,17},{2,10},{10... | collective-permute-start | bytes 835592 | tf_op jit(solution)/shard_map/ppermute | solution.py:431
  73.4 1.6 copy-start.1
  75.0 1.6 copy-start.4
  76.6 1.6 copy-start.8
  78.2 1.0 copy-start.21
  88.8 11.2 %copy-start.42 = (bf16[64,2048]{1,0:T(8,128)(2,1)}, bf16[64,2048]{1,0:T(8,128)(2,1)S(1)}, u32[]{:S(2)}) copy-start(bf16[64,2048]{1,0:T(8,128)(2,1)S(1)} %get-tuple-element.85) | copy-start | bytes 786436
  88.8 15.0 %collective-permute-start.27 = (bf16[64,2176]{1,0:T(8,128)(2,1)S(1)}, bf16[64,2176]{1,0:T(8,128)(2,1)S(1)}, u32[]{:S(2)}, u32[]{:S(2)}) collective-permute-start(bf16[64,2176]{1,0:T(8,128)(2,1)S(1)} %get-tuple-element.88), channel_id=1, source_target_pairs={{0,16},{8,24},{16,0},{24,8},{1,17},{9,25},{17,1},{25,9},{2,18},{10... | collective-permute-start | bytes 835592 | tf_op jit(solution)/shard_map/ppermute | solution.py:431
  90.3 19.8 %collective-permute-start.28 = (bf16[64,2176]{1,0:T(8,128)(2,1)}, bf16[64,2176]{1,0:T(8,128)(2,1)}, u32[]{:S(2)}, u32[]{:S(2)}) collective-permute-start(bf16[64,2176]{1,0:T(8,128)(2,1)} %get-tuple-element.89), channel_id=1, source_target_pairs={{0,24},{8,16},{16,8},{24,0},{1,25},{9,17},{17,9},{25,1},{2,26},{10... | collective-permute-start | bytes 835592 | tf_op jit(solution)/shard_map/ppermute | solution.py:431
  91.3 14.3 %collective-permute-start.3 = (f32[2,128,256]{2,1,0:T(8,128)S(1)}, f32[2,128,256]{2,1,0:T(8,128)S(1)}, u32[]{:S(2)}, u32[]{:S(2)}) collective-permute-start(f32[2,128,256]{2,1,0:T(8,128)S(1)} %pad_maximum_fusion.own_ref), channel_id=1, source_target_pairs={{0,8},{8,0},{16,24},{24,16},{1,9},{9,1},{17,25},{25,17},{2,10},{10... | collective-permute-start | bytes 786440 | tf_op jit(solution)/shard_map/ppermute | solution.py:431
  102.8 9.5 %collective-permute-start.20 = (bf16[64,2048]{1,0:T(8,128)(2,1)}, bf16[64,2048]{1,0:T(8,128)(2,1)}, u32[]{:S(2)}, u32[]{:S(2)}) collective-permute-start(bf16[64,2048]{1,0:T(8,128)(2,1)} %get-tuple-element.83), channel_id=1, source_target_pairs={{0,8},{8,0},{16,24},{24,16},{1,9},{9,1},{17,25},{25,17},{2,10},{10... | collective-permute-start | bytes 786440 | tf_op jit(solution)/shard_map/ppermute | solution.py:431
  104.5 9.3 %collective-permute-start.21 = (bf16[64,2048]{1,0:T(8,128)(2,1)}, bf16[64,2048]{1,0:T(8,128)(2,1)}, u32[]{:S(2)}, u32[]{:S(2)}) collective-permute-start(bf16[64,2048]{1,0:T(8,128)(2,1)} %get-tuple-element.84), channel_id=1, source_target_pairs={{0,16},{8,24},{16,0},{24,8},{1,17},{9,25},{17,1},{25,9},{2,18},{10... | collective-permute-start | bytes 786440 | tf_op jit(solution)/shard_map/ppermute | solution.py:431
  106.3 11.6 %collective-permute-start.35 = (bf16[64,2048]{1,0:T(8,128)(2,1)}, bf16[64,2048]{1,0:T(8,128)(2,1)}, u32[]{:S(2)}, u32[]{:S(2)}) collective-permute-start(bf16[64,2048]{1,0:T(8,128)(2,1)} %get-tuple-element.99), channel_id=1, source_target_pairs={{0,8},{8,0},{16,24},{24,16},{1,9},{9,1},{17,25},{25,17},{2,10},{10... | collective-permute-start | bytes 786440 | tf_op jit(solution)/shard_map/ppermute | solution.py:431
  110.1 38.7 %collective-permute-start.22 = (bf16[64,2048]{1,0:T(8,128)(2,1)}, bf16[64,2048]{1,0:T(8,128)(2,1)}, u32[]{:S(2)}, u32[]{:S(2)}) collective-permute-start(bf16[64,2048]{1,0:T(8,128)(2,1)} %copy-done.42), channel_id=1, source_target_pairs={{0,24},{8,16},{16,8},{24,0},{1,25},{9,17},{17,9},{25,1},{2,26},{10... | collective-permute-start | bytes 786440 | tf_op jit(solution)/shard_map/ppermute | solution.py:431
  112.3 24.3 %collective-permute-start.36 = (bf16[64,2048]{1,0:T(8,128)(2,1)}, bf16[64,2048]{1,0:T(8,128)(2,1)S(1)}, u32[]{:S(2)}, u32[]{:S(2)}) collective-permute-start(bf16[64,2048]{1,0:T(8,128)(2,1)} %copy-done.44), channel_id=1, source_target_pairs={{0,16},{8,24},{16,0},{24,8},{1,17},{9,25},{17,1},{25,9},{2,18},{10... | collective-permute-start | bytes 786440 | tf_op jit(solution)/shard_map/ppermute | solution.py:431
  113.8 23.3 %collective-permute-start.37 = (bf16[64,2048]{1,0:T(8,128)(2,1)}, bf16[64,2048]{1,0:T(8,128)(2,1)S(1)}, u32[]{:S(2)}, u32[]{:S(2)}) collective-permute-start(bf16[64,2048]{1,0:T(8,128)(2,1)} %copy-done.43), channel_id=1, source_target_pairs={{0,24},{8,16},{16,8},{24,0},{1,25},{9,17},{17,9},{25,1},{2,26},{10... | collective-permute-start | bytes 786440 | tf_op jit(solution)/shard_map/ppermute | solution.py:431
  117.9 22.1 %collective-permute-start.4 = (f32[2,128,128]{2,1,0:T(8,128)S(1)}, f32[2,128,128]{2,1,0:T(8,128)S(1)}, u32[]{:S(2)}, u32[]{:S(2)}) collective-permute-start(f32[2,128,128]{2,1,0:T(8,128)S(1)} %slice.3), channel_id=1, source_target_pairs={{0,16},{8,24},{16,0},{24,8},{1,17},{9,25},{17,1},{25,9},{2,18},{10... | collective-permute-start | bytes 393224 | tf_op jit(solution)/shard_map/ppermute | solution.py:431
  119.5 1.6 copy-start.2
  121.0 1.6 copy-start.5
  122.6 1.6 copy-start.9
  127.1 10.7 %copy-start.33 = (bf16[64,2048]{1,0:T(8,128)(2,1)S(1)}, bf16[64,2048]{1,0:T(8,128)(2,1)}, u32[]{:S(2)}) copy-start(bf16[64,2048]{1,0:T(8,128)(2,1)} %copy-done.32) | copy-start | bytes 786436
  136.6 3.5 %copy-start.40 = (bf16[64,2048]{1,0:T(8,128)(2,1)}, bf16[64,2048]{1,0:T(8,128)(2,1)S(1)}, u32[]{:S(2)}) copy-start(bf16[64,2048]{1,0:T(8,128)(2,1)S(1)} %get-tuple-element.93) | copy-start | bytes 786436
  136.6 12.4 %copy-start.23 = (bf16[64,2048]{1,0:T(8,128)(2,1)S(1)}, bf16[64,2048]{1,0:T(8,128)(2,1)}, u32[]{:S(2)}) copy-start(bf16[64,2048]{1,0:T(8,128)(2,1)} %copy-done.22) | copy-start | bytes 786436
  136.6 15.4 %collective-permute-start.29 = (bf16[64,2048]{1,0:T(8,128)(2,1)}, bf16[64,2048]{1,0:T(8,128)(2,1)}, u32[]{:S(2)}, u32[]{:S(2)}) collective-permute-start(bf16[64,2048]{1,0:T(8,128)(2,1)} %get-tuple-element.91), channel_id=1, source_target_pairs={{0,8},{8,0},{16,24},{24,16},{1,9},{9,1},{17,25},{25,17},{2,10},{10... | collective-permute-start | bytes 786440 | tf_op jit(solution)/shard_map/ppermute | solution.py:431
  137.1 16.4 %collective-permute-start.30 = (bf16[64,2048]{1,0:T(8,128)(2,1)}, bf16[64,2048]{1,0:T(8,128)(2,1)}, u32[]{:S(2)}, u32[]{:S(2)}) collective-permute-start(bf16[64,2048]{1,0:T(8,128)(2,1)} %get-tuple-element.92), channel_id=1, source_target_pairs={{0,16},{8,24},{16,0},{24,8},{1,17},{9,25},{17,1},{25,9},{2,18},{10... | collective-permute-start | bytes 786440 | tf_op jit(solution)/shard_map/ppermute | solution.py:431
  140.7 35.2 %collective-permute-start.38 = (bf16[128,2048]{1,0:T(8,128)(2,1)}, bf16[128,2048]{1,0:T(8,128)(2,1)}, u32[]{:S(2)}, u32[]{:S(2)}) collective-permute-start(bf16[128,2048]{1,0:T(8,128)(2,1)} %collect.5), channel_id=1, source_target_pairs={{0,2},{1,3},{2,4},{3,5},{4,6},{5,7},{6,0},{7,1},{8,10},{9,11},{10,... | collective-permute-start | bytes 1572872 | tf_op jit(solution)/shard_map/ppermute | solution.py:428
  148.9 5.3 %collective-permute-start.5 = (bf16[4,64,256]{2,1,0:T(8,128)(2,1)}, bf16[4,64,256]{2,1,0:T(8,128)(2,1)}, u32[]{:S(2)}, u32[]{:S(2)}) collective-permute-start(bf16[4,64,256]{2,1,0:T(8,128)(2,1)} %get-tuple-element.62), channel_id=1, source_target_pairs={{0,1},{1,0},{2,3},{3,2},{4,5},{5,4},{6,7},{7,6},{8,9},{9,8},{10,11... | collective-permute-start | bytes 393224 | tf_op jit(solution)/shard_map/ppermute | solution.py:425
  148.9 3.1 %copy-start.46 = (bf16[64,2176]{1,0:T(8,128)(2,1)S(1)}, bf16[64,2176]{1,0:T(8,128)(2,1)}, u32[]{:S(2)}) copy-start(bf16[64,2176]{1,0:T(8,128)(2,1)} %get-tuple-element.66) | copy-start | bytes 835588
  148.9 4.6 %copy-start.45 = (bf16[64,2176]{1,0:T(8,128)(2,1)S(1)}, bf16[64,2176]{1,0:T(8,128)(2,1)}, u32[]{:S(2)}) copy-start(bf16[64,2176]{1,0:T(8,128)(2,1)} %get-tuple-element.67) | copy-start | bytes 835588
  148.9 5.3 %copy-start.41 = (bf16[64,2048]{1,0:T(8,128)(2,1)S(1)}, bf16[64,2048]{1,0:T(8,128)(2,1)}, u32[]{:S(2)}) copy-start(bf16[64,2048]{1,0:T(8,128)(2,1)} %copy-done.40) | copy-start | bytes 786436
  148.9 7.6 %copy-start.11 = (bf16[256,2048]{1,0:T(8,128)(2,1)S(1)}, bf16[256,2048]{1,0:T(8,128)(2,1)}, u32[]{:S(2)}) copy-start(bf16[256,2048]{1,0:T(8,128)(2,1)} %own_ref.1) | copy-start | bytes 3145732
  148.9 7.6 %copy-start.39 = (bf16[4,64,256]{2,1,0:T(8,128)(2,1)S(1)}, bf16[4,64,256]{2,1,0:T(8,128)(2,1)}, u32[]{:S(2)}) copy-start(bf16[4,64,256]{2,1,0:T(8,128)(2,1)} %copy-done.38) | copy-start | bytes 393220
  150.6 26.9 %collective-permute-start.10 = (bf16[64,2176]{1,0:T(8,128)(2,1)}, bf16[64,2176]{1,0:T(8,128)(2,1)S(1)}, u32[]{:S(2)}, u32[]{:S(2)}) collective-permute-start(bf16[64,2176]{1,0:T(8,128)(2,1)} %get-tuple-element.65), channel_id=1, source_target_pairs={{0,8},{8,0},{16,24},{24,16},{1,9},{9,1},{17,25},{25,17},{2,10},{10... | collective-permute-start | bytes 835592 | tf_op jit(solution)/shard_map/ppermute | solution.py:431
  152.0 31.8 %collective-permute-start.11 = (bf16[64,2176]{1,0:T(8,128)(2,1)S(1)}, bf16[64,2176]{1,0:T(8,128)(2,1)S(1)}, u32[]{:S(2)}, u32[]{:S(2)}) collective-permute-start(bf16[64,2176]{1,0:T(8,128)(2,1)S(1)} %copy-done.46), channel_id=1, source_target_pairs={{0,16},{8,24},{16,0},{24,8},{1,17},{9,25},{17,1},{25,9},{2,18},{10... | collective-permute-start | bytes 835592 | tf_op jit(solution)/shard_map/ppermute | solution.py:431
  153.5 30.3 %collective-permute-start.12 = (bf16[64,2176]{1,0:T(8,128)(2,1)S(1)}, bf16[64,2176]{1,0:T(8,128)(2,1)S(1)}, u32[]{:S(2)}, u32[]{:S(2)}) collective-permute-start(bf16[64,2176]{1,0:T(8,128)(2,1)S(1)} %copy-done.45), channel_id=1, source_target_pairs={{0,24},{8,16},{16,8},{24,0},{1,25},{9,17},{17,9},{25,1},{2,26},{10... | collective-permute-start | bytes 835592 | tf_op jit(solution)/shard_map/ppermute | solution.py:431
  154.2 18.1 %collective-permute-start.31 = (bf16[64,2048]{1,0:T(8,128)(2,1)S(1)}, bf16[64,2048]{1,0:T(8,128)(2,1)S(1)}, u32[]{:S(2)}, u32[]{:S(2)}) collective-permute-start(bf16[64,2048]{1,0:T(8,128)(2,1)S(1)} %copy-done.41), channel_id=1, source_target_pairs={{0,24},{8,16},{16,8},{24,0},{1,25},{9,17},{17,9},{25,1},{2,26},{10... | collective-permute-start | bytes 786440 | tf_op jit(solution)/shard_map/ppermute | solution.py:431
  156.5 19.4 %copy-start.25 = (bf16[64,2048]{1,0:T(8,128)(2,1)S(1)}, bf16[64,2048]{1,0:T(8,128)(2,1)}, u32[]{:S(2)}) copy-start(bf16[64,2048]{1,0:T(8,128)(2,1)} %copy-done.24) | copy-start | bytes 786436
  156.5 29.4 %copy-start.10 = (bf16[4,128,2048]{2,1,0:T(8,128)(2,1)S(1)}, bf16[4,128,2048]{2,1,0:T(8,128)(2,1)}, u32[]{:S(2)}) copy-start(bf16[4,128,2048]{2,1,0:T(8,128)(2,1)} %copy-done.7) | copy-start | bytes 6291460
  156.5 29.4 %copy-start.13 = (bf16[64,2176]{1,0:T(8,128)(2,1)S(1)}, bf16[64,2176]{1,0:T(8,128)(2,1)}, u32[]{:S(2)}) copy-start(bf16[64,2176]{1,0:T(8,128)(2,1)} %get-tuple-element.64.refs_0_) | copy-start | bytes 835588
  159.2 26.7 %copy-start.3 = (bf16[4,128,2048]{2,1,0:T(8,128)(2,1)S(1)}, bf16[4,128,2048]{2,1,0:T(8,128)(2,1)}, u32[]{:S(2)}) copy-start(bf16[4,128,2048]{2,1,0:T(8,128)(2,1)} %refs_6_.3) | copy-start | bytes 6291460
  159.2 26.7 %copy-start.6 = (bf16[4,128,2048]{2,1,0:T(8,128)(2,1)S(1)}, bf16[4,128,2048]{2,1,0:T(8,128)(2,1)}, u32[]{:S(2)}) copy-start(bf16[4,128,2048]{2,1,0:T(8,128)(2,1)} %refs_8_.3) | copy-start | bytes 6291460
  172.4 57.2 %collective-permute-start.23 = (bf16[128,2048]{1,0:T(8,128)(2,1)S(1)}, bf16[128,2048]{1,0:T(8,128)(2,1)S(1)}, u32[]{:S(2)}, u32[]{:S(2)}) collective-permute-start(bf16[128,2048]{1,0:T(8,128)(2,1)S(1)} %collect.4), channel_id=1, source_target_pairs={{0,6},{1,7},{2,0},{3,1},{4,2},{5,3},{6,4},{7,5},{8,14},{9,15},{10,... | collective-permute-start | bytes 1572872 | tf_op jit(solution)/shard_map/ppermute | solution.py:428
  175.9 22.2 %collective-permute-start.9 = (bf16[64,2048]{1,0:T(8,128)(2,1)S(1)}, bf16[64,2048]{1,0:T(8,128)(2,1)S(1)}, u32[]{:S(2)}, u32[]{:S(2)}) collective-permute-start(bf16[64,2048]{1,0:T(8,128)(2,1)S(1)} %get-tuple-element.103), channel_id=1, source_target_pairs={{0,2},{1,3},{2,4},{3,5},{4,6},{5,7},{6,0},{7,1},{8,10},{9,11},{10,... | collective-permute-start | bytes 786440 | tf_op jit(solution)/shard_map/ppermute | solution.py:428
  177.6 33.2 %collective-permute-start.8 = (bf16[64,2048]{1,0:T(8,128)(2,1)S(1)}, bf16[64,2048]{1,0:T(8,128)(2,1)S(1)}, u32[]{:S(2)}, u32[]{:S(2)}) collective-permute-start(bf16[64,2048]{1,0:T(8,128)(2,1)S(1)} %get-tuple-element.104), channel_id=1, source_target_pairs={{0,4},{1,5},{2,6},{3,7},{4,0},{5,1},{6,2},{7,3},{8,12},{9,13},{10,... | collective-permute-start | bytes 786440 | tf_op jit(solution)/shard_map/ppermute | solution.py:428
  183.8 37.5 %collective-permute-start.7 = (bf16[64,2048]{1,0:T(8,128)(2,1)S(1)}, bf16[64,2048]{1,0:T(8,128)(2,1)S(1)}, u32[]{:S(2)}, u32[]{:S(2)}) collective-permute-start(bf16[64,2048]{1,0:T(8,128)(2,1)S(1)} %get-tuple-element.102), channel_id=1, source_target_pairs={{0,6},{1,7},{2,0},{3,1},{4,2},{5,3},{6,4},{7,5},{8,14},{9,15},{10,... | collective-permute-start | bytes 786440 | tf_op jit(solution)/shard_map/ppermute | solution.py:428
  183.8 45.7 %collective-permute-start.39 = (bf16[128,2048]{1,0:T(8,128)(2,1)S(1)}, bf16[128,2048]{1,0:T(8,128)(2,1)S(1)}, u32[]{:S(2)}, u32[]{:S(2)}) collective-permute-start(bf16[128,2048]{1,0:T(8,128)(2,1)S(1)} %collect.6), channel_id=1, source_target_pairs={{0,2},{1,3},{2,4},{3,5},{4,6},{5,7},{6,0},{7,1},{8,10},{9,11},{10,... | collective-permute-start | bytes 1572872 | tf_op jit(solution)/shard_map/ppermute | solution.py:428
  185.9 43.7 %copy-start.12 = (bf16[128,2176]{1,0:T(8,128)(2,1)S(1)}, bf16[128,2176]{1,0:T(8,128)(2,1)}, u32[]{:S(2)}) copy-start(bf16[128,2176]{1,0:T(8,128)(2,1)} %get-tuple-element.63.meta_ref) | copy-start | bytes 1671172
  198.1 24.4 %collective-permute-start.13 = (bf16[64,2048]{1,0:T(8,128)(2,1)S(1)}, bf16[64,2048]{1,0:T(8,128)(2,1)S(1)}, u32[]{:S(2)}, u32[]{:S(2)}) collective-permute-start(bf16[64,2048]{1,0:T(8,128)(2,1)S(1)} %get-tuple-element.75), channel_id=1, source_target_pairs={{0,8},{8,0},{16,24},{24,16},{1,9},{9,1},{17,25},{25,17},{2,10},{10... | collective-permute-start | bytes 786440 | tf_op jit(solution)/shard_map/ppermute | solution.py:431
  210.7 11.7 %collective-permute-start.14 = (bf16[64,2048]{1,0:T(8,128)(2,1)S(1)}, bf16[64,2048]{1,0:T(8,128)(2,1)S(1)}, u32[]{:S(2)}, u32[]{:S(2)}) collective-permute-start(bf16[64,2048]{1,0:T(8,128)(2,1)S(1)} %get-tuple-element.76), channel_id=1, source_target_pairs={{0,16},{8,24},{16,0},{24,8},{1,17},{9,25},{17,1},{25,9},{2,18},{10... | collective-permute-start | bytes 786440 | tf_op jit(solution)/shard_map/ppermute | solution.py:431
  221.4 8.2 %collective-permute-start.15 = (bf16[64,2048]{1,0:T(8,128)(2,1)S(1)}, bf16[64,2048]{1,0:T(8,128)(2,1)S(1)}, u32[]{:S(2)}, u32[]{:S(2)}) collective-permute-start(bf16[64,2048]{1,0:T(8,128)(2,1)S(1)} %get-tuple-element.77), channel_id=1, source_target_pairs={{0,24},{8,16},{16,8},{24,0},{1,25},{9,17},{17,9},{25,1},{2,26},{10... | collective-permute-start | bytes 786440 | tf_op jit(solution)/shard_map/ppermute | solution.py:431
  (23 other events, 18.6 us)
where the time goes:
time: 232 us; the launch traced here: 231 us
  waiting for transfers between devices  80.7 us (35%)
  Pallas kernels  69.9 us (30%)
  starting transfers between devices  45.5 us (20%)
  local copies, waits for them, and re-layouts  30.6 us (13%)
  other arithmetic  3.18 us (1%)
    ppermute x9, waiting for transfers between devices, send(): lax.ppermute(x, 'tp', [(y, (y + chips * CORES) % tp) for y in range(tp)])  56 us
    pallas_call x4, Pallas kernels, expert_part(): pl.pallas_call(functools.partial(expert_kernel, peers, slots), in_specs=[...  32.4 us
    unnamed x94, local copies, waits for them, and re-layouts  30.4 us
    ppermute x26, starting transfers between devices, trade(): return lax.ppermute(x, 'ep', [(y, y ^ distance) for y in range(ep)])  28.9 us
    ppermute x26, waiting for transfers between devices, trade(): return lax.ppermute(x, 'ep', [(y, y ^ distance) for y in range(ep)])  24.7 us
    pallas_call x2, Pallas kernels, mixer_local(): pl.pallas_call(functools.partial(mixer_kernel, head), grid=(1,), in_specs...  17.8 us
    ppermute x9, starting transfers between devices, send(): lax.ppermute(x, 'tp', [(y, (y + chips * CORES) % tp) for y in range(tp)])  15.9 us
    pallas_call x4, Pallas kernels, collect(): pl.pallas_call(functools.partial(collect_kernel, peers, slots), grid=(1,)...  6.82 us
  transfers between devices with their start and end apart: 40, of which 10 were waited for; matrix products, arithmetic and copies ran while one was open for 1% of the time, Pallas kernels for 30%

commit v1 on v0

--- a/solution.py
+++ b/solution.py
@@ -17,6 +17,8 @@
 CORES = 2
 META = 128
 CHUNK = 128
+FIRST_ROOM, EXPERT_ROOM = 64000 * 1024, 24 * 2**20
+FETCH = (1,)
 NORM_EPS = 1e-06
 
 
@@ -40,7 +42,19 @@
     return jnp.dot(a, b, precision=EXACT, preferred_element_type=F32)
 
 
-def mixer_kernel(head, rate_ref, q_ref, k_ref, v_ref, write_ref, decay_ref, extra_ref, local_ref, proj_ref, joint_ref):
+def halves(x):
+    high = x.astype(BF16)
+    return high, (x - high.astype(F32)).astype(BF16)
+
+
+def mm3(a, b):
+    (ah, al), (bh, bl) = halves(a), halves(b)
+    dot = lambda x, y: jnp.dot(x, y, preferred_element_type=F32)
+    return dot(ah, bh) + (dot(ah, bl) + dot(al, bh))
+
+
+def mixer_kernel(head, rate_ref, q_ref, k_ref, v_ref, write_ref, decay_ref, extra_ref, *refs):
+    early_refs, (local_ref, proj_ref, joint_ref) = refs[:-3], refs[-3:]
     length = q_ref.shape[0]
     chunks = length // CHUNK
     i = lax.broadcasted_iota(jnp.int32, (CHUNK, CHUNK), 0)
@@ -70,9 +84,9 @@
     beta = [columns[:, len(every) + n : len(every) + n + 1] for n in every]
     last = [r[:, CHUNK - 1 :] for r in row]
     decay = [jnp.where(i >= j, jnp.exp(jnp.where(i >= j, col[n] - row[n], 0.0)), 0.0) for n in every]
-    gram = [mm(k[n], kt[n]) for n in every]
+    gram = [mm3(k[n], kt[n]) for n in every]
     lower = [jnp.where(i > j, gram[n] * decay[n] * beta[n], 0.0) for n in every]
-    scores = [mm(q[n], kt[n]) * decay[n] for n in every]
+    scores = [mm3(q[n], kt[n]) * decay[n] for n in every]
     eye = jnp.where(i == j, 1.0, 0.0)
     small = 16
     near = (i // small) == (j // small)
@@ -80,47 +94,50 @@
     inverse = [eye - x for x in power]
     reach = 2
     while reach < small:
-        power = [mm(x, x) for x in power]
-        inverse = [x + mm(x, y) for x, y in zip(inverse, power)]
+        power = [mm3(x, x) for x in power]
+        inverse = [x + mm3(x, y) for x, y in zip(inverse, power)]
         reach *= 2
     while small < CHUNK:
         band = ((i // (2 * small)) == (j // (2 * small))) & ((i // small) != (j // small))
-        half = [mm(jnp.where(band, x, 0.0), y) for x, y in zip(lower, inverse)]
-        inverse = [y - mm(y, x) for x, y in zip(half, inverse)]
+        half = [mm3(jnp.where(band, x, 0.0), y) for x, y in zip(lower, inverse)]
+        inverse = [y - mm3(y, x) for x, y in zip(half, inverse)]
         small *= 2
     grown = [jnp.exp(x) for x in col]
     rhs = [jnp.concatenate([v[n] * beta[n], k[n] * (beta[n] * grown[n])], axis=1) for n in every]
-    solved = [mm(inverse[n], rhs[n]) for n in every]
+    solved = [mm3(inverse[n], rhs[n]) for n in every]
     blank = jnp.zeros((CHUNK, DK), F32)
     start = jnp.concatenate([jnp.zeros((DK, DV), F32), eye], axis=1)
     joint = start
     for n in every:
-        update = jnp.concatenate([solved[n][:, :DV], blank], axis=1) - mm(solved[n][:, DV:], joint)
-        out = mm(q[n] * grown[n], joint) + mm(scores[n], update)
-        joint = joint * jnp.exp(last[n]) + mm(kt[n] * jnp.exp(last[n] - row[n]), update)
+        update = jnp.concatenate([solved[n][:, :DV], blank], axis=1) - mm3(solved[n][:, DV:], joint)
+        out = mm3(q[n] * grown[n], joint) + mm3(scores[n], update)
+        joint = joint * jnp.exp(last[n]) + mm3(kt[n] * jnp.exp(last[n] - row[n]), update)
         local_ref[spans[n], :] = out[:, :DV]
         proj_ref[spans[n], :] = out[:, DV:]
-    joint_ref[...] = joint
-
-
-def mixer_local(head, rates, queries, keys, values, write, decay, extra):
+    for number, early_ref in enumerate(early_refs):
+        joint_ref[number] = early_ref[0]
+    joint_ref[len(early_refs)] = joint
+
+
+def mixer_local(head, rates, queries, keys, values, write, decay, extra, early):
     length = queries.shape[0]
     tall = pl.BlockSpec((length, DK), lambda x: (0, head))
     gate = pl.BlockSpec(write.shape, lambda x: (0, 0))
     flat = pl.BlockSpec((length, DK), lambda x: (0, 0))
+    ends = lambda n: pl.BlockSpec((n, DK, DV + DK), lambda x: (0, 0, 0))
     return pl.pallas_call(
         functools.partial(mixer_kernel, head),
         grid=(1,),
-        in_specs=[SMEM] + [tall] * 3 + [gate] * 3,
-        out_specs=[flat, flat, pl.BlockSpec((DK, DV + DK), lambda x: (0, 0))],
+        in_specs=[SMEM] + [tall] * 3 + [gate] * 3 + [ends(1)] * len(early),
+        out_specs=[flat, flat, ends(1 + len(early))],
         out_shape=[
             jax.ShapeDtypeStruct((length, DV), F32),
             jax.ShapeDtypeStruct((length, DK), F32),
-            jax.ShapeDtypeStruct((DK, DV + DK), F32),
+            jax.ShapeDtypeStruct((1 + len(early), DK, DV + DK), F32),
         ],
         cost_estimate=cost(length // CHUNK * 26 * 6 * 2 * 128**3, length * DK * 14),
         name="mixer_local",
-    )(rates, queries, keys, values, write, decay, extra)
+    )(rates, queries, keys, values, write, decay, extra, *early)
 
 
 def join_kernel(late_ref, own_ref, got_ref, inner_ref, own_out, inner_out):
@@ -154,14 +171,14 @@
     states = []
     for h in range(heads):
         inner = inner_ref[h]
-        state = mm(inner[:, DV:], got_ref[h]) + inner[:, :DV]
+        state = mm3(inner[:, DV:], got_ref[h]) + inner[:, :DV]
         states.append(jnp.where(late, state, inner[:, :DV]))
     depth, rows = mine_ref.shape[0], mine_ref.shape[1]
     for out_ref, shift in ((mine_ref, core_ref[0]), (other_ref, 1 - core_ref[0])):
         for z in range(depth):
             span = pl.ds(pl.multiple_of((z * CORES + shift) * rows, rows), rows)
             for h in range(heads):
-                out = local_refs[h][span, :] + mm(proj_refs[h][span, :], states[h])
+                out = local_refs[h][span, :] + mm3(proj_refs[h][span, :], states[h])
                 out_ref[z, :, h * DV : (h + 1) * DV] = out.astype(BF16)
 
 
@@ -176,50 +193,67 @@
         in_specs=[SMEM] * 2 + [full(length, width)] * (2 * heads) + [full(*got.shape), full(*inner.shape)],
         out_specs=[full(*half.shape)] * 2,
         out_shape=[half, half],
-        compiler_params=room(8),
         cost_estimate=cost(6 * 2 * length * width * DK * heads, length * width * 10 * heads),
         name="attend",
     )(late, core, *local, *proj, got, inner)
 
 
-def project_kernel(mine_ref, theirs_ref, own_ref, pair_ref, out_ref):
+def project_kernel(level_ref, mine_ref, theirs_ref, own_ref, pair_ref, *refs):
     depth, rows, width = mine_ref.shape
+    out_refs, (weight, ready) = refs[:depth], refs[depth:]
+    tile = weight.shape[2]
+    steps = weight.shape[0]
+
+    def fetch(step, half):
+        source = (own_ref, pair_ref)[half]
+        return pltpu.make_async_copy(
+            source.at[:, pl.ds(step * tile, tile)],
+            weight.at[step, pl.ds(half * width, width)],
+            ready.at[step, half],
+        )
+
+    for step in range(steps):
+        for half in range(CORES):
+            fetch(step, half).start()
+    order = [lax.rem(level_ref[0] + depth - hop, depth) for hop in range(depth)]
     left = jnp.concatenate(
-        [x[...].reshape(depth * rows, width) for x in (mine_ref, theirs_ref)], axis=1
+        [jnp.concatenate([mine_ref[at], theirs_ref[at]], axis=1) for at in order], axis=0
     )
-    tile = 512
-
-    def body(step, carry):
-        span = pl.ds(pl.multiple_of(step * tile, tile), tile)
-        right = jnp.concatenate([own_ref[:, span], pair_ref[:, span]], axis=0)
-        part = jnp.dot(left, right, preferred_element_type=F32).astype(BF16)
-        out_ref[:, :, span] = part.reshape(depth, rows, tile)
-        return carry
-
-    lax.fori_loop(0, out_ref.shape[2] // tile, body, 0)
-
-
-def project(mine, theirs, own, pair):
+    for step in range(steps):
+        for half in range(CORES):
+            fetch(step, half).wait()
+        part = jnp.dot(left, weight[step], preferred_element_type=F32).astype(BF16)
+        for hop, out_ref in enumerate(out_refs):
+            out_ref[:, step * tile : (step + 1) * tile] = part[hop * rows : (hop + 1) * rows, :]
+
+
+def project(level, mine, theirs, own, pair):
     depth, rows, width = mine.shape
     wide = own.shape[1]
+    tile = 512
     return pl.pallas_call(
         project_kernel,
-        in_specs=[VMEM] * 4,
-        out_specs=VMEM,
-        out_shape=jax.ShapeDtypeStruct((depth, rows, wide), BF16),
+        in_specs=[SMEM, VMEM, VMEM, HBM, HBM],
+        out_specs=[VMEM] * depth,
+        out_shape=[jax.ShapeDtypeStruct((rows, wide), BF16)] * depth,
+        scratch_shapes=[
+            pltpu.VMEM((wide // tile, CORES * width, tile), BF16),
+            pltpu.SemaphoreType.DMA((wide // tile, CORES)),
+        ],
         compiler_params=room(8),
         cost_estimate=cost(4 * depth * rows * width * wide, 4 * width * wide + 2 * depth * rows * wide),
         name="project",
-    )(mine, theirs, own, pair)
-
-
-def prepare_kernel(own, peers, slots, me_ref, x_ref, scale_ref, index_ref, gain_ref, block_ref, *out_refs):
+    )(level, mine, theirs, own, pair)
+
+
+def prepare_kernel(own, peers, slots, me_ref, x_ref, scale_ref, index_ref, gain_ref, logit_ref, block_ref, *out_refs):
     rows, width = x_ref.shape
     x = x_ref[...].astype(F32)
     inv = lax.rsqrt(jnp.mean(x * x, axis=-1, keepdims=True) + NORM_EPS)
     block_ref[:, :width] = (x * inv * scale_ref[...]).astype(BF16)
     shift = own.bit_length() - 1
-    names = jnp.transpose(jnp.concatenate([index_ref[...].astype(F32), gain_ref[...]], axis=0))
+    given = [index_ref[...].astype(F32), gain_ref[...], logit_ref[...], jnp.zeros((8 - TOPK - 2, rows), F32)]
+    names = jnp.transpose(jnp.concatenate(given, axis=0))
     picks = [names[:, n : n + 1].astype(jnp.int32) for n in range(TOPK)]
     gain, logit = names[:, TOPK : TOPK + 1], names[:, TOPK + 1 : TOPK + 2]
     home = [lax.shift_right_logical(x, jnp.full_like(x, shift)) for x in picks]
@@ -245,8 +279,7 @@
 
 def prepare(own, peers, slots, me, tokens, scale, index, weight, logit):
     rows, width = tokens.shape
-    gains = jnp.stack([weight, logit] + [jnp.zeros_like(weight)] * 4)
-    inputs = (tokens, scale.reshape(1, -1), index.T, gains)
+    inputs = (tokens, scale.reshape(1, -1), index.T, weight.reshape(1, -1), logit.reshape(1, -1))
     full = lambda *shape: pl.BlockSpec(shape, lambda x: (0,) * len(shape))
     block = jax.ShapeDtypeStruct((rows, width + META), BF16)
     return pl.pallas_call(
@@ -291,33 +324,34 @@
     )(me, block)
 
 
-def expert_kernel(peers, slots, me_ref, *refs):
-    x_refs, sources, refs = refs[:peers], refs[peers : peers + 6], refs[peers + 6 :]
-    out_refs, (x_all, hidden, *kept, ready) = refs[:peers], refs[peers:]
-    gate_a, gate_b, up_a, up_b, down_a, down_b = kept
-    own, half, width = gate_a.shape
+def expert_kernel(moved, peers, slots, me_ref, *refs):
+    x_refs, refs = refs[:peers], refs[peers:]
+    sources, out_refs = refs[:6], refs[6 : 6 + peers]
+    x_all, hidden, held, ready = refs[6 + peers :]
+    kept = [held.at[moved.index(x)] if x in moved else sources[x] for x in range(6)]
+    own, half, width = sources[0].shape
     units = 2 * half
     rows = peers * slots
-    tile = 256
+    tile = 512
 
     def fetch(which, expert):
         return pltpu.make_async_copy(
             sources[which].at[expert], kept[which].at[expert], ready.at[which, expert]
         )
 
-    for expert in range(own):
-        for which in range(4):
-            fetch(which, expert).start()
-    for expert in range(own):
-        for which in (4, 5):
-            fetch(which, expert).start()
+    inner_moved = [x for x in moved if x < 4]
+    outer_moved = [x for x in moved if x >= 4]
+    for whiches in (inner_moved, outer_moved):
+        for expert in range(own):
+            for which in whiches:
+                fetch(which, expert).start()
     for number, x_ref in enumerate(x_refs):
         x_all[number * slots : (number + 1) * slots, :] = x_ref[...]
     meta = x_all[:, width:].astype(F32)
     me = me_ref[0].astype(F32)
 
     def inward(expert, carry):
-        for which in range(4):
+        for which in inner_moved:
             fetch(which, expert).wait()
         here = expert.astype(F32)
         weight = jnp.zeros((rows, 1), F32)
@@ -325,7 +359,7 @@
             fits = (meta[:, choice : choice + 1] == me) & (meta[:, 4 + choice : 5 + choice] == here)
             value = meta[:, 6 + choice : 7 + choice] + meta[:, 8 + choice : 9 + choice]
             weight = weight + jnp.where(fits, value, 0.0)
-        inner = jnp.concatenate([gate_a[expert], gate_b[expert], up_a[expert], up_b[expert]], axis=0)
+        inner = jnp.concatenate([kept[x][expert] for x in range(4)], axis=0)
         both = lax.dot_general(
             x_all[:, :width], inner, (((1,), (1,)), ((), ())), preferred_element_type=F32
         )
@@ -335,15 +369,13 @@
 
     lax.fori_loop(0, own, inward, 0)
     for expert in range(own):
-        for which in (4, 5):
+        for which in outer_moved:
             fetch(which, expert).wait()
 
     def outward(step, carry):
         span = pl.ds(pl.multiple_of(step * tile, tile), tile)
         left = jnp.concatenate([hidden[x] for x in range(own)], axis=1)
-        right = jnp.concatenate(
-            [y for x in range(own) for y in (down_a[x, :, span], down_b[x, :, span])], axis=0
-        )
+        right = jnp.concatenate([kept[y][x, :, span] for x in range(own) for y in (4, 5)], axis=0)
         part = jnp.dot(left, right, preferred_element_type=F32).astype(BF16)
         for number, out_ref in enumerate(out_refs):
             out_ref[:, span] = part[number * slots : (number + 1) * slots, :]
@@ -352,18 +384,22 @@
     lax.fori_loop(0, width // tile, outward, 0)
 
 
-def expert_part(peers, slots, me, arrived, weights):
-    own, units, width = weights[0].shape
+def expert_part(first, peers, slots, me, arrived, weights):
+    own, units, width = weights[0].shape[-3:]
     rows = peers * slots
-    return pl.pallas_call(
-        functools.partial(expert_kernel, peers, slots),
-        in_specs=[SMEM] + [VMEM] * peers + [HBM] * 6,
+    moved = tuple(range(6)) if first else (1, 3, 5)
+    return pl.pallas_call(
+        functools.partial(expert_kernel, moved, peers, slots),
+        in_specs=[SMEM] + [VMEM] * peers + [HBM if x in moved else VMEM for x in range(6)],
         out_specs=[VMEM] * peers,
         out_shape=[jax.ShapeDtypeStruct((slots, width), BF16)] * peers,
-        scratch_shapes=[pltpu.VMEM((rows, width + META), BF16), pltpu.VMEM((own, rows, 2 * units), BF16)]
-        + [pltpu.VMEM((own, units, width), BF16)] * 6
-        + [pltpu.SemaphoreType.DMA((6, own))],
-        compiler_params=room(28),
+        scratch_shapes=[
+            pltpu.VMEM((rows, width + META), BF16),
+            pltpu.VMEM((own, rows, 2 * units), BF16),
+            pltpu.VMEM((len(moved), own, units, width), BF16),
+            pltpu.SemaphoreType.DMA((6, own)),
+        ],
+        compiler_params=pltpu.CompilerParams(vmem_limit_bytes=FIRST_ROOM if first else EXPERT_ROOM),
         cost_estimate=cost(12 * own * units * rows * width, 12 * own * units * width + 4 * rows * width),
         name="expert_part",
     )(me, *arrived, *weights)
@@ -483,11 +519,12 @@
             write_strength_logit,
             decay_preactivation,
             extra_log_decay,
+            ends if head == heads - 1 else [],
         )
         local.append(x)
         proj.append(y)
         ends.append(end)
-    joint = jnp.stack(ends)
+    joint = ends[-1]
     joint, weights = lax.optimization_barrier((joint, weights))
     eye = jnp.concatenate([jnp.zeros((DK, DV), F32), jnp.eye(DK, dtype=F32)], axis=1)
     inner = jnp.broadcast_to(eye, joint.shape)
@@ -502,20 +539,16 @@
         span *= 2
     mine, other = attend(depth, late, scalar(core), local, proj, got, inner)
     theirs = swap(other)
-    partial = project(mine, theirs, output_weight, out_pair)
-
-    def piece(hop):
-        at = (level + depth - hop) % depth
-        return lax.dynamic_index_in_dim(partial, at, 0, keepdims=False)
-
-    mixed = piece(0).astype(F32)
+    pieces = project(scalar(level), mine, theirs, output_weight, out_pair)
+
+    mixed = pieces[0].astype(F32)
     for hop in range(1, depth):
-        mixed = mixed + send(piece(hop), -hop).astype(F32)
-
-    found = []
-    for hop in range(depth):
-        produced = expert_part(ep, slots, me1, arrived[hop], weights)
-        found.append(give_back(produced))
+        mixed = mixed + send(pieces[hop], -hop).astype(F32)
+
+    found = {}
+    for hop in list(range(1, depth)) + [0]:
+        produced = expert_part(hop in FETCH, ep, slots, me1, arrived[hop], weights)
+        found[hop] = give_back(produced)
     running, near = [], []
     for hop in range(1, depth):
         total = collect(ep, slots, me1, blocks[hop], found[hop], running)
@@ -523,7 +556,9 @@
             near = [send(total, -1)]
         else:
             running = [send(total, 1)]
-    expert_out = collect(ep, slots, me1, blocks[0], found[0], near + running)
+    expert_out = collect(ep, slots, me1, blocks[0], found[0], near)
+    if running:
+        expert_out = (expert_out.astype(F32) + running[0].astype(F32)).astype(BF16)
     return (mixed.astype(BF16), expert_out)
 
 

time: 232 us -> 210 us (0.905)
  the two profiles are of different devices: /device:TPU:10 before, /device:TPU:0 now
where the time goes in v1:
time: 210 us
  waiting for transfers between devices  83.3 us (40%)
  Pallas kernels  64.7 us (31%)
  starting transfers between devices  39.7 us (19%)
  local copies, waits for them, and re-layouts  19.2 us (9%)
    ppermute x9, waiting for transfers between devices, send(): lax.ppermute(x, 'tp', [(y, (y + chips * CORES) % tp) for y in range(tp)])  65.8 us
    pallas_call x4, Pallas kernels, expert_part(): pl.pallas_call(functools.partial(expert_kernel, moved, peers, slots), in_...  31.9 us
    ppermute x26, starting transfers between devices, trade(): return lax.ppermute(x, 'ep', [(y, y ^ distance) for y in range(ep)])  28.5 us
    unnamed x74, local copies, waits for them, and re-layouts  19.1 us
    ppermute x26, waiting for transfers between devices, trade(): return lax.ppermute(x, 'ep', [(y, y ^ distance) for y in range(ep)])  15.9 us
    pallas_call x2, Pallas kernels, mixer_local(): pl.pallas_call(functools.partial(mixer_kernel, head), grid=(1,), in_specs...  13.1 us
    ppermute x9, starting transfers between devices, send(): lax.ppermute(x, 'tp', [(y, (y + chips * CORES) % tp) for y in range(tp)])  10.1 us
    pallas_call x4, Pallas kernels, collect(): pl.pallas_call(functools.partial(collect_kernel, peers, slots), grid=(1,)...  6.3 us
  transfers between devices with their start and end apart: 40, of which 11 were waited for; matrix products, arithmetic and copies ran while one was open for 0% of the time, Pallas kernels for 31%

profile of v1, /device:TPU:0, one launch (start us, length us, event | category | flops | bytes accessed | tf_op | source)
XLA Modules:
  0.0 209.7 jit_solution(12779208269170229266)
XLA Ops:
  1.7 3.2 %prepare.1 = (bf16[128,2176]{1,0:T(8,128)(2,1)}, bf16[64,2176]{1,0:T(8,128)(2,1)}, bf16[64,2176]{1,0:T(8,128)(2,1)}, bf16[64,2176]{1,0:T(8,128)(2,1)}, bf16[64,2176]{1,0:T(8,128)(2,1)}) custom-call(s32[1]{0:T(128)} %bitcast.4.me_ref, bf16[128,2048]{1,0:T(8,128)(2,1)} %x_ref.1, f32[1,2048]{1,0:T(1,128)} %bitcast.9, s32[2,128]{1,0:T(2,128)} %bitcast.10, ...), custom_call_target="tpu_custom_call" | custom-call | flops 134217728 | bytes 2097152 | tf_op jit(solution)/shard_map/prepare/pallas_call | solution.py:285
  4.9 2.6 %collective-permute-start.16 = (bf16[128,2176]{1,0:T(8,128)(2,1)}, bf16[128,2176]{1,0:T(8,128)(2,1)S(1)}, u32[]{:S(2)}, u32[]{:S(2)}) collective-permute-start(bf16[128,2176]{1,0:T(8,128)(2,1)} %get-tuple-element.71.meta_ref), channel_id=1, source_target_pairs={{0,2},{1,3},{2,4},{3,5},{4,6},{5,7},{6,0},{7,1},{8,10},{9,11},{10,... | collective-permute-start | bytes 1671176 | tf_op jit(solution)/shard_map/ppermute | solution.py:464
  7.5 15.5 %collective-permute-done.16.block_ref.meta_ref = bf16[128,2176]{1,0:T(8,128)(2,1)S(1)} collective-permute-done((bf16[128,2176]{1,0:T(8,128)(2,1)}, bf16[128,2176]{1,0:T(8,128)(2,1)S(1)}, u32[]{:S(2)}, u32[]{:S(2)}) %collective-permute-start.16) | collective-permute-done | bytes 557088 | tf_op jit(solution)/shard_map/ppermute | solution.py:464
  23.0 16.3 %collective-permute-done.24.block_ref.meta_ref = bf16[128,2176]{1,0:T(8,128)(2,1)} collective-permute-done((bf16[128,2176]{1,0:T(8,128)(2,1)S(1)}, bf16[128,2176]{1,0:T(8,128)(2,1)}, u32[]{:S(2)}, u32[]{:S(2)}) %collective-permute-start.24) | collective-permute-done | bytes 557088 | tf_op jit(solution)/shard_map/ppermute | solution.py:464
  39.3 6.5 %mixer_local.2 = (f32[512,128]{1,0:T(8,128)}, f32[512,128]{1,0:T(8,128)}, f32[1,128,256]{2,1,0:T(8,128)}) custom-call(f32[2]{0:T(128)} %rate_ref.3, bf16[512,256]{1,0:T(8,128)(2,1)} %q_ref.3, bf16[512,256]{1,0:T(8,128)(2,1)} %k_ref.3, bf16[512,256]{1,0:T(8,128)(2,1)} %v_ref.3, bf16[2,512]{1,0:T(2,128)(2,1)} %write_ref.3, bf16[2,512]{1,0:T(2,128)(2,1)} %decay_ref.3, ...), custom_call_target="tpu_custom_call" | custom-call | flops 2617245696 | bytes 917504 | tf_op jit(solution)/shard_map/mixer_local/pallas_call | solution.py:128
  45.7 1.4 dispatch.3
  47.9 6.9 %collective-permute-done.25.block_ref.meta_ref = bf16[128,2176]{1,0:T(8,128)(2,1)S(1)} collective-permute-done((bf16[128,2176]{1,0:T(8,128)(2,1)}, bf16[128,2176]{1,0:T(8,128)(2,1)S(1)}, u32[]{:S(2)}, u32[]{:S(2)}) %collective-permute-start.25) | collective-permute-done | bytes 557088 | tf_op jit(solution)/shard_map/ppermute | solution.py:464
  54.8 1.0 collective-permute-start.17
  55.8 1.6 collective-permute-start.18
  57.4 0.9 collective-permute-start.19
  58.3 6.6 %mixer_local.3 = (f32[512,128]{1,0:T(8,128)}, f32[512,128]{1,0:T(8,128)}, f32[2,128,256]{2,1,0:T(8,128)}) custom-call(f32[2]{0:T(128)} %rate_ref.3, bf16[512,256]{1,0:T(8,128)(2,1)} %q_ref.3, bf16[512,256]{1,0:T(8,128)(2,1)} %k_ref.3, bf16[512,256]{1,0:T(8,128)(2,1)} %v_ref.3, bf16[2,512]{1,0:T(2,128)(2,1)} %write_ref.3, bf16[2,512]{1,0:T(2,128)(2,1)} %decay_ref.3, ...), custom_call_target="tpu_custom_call" | custom-call | flops 2617245696 | bytes 917504 | tf_op jit(solution)/shard_map/mixer_local/pallas_call | solution.py:128
  65.0 2.5 %dispatch.5 = (bf16[64,2176]{1,0:T(8,128)(2,1)S(1)}, bf16[64,2176]{1,0:T(8,128)(2,1)}, bf16[64,2176]{1,0:T(8,128)(2,1)}, bf16[64,2176]{1,0:T(8,128)(2,1)}) custom-call(s32[1]{0:T(128)} %bitcast.4.me_ref, bf16[128,2176]{1,0:T(8,128)(2,1)} %collective-permute-done.24.block_ref.meta_ref), custom_call_target="tpu_custom_call" | custom-call | flops 142606336 | bytes 1671168 | tf_op jit(solution)/shard_map/dispatch/pallas_call | solution.py:316
  70.3 0.7 copy-done.32
  71.0 1.0 collective-permute-start.10
  72.0 1.0 collective-permute-start.32
  73.0 1.1 collective-permute-start.33
  74.1 1.4 collective-permute-start.34
  75.5 8.8 %expert_part.5 = (bf16[64,2048]{1,0:T(8,128)(2,1)}, bf16[64,2048]{1,0:T(8,128)(2,1)}, bf16[64,2048]{1,0:T(8,128)(2,1)}, bf16[64,2048]{1,0:T(8,128)(2,1)}) custom-call(s32[1]{0:T(128)} %bitcast.4.me_ref, bf16[64,2176]{1,0:T(8,128)(2,1)} %copy-done.13, bf16[64,2176]{1,0:T(8,128)(2,1)} %collective-permute-done.17.refs_1_, ...), custom_call_target="tpu_custom_call" | custom-call | flops 3221225472 | bytes 14680064 | tf_op jit(solution)/shard_map/expert_part/pallas_call | solution.py:391
  84.3 2.5 %collective-permute-done.32.refs_1_ = bf16[64,2176]{1,0:T(8,128)(2,1)} collective-permute-done((bf16[64,2176]{1,0:T(8,128)(2,1)}, bf16[64,2176]{1,0:T(8,128)(2,1)}, u32[]{:S(2)}, u32[]{:S(2)}) %collective-permute-start.32) | collective-permute-done | bytes 278560 | tf_op jit(solution)/shard_map/ppermute | solution.py:467
  86.8 1.1 collective-permute-start.11
  87.9 1.4 collective-permute-start.12
  89.3 4.0 %collective-permute-done.34.refs_3_ = bf16[64,2176]{1,0:T(8,128)(2,1)} collective-permute-done((bf16[64,2176]{1,0:T(8,128)(2,1)}, bf16[64,2176]{1,0:T(8,128)(2,1)}, u32[]{:S(2)}, u32[]{:S(2)}) %collective-permute-start.34) | collective-permute-done | bytes 278560 | tf_op jit(solution)/shard_map/ppermute | solution.py:467
  93.3 1.5 collective-permute-start.26
  94.8 1.6 copy-done
  96.4 1.6 copy-done.2
  98.0 1.6 copy-done.4
  99.6 1.6 copy-done.7
  101.2 1.0 copy-done.12
  102.2 8.1 %expert_part.7 = (bf16[64,2048]{1,0:T(8,128)(2,1)S(1)}, bf16[64,2048]{1,0:T(8,128)(2,1)S(1)}, bf16[64,2048]{1,0:T(8,128)(2,1)S(1)}, bf16[64,2048]{1,0:T(8,128)(2,1)S(1)}) custom-call(s32[1]{0:T(128)} %bitcast.4.me_ref, bf16[64,2176]{1,0:T(8,128)(2,1)S(1)} %copy-done.12, bf16[64,2176]{1,0:T(8,128)(2,1)} %collective-permute-done.32.refs_1_, ...), custom_call_target="tpu_custom_call" | custom-call | flops 3221225472 | bytes 14680064 | tf_op jit(solution)/shard_map/expert_part/pallas_call | solution.py:391
  110.9 1.5 collective-permute-start.28
  112.4 1.5 collective-permute-start.35
  114.4 8.0 %expert_part.4 = (bf16[64,2048]{1,0:T(8,128)(2,1)S(1)}, bf16[64,2048]{1,0:T(8,128)(2,1)}, bf16[64,2048]{1,0:T(8,128)(2,1)}, bf16[64,2048]{1,0:T(8,128)(2,1)S(1)}) custom-call(s32[1]{0:T(128)} %bitcast.4.me_ref, bf16[64,2176]{1,0:T(8,128)(2,1)S(1)} %copy-done.10, bf16[64,2176]{1,0:T(8,128)(2,1)} %collective-permute-done.10.refs_1_, ...), custom_call_target="tpu_custom_call" | custom-call | flops 3221225472 | bytes 14680064 | tf_op jit(solution)/shard_map/expert_part/pallas_call | solution.py:391
  122.4 1.1 collective-permute-start.20
  123.5 1.1 collective-permute-start.21
  124.6 1.4 collective-permute-start.22
  126.0 0.7 collective-permute-done.35.refs_1_
  126.7 0.8 collective-permute-start.37
  127.5 2.6 %collective-permute-done.36.refs_2_ = bf16[64,2048]{1,0:T(8,128)(2,1)S(1)} collective-permute-done((bf16[64,2048]{1,0:T(8,128)(2,1)S(1)}, bf16[64,2048]{1,0:T(8,128)(2,1)S(1)}, u32[]{:S(2)}, u32[]{:S(2)}) %collective-permute-start.36) | collective-permute-done | bytes 262176 | tf_op jit(solution)/shard_map/ppermute | solution.py:467
  130.1 7.0 %expert_part.6 = (bf16[64,2048]{1,0:T(8,128)(2,1)S(1)}, bf16[64,2048]{1,0:T(8,128)(2,1)}, bf16[64,2048]{1,0:T(8,128)(2,1)}, bf16[64,2048]{1,0:T(8,128)(2,1)}) custom-call(s32[1]{0:T(128)} %bitcast.4.me_ref, bf16[64,2176]{1,0:T(8,128)(2,1)S(1)} %get-tuple-element.94.refs_0_, bf16[64,2176]{1,0:T(8,128)(2,1)S(1)} %collective-permute-done.26.refs_1_, ...), custom_call_target="tpu_custom_call" | custom-call | flops 3221225472 | bytes 14680064 | tf_op jit(solution)/shard_map/expert_part/pallas_call | solution.py:391
  137.8 6.1 %collective-permute-done.37.refs_3_ = bf16[64,2048]{1,0:T(8,128)(2,1)S(1)} collective-permute-done((bf16[64,2048]{1,0:T(8,128)(2,1)S(1)}, bf16[64,2048]{1,0:T(8,128)(2,1)S(1)}, u32[]{:S(2)}, u32[]{:S(2)}) %collective-permute-start.37) | collective-permute-done | bytes 262176 | tf_op jit(solution)/shard_map/ppermute | solution.py:467
  144.4 2.0 collect.6
  147.1 1.0 collective-permute-start.14
  148.8 1.7 collective-permute-start.29
  151.9 0.9 collective-permute-start.4
  152.8 0.9 copy-done.20
  153.8 0.9 copy-done.22
  154.7 0.9 copy-done.25
  155.7 2.2 %collect.4 = bf16[128,2048]{1,0:T(8,128)(2,1)} custom-call(s32[1]{0:T(128)} %bitcast.4.me_ref, bf16[128,2176]{1,0:T(8,128)(2,1)S(1)} %collective-permute-done.16.block_ref.meta_ref, bf16[64,2048]{1,0:T(8,128)(2,1)S(1)} %copy-done.20, bf16[64,2048]{1,0:T(8,128)(2,1)S(1)} %copy-done.22, bf16[64,2048]{1,0:T(8,128)(2,1)S(1)} %copy-done.25, ...), custom_call_target="tpu_custom_call" | custom-call | flops 134217728 | bytes 2097152 | tf_op jit(solution)/shard_map/collect/pallas_call | solution.py:421
  157.9 3.8 %collective-permute-start.23 = (bf16[128,2048]{1,0:T(8,128)(2,1)}, bf16[128,2048]{1,0:T(8,128)(2,1)S(1)}, u32[]{:S(2)}, u32[]{:S(2)}) collective-permute-start(bf16[128,2048]{1,0:T(8,128)(2,1)} %collect.4), channel_id=1, source_target_pairs={{0,6},{1,7},{2,0},{3,1},{4,2},{5,3},{6,4},{7,5},{8,14},{9,15},{10,... | collective-permute-start | bytes 1572872 | tf_op jit(solution)/shard_map/ppermute | solution.py:464
  161.7 1.1 collective-permute-start.30
  162.9 0.8 collective-permute-start.31
  163.7 2.7 %attend.1 = (bf16[4,64,256]{2,1,0:T(8,128)(2,1)}, bf16[4,64,256]{2,1,0:T(8,128)(2,1)}) custom-call(s32[1]{0:T(128)} %bitcast.1.late_ref, s32[1]{0:T(128)} %bitcast.2.core_ref, f32[512,128]{1,0:T(8,128)} %get-tuple-element.56.refs_0_, f32[512,128]{1,0:T(8,128)} %get-tuple-element.58.refs_1_, f32[512,128]{1,0:T(8,128)} %get-tuple-element.59.refs_2_, ...), custom_call_target="tpu_custom_call" | custom-call | flops 201326592 | bytes 1310720 | tf_op jit(solution)/shard_map/attend/pallas_call | solution.py:190
  167.1 1.6 collective-permute-done.5.theirs_ref
  168.7 2.1 collective-permute-start.15
  170.8 0.9 copy-done.27
  171.7 2.3 %project.1 = (bf16[64,2048]{1,0:T(8,128)(2,1)S(1)}, bf16[64,2048]{1,0:T(8,128)(2,1)S(1)}, bf16[64,2048]{1,0:T(8,128)(2,1)S(1)}, bf16[64,2048]{1,0:T(8,128)(2,1)S(1)}) custom-call(s32[1]{0:T(128)} %bitcast.level_ref, bf16[4,64,256]{2,1,0:T(8,128)(2,1)S(1)} %copy-done.27, bf16[4,64,256]{2,1,0:T(8,128)(2,1)S(1)} %collective-permute-done.5.theirs_ref, ...), custom_call_target="tpu_custom_call" | custom-call | flops 536870912 | bytes 3145728 | tf_op jit(solution)/shard_map/project/pallas_call | solution.py:234
  174.2 2.0 collective-permute-start.9
  176.2 0.9 copy-done.15
  177.1 1.6 collect.7
  178.8 1.5 collective-permute-start.39
  180.8 2.3 %collective-permute-done.7 = bf16[64,2048]{1,0:T(8,128)(2,1)S(1)} collective-permute-done((bf16[64,2048]{1,0:T(8,128)(2,1)S(1)}, bf16[64,2048]{1,0:T(8,128)(2,1)S(1)}, u32[]{:S(2)}, u32[]{:S(2)}) %collective-permute-start.7) | collective-permute-done | bytes 262176 | tf_op jit(solution)/shard_map/ppermute | solution.py:464
  183.1 24.8 %collective-permute-done.8 = bf16[64,2048]{1,0:T(8,128)(2,1)S(1)} collective-permute-done((bf16[64,2048]{1,0:T(8,128)(2,1)S(1)}, bf16[64,2048]{1,0:T(8,128)(2,1)S(1)}, u32[]{:S(2)}, u32[]{:S(2)}) %collective-permute-start.8) | collective-permute-done | bytes 262176 | tf_op jit(solution)/shard_map/ppermute | solution.py:464
  207.9 0.8 add_convert_fusion.1
  208.7 0.9 add_convert_fusion
  (113 shorter events, 11.0 us)
Async XLA Ops:
  0.6 55.2 %collective-permute-start = (bf16[4,128,2048]{2,1,0:T(8,128)(2,1)}, bf16[4,128,2048]{2,1,0:T(8,128)(2,1)S(1)}, u32[]{:S(2)}, u32[]{:S(2)}) collective-permute-start(bf16[4,128,2048]{2,1,0:T(8,128)(2,1)} %refs_4_.3), channel_id=1, source_target_pairs={{0,1},{1,0},{2,3},{3,2},{4,5},{5,4},{6,7},{7,6},{8,9},{9,8},{10,11... | collective-permute-start | bytes 6291464 | tf_op jit(solution)/shard_map/ppermute | solution.py:461
  1.2 56.2 %collective-permute-start.1 = (bf16[4,128,2048]{2,1,0:T(8,128)(2,1)}, bf16[4,128,2048]{2,1,0:T(8,128)(2,1)}, u32[]{:S(2)}, u32[]{:S(2)}) collective-permute-start(bf16[4,128,2048]{2,1,0:T(8,128)(2,1)} %refs_6_.3), channel_id=1, source_target_pairs={{0,1},{1,0},{2,3},{3,2},{4,5},{5,4},{6,7},{7,6},{8,9},{9,8},{10,11... | collective-permute-start | bytes 6291464 | tf_op jit(solution)/shard_map/ppermute | solution.py:461
  1.3 69.7 %collective-permute-start.2 = (bf16[4,128,2048]{2,1,0:T(8,128)(2,1)}, bf16[4,128,2048]{2,1,0:T(8,128)(2,1)}, u32[]{:S(2)}, u32[]{:S(2)}) collective-permute-start(bf16[4,128,2048]{2,1,0:T(8,128)(2,1)} %refs_8_.3), channel_id=1, source_target_pairs={{0,1},{1,0},{2,3},{3,2},{4,5},{5,4},{6,7},{7,6},{8,9},{9,8},{10,11... | collective-permute-start | bytes 6291464 | tf_op jit(solution)/shard_map/ppermute | solution.py:461
  4.9 18.1 %collective-permute-start.16 = (bf16[128,2176]{1,0:T(8,128)(2,1)}, bf16[128,2176]{1,0:T(8,128)(2,1)S(1)}, u32[]{:S(2)}, u32[]{:S(2)}) collective-permute-start(bf16[128,2176]{1,0:T(8,128)(2,1)} %get-tuple-element.71.meta_ref), channel_id=1, source_target_pairs={{0,2},{1,3},{2,4},{3,5},{4,6},{5,7},{6,0},{7,1},{8,10},{9,11},{10,... | collective-permute-start | bytes 1671176 | tf_op jit(solution)/shard_map/ppermute | solution.py:464
  23.0 16.3 %collective-permute-start.24 = (bf16[128,2176]{1,0:T(8,128)(2,1)S(1)}, bf16[128,2176]{1,0:T(8,128)(2,1)}, u32[]{:S(2)}, u32[]{:S(2)}) collective-permute-start(bf16[128,2176]{1,0:T(8,128)(2,1)S(1)} %collective-permute-done.16.block_ref.meta_ref), channel_id=1, source_target_pairs={{0,2},{1,3},{2,4},{3,5},{4,6},{5,7},{6,0},{7,1},{8,10},{9,11},{10,... | collective-permute-start | bytes 1671176 | tf_op jit(solution)/shard_map/ppermute | solution.py:464
  39.3 15.5 %collective-permute-start.25 = (bf16[128,2176]{1,0:T(8,128)(2,1)}, bf16[128,2176]{1,0:T(8,128)(2,1)S(1)}, u32[]{:S(2)}, u32[]{:S(2)}) collective-permute-start(bf16[128,2176]{1,0:T(8,128)(2,1)} %collective-permute-done.24.block_ref.meta_ref), channel_id=1, source_target_pairs={{0,2},{1,3},{2,4},{3,5},{4,6},{5,7},{6,0},{7,1},{8,10},{9,11},{10,... | collective-permute-start | bytes 1671176 | tf_op jit(solution)/shard_map/ppermute | solution.py:464
  39.3 74.6 %collective-permute-start.6 = (bf16[256,2048]{1,0:T(8,128)(2,1)}, bf16[256,2048]{1,0:T(8,128)(2,1)}, u32[]{:S(2)}, u32[]{:S(2)}) collective-permute-start(bf16[256,2048]{1,0:T(8,128)(2,1)} %own_ref.1), channel_id=1, source_target_pairs={{0,1},{1,0},{2,3},{3,2},{4,5},{5,4},{6,7},{7,6},{8,9},{9,8},{10,11... | collective-permute-start | bytes 3145736 | tf_op jit(solution)/shard_map/ppermute | solution.py:461
  54.8 17.2 %collective-permute-start.17 = (bf16[64,2176]{1,0:T(8,128)(2,1)}, bf16[64,2176]{1,0:T(8,128)(2,1)}, u32[]{:S(2)}, u32[]{:S(2)}) collective-permute-start(bf16[64,2176]{1,0:T(8,128)(2,1)} %get-tuple-element.87), channel_id=1, source_target_pairs={{0,8},{8,0},{16,24},{24,16},{1,9},{9,1},{17,25},{25,17},{2,10},{10... | collective-permute-start | bytes 835592 | tf_op jit(solution)/shard_map/ppermute | solution.py:467
  55.8 9.1 %copy-start.6 = (bf16[4,128,2048]{2,1,0:T(8,128)(2,1)}, bf16[4,128,2048]{2,1,0:T(8,128)(2,1)S(1)}, u32[]{:S(2)}) copy-start(bf16[4,128,2048]{2,1,0:T(8,128)(2,1)S(1)} %collective-permute-done.refs_5_) | copy-start | bytes 6291460
  55.8 17.2 %collective-permute-start.18 = (bf16[64,2176]{1,0:T(8,128)(2,1)}, bf16[64,2176]{1,0:T(8,128)(2,1)}, u32[]{:S(2)}, u32[]{:S(2)}) collective-permute-start(bf16[64,2176]{1,0:T(8,128)(2,1)} %get-tuple-element.88), channel_id=1, source_target_pairs={{0,16},{8,24},{16,0},{24,8},{1,17},{9,25},{17,1},{25,9},{2,18},{10... | collective-permute-start | bytes 835592 | tf_op jit(solution)/shard_map/ppermute | solution.py:467
  57.4 16.7 %collective-permute-start.19 = (bf16[64,2176]{1,0:T(8,128)(2,1)}, bf16[64,2176]{1,0:T(8,128)(2,1)}, u32[]{:S(2)}, u32[]{:S(2)}) collective-permute-start(bf16[64,2176]{1,0:T(8,128)(2,1)} %get-tuple-element.89), channel_id=1, source_target_pairs={{0,24},{8,16},{16,8},{24,0},{1,25},{9,17},{17,9},{25,1},{2,26},{10... | collective-permute-start | bytes 835592 | tf_op jit(solution)/shard_map/ppermute | solution.py:467
  71.0 39.3 %collective-permute-start.10 = (bf16[64,2176]{1,0:T(8,128)(2,1)}, bf16[64,2176]{1,0:T(8,128)(2,1)}, u32[]{:S(2)}, u32[]{:S(2)}) collective-permute-start(bf16[64,2176]{1,0:T(8,128)(2,1)} %get-tuple-element.73), channel_id=1, source_target_pairs={{0,8},{8,0},{16,24},{24,16},{1,9},{9,1},{17,25},{25,17},{2,10},{10... | collective-permute-start | bytes 835592 | tf_op jit(solution)/shard_map/ppermute | solution.py:467
  72.0 14.8 %collective-permute-start.32 = (bf16[64,2176]{1,0:T(8,128)(2,1)}, bf16[64,2176]{1,0:T(8,128)(2,1)}, u32[]{:S(2)}, u32[]{:S(2)}) collective-permute-start(bf16[64,2176]{1,0:T(8,128)(2,1)} %get-tuple-element.103), channel_id=1, source_target_pairs={{0,8},{8,0},{16,24},{24,16},{1,9},{9,1},{17,25},{25,17},{2,10},{10... | collective-permute-start | bytes 835592 | tf_op jit(solution)/shard_map/ppermute | solution.py:467
  73.0 14.8 %collective-permute-start.33 = (bf16[64,2176]{1,0:T(8,128)(2,1)}, bf16[64,2176]{1,0:T(8,128)(2,1)}, u32[]{:S(2)}, u32[]{:S(2)}) collective-permute-start(bf16[64,2176]{1,0:T(8,128)(2,1)} %get-tuple-element.104), channel_id=1, source_target_pairs={{0,16},{8,24},{16,0},{24,8},{1,17},{9,25},{17,1},{25,9},{2,18},{10... | collective-permute-start | bytes 835592 | tf_op jit(solution)/shard_map/ppermute | solution.py:467
  74.1 19.2 %collective-permute-start.34 = (bf16[64,2176]{1,0:T(8,128)(2,1)}, bf16[64,2176]{1,0:T(8,128)(2,1)}, u32[]{:S(2)}, u32[]{:S(2)}) collective-permute-start(bf16[64,2176]{1,0:T(8,128)(2,1)} %get-tuple-element.105), channel_id=1, source_target_pairs={{0,24},{8,16},{16,8},{24,0},{1,25},{9,17},{17,9},{25,1},{2,26},{10... | collective-permute-start | bytes 835592 | tf_op jit(solution)/shard_map/ppermute | solution.py:467
  86.8 24.1 %collective-permute-start.11 = (bf16[64,2176]{1,0:T(8,128)(2,1)}, bf16[64,2176]{1,0:T(8,128)(2,1)S(1)}, u32[]{:S(2)}, u32[]{:S(2)}) collective-permute-start(bf16[64,2176]{1,0:T(8,128)(2,1)} %get-tuple-element.74), channel_id=1, source_target_pairs={{0,16},{8,24},{16,0},{24,8},{1,17},{9,25},{17,1},{25,9},{2,18},{10... | collective-permute-start | bytes 835592 | tf_op jit(solution)/shard_map/ppermute | solution.py:467
  87.9 24.5 %collective-permute-start.12 = (bf16[64,2176]{1,0:T(8,128)(2,1)}, bf16[64,2176]{1,0:T(8,128)(2,1)S(1)}, u32[]{:S(2)}, u32[]{:S(2)}) collective-permute-start(bf16[64,2176]{1,0:T(8,128)(2,1)} %get-tuple-element.75), channel_id=1, source_target_pairs={{0,24},{8,16},{16,8},{24,0},{1,25},{9,17},{17,9},{25,1},{2,26},{10... | collective-permute-start | bytes 835592 | tf_op jit(solution)/shard_map/ppermute | solution.py:467
  93.3 29.1 %collective-permute-start.26 = (bf16[64,2176]{1,0:T(8,128)(2,1)}, bf16[64,2176]{1,0:T(8,128)(2,1)S(1)}, u32[]{:S(2)}, u32[]{:S(2)}) collective-permute-start(bf16[64,2176]{1,0:T(8,128)(2,1)} %copy-done.32), channel_id=1, source_target_pairs={{0,8},{8,0},{16,24},{24,16},{1,9},{9,1},{17,25},{25,17},{2,10},{10... | collective-permute-start | bytes 835592 | tf_op jit(solution)/shard_map/ppermute | solution.py:467
  94.8 1.6 copy-start
  96.4 1.6 copy-start.2
  98.0 1.6 copy-start.4
  99.6 1.6 copy-start.7
  101.2 1.0 copy-start.12
  102.2 8.2 %copy-start.31 = (bf16[64,2176]{1,0:T(8,128)(2,1)S(1)}, bf16[64,2176]{1,0:T(8,128)(2,1)}, u32[]{:S(2)}) copy-start(bf16[64,2176]{1,0:T(8,128)(2,1)} %copy-done.30) | copy-start | bytes 835588
  102.2 8.7 %copy-start.29 = (bf16[64,2176]{1,0:T(8,128)(2,1)S(1)}, bf16[64,2176]{1,0:T(8,128)(2,1)}, u32[]{:S(2)}) copy-start(bf16[64,2176]{1,0:T(8,128)(2,1)} %copy-done.28) | copy-start | bytes 835588
  102.2 12.2 %copy-start.1 = (bf16[4,128,2048]{2,1,0:T(8,128)(2,1)S(1)}, bf16[4,128,2048]{2,1,0:T(8,128)(2,1)}, u32[]{:S(2)}) copy-start(bf16[4,128,2048]{2,1,0:T(8,128)(2,1)} %refs_4_.3) | copy-start | bytes 6291460
  102.2 12.2 %copy-start.3 = (bf16[4,128,2048]{2,1,0:T(8,128)(2,1)S(1)}, bf16[4,128,2048]{2,1,0:T(8,128)(2,1)}, u32[]{:S(2)}) copy-start(bf16[4,128,2048]{2,1,0:T(8,128)(2,1)} %refs_6_.3) | copy-start | bytes 6291460
  102.2 12.2 %copy-start.5 = (bf16[4,128,2048]{2,1,0:T(8,128)(2,1)S(1)}, bf16[4,128,2048]{2,1,0:T(8,128)(2,1)}, u32[]{:S(2)}) copy-start(bf16[4,128,2048]{2,1,0:T(8,128)(2,1)} %refs_8_.3) | copy-start | bytes 6291460
  102.2 12.2 %copy-start.10 = (bf16[64,2176]{1,0:T(8,128)(2,1)S(1)}, bf16[64,2176]{1,0:T(8,128)(2,1)}, u32[]{:S(2)}) copy-start(bf16[64,2176]{1,0:T(8,128)(2,1)} %get-tuple-element.72.refs_0_) | copy-start | bytes 835588
  110.3 13.2 %collective-permute-start.27 = (bf16[64,2176]{1,0:T(8,128)(2,1)S(1)}, bf16[64,2176]{1,0:T(8,128)(2,1)S(1)}, u32[]{:S(2)}, u32[]{:S(2)}) collective-permute-start(bf16[64,2176]{1,0:T(8,128)(2,1)S(1)} %copy-done.31), channel_id=1, source_target_pairs={{0,16},{8,24},{16,0},{24,8},{1,17},{9,25},{17,1},{25,9},{2,18},{10... | collective-permute-start | bytes 835592 | tf_op jit(solution)/shard_map/ppermute | solution.py:467
  110.9 13.7 %collective-permute-start.28 = (bf16[64,2176]{1,0:T(8,128)(2,1)S(1)}, bf16[64,2176]{1,0:T(8,128)(2,1)S(1)}, u32[]{:S(2)}, u32[]{:S(2)}) collective-permute-start(bf16[64,2176]{1,0:T(8,128)(2,1)S(1)} %copy-done.29), channel_id=1, source_target_pairs={{0,24},{8,16},{16,8},{24,0},{1,25},{9,17},{17,9},{25,1},{2,26},{10... | collective-permute-start | bytes 835592 | tf_op jit(solution)/shard_map/ppermute | solution.py:467
  112.4 14.4 %collective-permute-start.35 = (bf16[64,2048]{1,0:T(8,128)(2,1)S(1)}, bf16[64,2048]{1,0:T(8,128)(2,1)S(1)}, u32[]{:S(2)}, u32[]{:S(2)}) collective-permute-start(bf16[64,2048]{1,0:T(8,128)(2,1)S(1)} %get-tuple-element.107), channel_id=1, source_target_pairs={{0,8},{8,0},{16,24},{24,16},{1,9},{9,1},{17,25},{25,17},{2,10},{10... | collective-permute-start | bytes 786440 | tf_op jit(solution)/shard_map/ppermute | solution.py:467
  113.9 16.2 %collective-permute-start.36 = (bf16[64,2048]{1,0:T(8,128)(2,1)S(1)}, bf16[64,2048]{1,0:T(8,128)(2,1)S(1)}, u32[]{:S(2)}, u32[]{:S(2)}) collective-permute-start(bf16[64,2048]{1,0:T(8,128)(2,1)S(1)} %get-tuple-element.108), channel_id=1, source_target_pairs={{0,16},{8,24},{16,0},{24,8},{1,17},{9,25},{17,1},{25,9},{2,18},{10... | collective-permute-start | bytes 786440 | tf_op jit(solution)/shard_map/ppermute | solution.py:467
  114.4 8.0 %copy-start.36 = (bf16[64,2048]{1,0:T(8,128)(2,1)S(1)}, bf16[64,2048]{1,0:T(8,128)(2,1)}, u32[]{:S(2)}) copy-start(bf16[64,2048]{1,0:T(8,128)(2,1)} %get-tuple-element.91) | copy-start | bytes 786436
  114.4 9.1 %copy-start.35 = (bf16[64,2048]{1,0:T(8,128)(2,1)S(1)}, bf16[64,2048]{1,0:T(8,128)(2,1)}, u32[]{:S(2)}) copy-start(bf16[64,2048]{1,0:T(8,128)(2,1)} %get-tuple-element.92) | copy-start | bytes 786436
  114.4 15.7 %copy-start.26 = (f32[2,128,256]{2,1,0:T(8,128)S(1)}, f32[2,128,256]{2,1,0:T(8,128)}, u32[]{:S(2)}) copy-start(f32[2,128,256]{2,1,0:T(8,128)} %get-tuple-element.62.own_ref) | copy-start | bytes 786436
  122.4 7.7 %copy-start.33 = (bf16[64,2048]{1,0:T(8,128)(2,1)}, bf16[64,2048]{1,0:T(8,128)(2,1)S(1)}, u32[]{:S(2)}) copy-start(bf16[64,2048]{1,0:T(8,128)(2,1)S(1)} %get-tuple-element.85) | copy-start | bytes 786436
  122.4 24.0 %collective-permute-start.20 = (bf16[64,2048]{1,0:T(8,128)(2,1)S(1)}, bf16[64,2048]{1,0:T(8,128)(2,1)S(1)}, u32[]{:S(2)}, u32[]{:S(2)}) collective-permute-start(bf16[64,2048]{1,0:T(8,128)(2,1)S(1)} %copy-done.36), channel_id=1, source_target_pairs={{0,8},{8,0},{16,24},{24,16},{1,9},{9,1},{17,25},{25,17},{2,10},{10... | collective-permute-start | bytes 786440 | tf_op jit(solution)/shard_map/ppermute | solution.py:467
  123.5 24.6 %collective-permute-start.21 = (bf16[64,2048]{1,0:T(8,128)(2,1)S(1)}, bf16[64,2048]{1,0:T(8,128)(2,1)S(1)}, u32[]{:S(2)}, u32[]{:S(2)}) collective-permute-start(bf16[64,2048]{1,0:T(8,128)(2,1)S(1)} %copy-done.35), channel_id=1, source_target_pairs={{0,16},{8,24},{16,0},{24,8},{1,17},{9,25},{17,1},{25,9},{2,18},{10... | collective-permute-start | bytes 786440 | tf_op jit(solution)/shard_map/ppermute | solution.py:467
  124.6 27.3 %collective-permute-start.22 = (bf16[64,2048]{1,0:T(8,128)(2,1)}, bf16[64,2048]{1,0:T(8,128)(2,1)}, u32[]{:S(2)}, u32[]{:S(2)}) collective-permute-start(bf16[64,2048]{1,0:T(8,128)(2,1)} %get-tuple-element.93), channel_id=1, source_target_pairs={{0,24},{8,16},{16,8},{24,0},{1,25},{9,17},{17,9},{25,1},{2,26},{10... | collective-permute-start | bytes 786440 | tf_op jit(solution)/shard_map/ppermute | solution.py:467
  126.7 17.2 %collective-permute-start.37 = (bf16[64,2048]{1,0:T(8,128)(2,1)S(1)}, bf16[64,2048]{1,0:T(8,128)(2,1)S(1)}, u32[]{:S(2)}, u32[]{:S(2)}) collective-permute-start(bf16[64,2048]{1,0:T(8,128)(2,1)S(1)} %get-tuple-element.109), channel_id=1, source_target_pairs={{0,24},{8,16},{16,8},{24,0},{1,25},{9,17},{17,9},{25,1},{2,26},{10... | collective-permute-start | bytes 786440 | tf_op jit(solution)/shard_map/ppermute | solution.py:467
  130.1 20.4 %collective-permute-start.3 = (f32[2,128,256]{2,1,0:T(8,128)S(1)}, f32[2,128,256]{2,1,0:T(8,128)S(1)}, u32[]{:S(2)}, u32[]{:S(2)}) collective-permute-start(f32[2,128,256]{2,1,0:T(8,128)S(1)} %copy-done.26), channel_id=1, source_target_pairs={{0,8},{8,0},{16,24},{24,16},{1,9},{9,1},{17,25},{25,17},{2,10},{10... | collective-permute-start | bytes 786440 | tf_op jit(solution)/shard_map/ppermute | solution.py:467
  143.9 14.0 %collective-permute-start.13 = (bf16[64,2048]{1,0:T(8,128)(2,1)}, bf16[64,2048]{1,0:T(8,128)(2,1)S(1)}, u32[]{:S(2)}, u32[]{:S(2)}) collective-permute-start(bf16[64,2048]{1,0:T(8,128)(2,1)} %get-tuple-element.83), channel_id=1, source_target_pairs={{0,8},{8,0},{16,24},{24,16},{1,9},{9,1},{17,25},{25,17},{2,10},{10... | collective-permute-start | bytes 786440 | tf_op jit(solution)/shard_map/ppermute | solution.py:467
  147.1 14.6 %collective-permute-start.14 = (bf16[64,2048]{1,0:T(8,128)(2,1)}, bf16[64,2048]{1,0:T(8,128)(2,1)S(1)}, u32[]{:S(2)}, u32[]{:S(2)}) collective-permute-start(bf16[64,2048]{1,0:T(8,128)(2,1)} %get-tuple-element.84), channel_id=1, source_target_pairs={{0,16},{8,24},{16,0},{24,8},{1,17},{9,25},{17,1},{25,9},{2,18},{10... | collective-permute-start | bytes 786440 | tf_op jit(solution)/shard_map/ppermute | solution.py:467
  148.8 17.6 %collective-permute-start.29 = (bf16[64,2048]{1,0:T(8,128)(2,1)}, bf16[64,2048]{1,0:T(8,128)(2,1)S(1)}, u32[]{:S(2)}, u32[]{:S(2)}) collective-permute-start(bf16[64,2048]{1,0:T(8,128)(2,1)} %get-tuple-element.99), channel_id=1, source_target_pairs={{0,8},{8,0},{16,24},{24,16},{1,9},{9,1},{17,25},{25,17},{2,10},{10... | collective-permute-start | bytes 786440 | tf_op jit(solution)/shard_map/ppermute | solution.py:467
  150.5 23.7 %collective-permute-start.38 = (bf16[128,2048]{1,0:T(8,128)(2,1)}, bf16[128,2048]{1,0:T(8,128)(2,1)}, u32[]{:S(2)}, u32[]{:S(2)}) collective-permute-start(bf16[128,2048]{1,0:T(8,128)(2,1)} %collect.6), channel_id=1, source_target_pairs={{0,2},{1,3},{2,4},{3,5},{4,6},{5,7},{6,0},{7,1},{8,10},{9,11},{10,... | collective-permute-start | bytes 1572872 | tf_op jit(solution)/shard_map/ppermute | solution.py:464
  151.9 18.9 %copy-start.8 = (bf16[256,2048]{1,0:T(8,128)(2,1)S(1)}, bf16[256,2048]{1,0:T(8,128)(2,1)}, u32[]{:S(2)}) copy-start(bf16[256,2048]{1,0:T(8,128)(2,1)} %own_ref.1) | copy-start | bytes 3145732
  151.9 11.0 %collective-permute-start.4 = (f32[2,128,128]{2,1,0:T(8,128)S(1)}, f32[2,128,128]{2,1,0:T(8,128)S(1)}, u32[]{:S(2)}, u32[]{:S(2)}) collective-permute-start(f32[2,128,128]{2,1,0:T(8,128)S(1)} %slice.3), channel_id=1, source_target_pairs={{0,16},{8,24},{16,0},{24,8},{1,17},{9,25},{17,1},{25,9},{2,18},{10... | collective-permute-start | bytes 393224 | tf_op jit(solution)/shard_map/ppermute | solution.py:467
  152.8 0.9 copy-start.20
  153.8 0.9 copy-start.22
  157.9 22.4 %collective-permute-start.23 = (bf16[128,2048]{1,0:T(8,128)(2,1)}, bf16[128,2048]{1,0:T(8,128)(2,1)S(1)}, u32[]{:S(2)}, u32[]{:S(2)}) collective-permute-start(bf16[128,2048]{1,0:T(8,128)(2,1)} %collect.4), channel_id=1, source_target_pairs={{0,6},{1,7},{2,0},{3,1},{4,2},{5,3},{6,4},{7,5},{8,14},{9,15},{10,... | collective-permute-start | bytes 1572872 | tf_op jit(solution)/shard_map/ppermute | solution.py:464
  161.7 9.0 %copy-start.16 = (bf16[64,2048]{1,0:T(8,128)(2,1)}, bf16[64,2048]{1,0:T(8,128)(2,1)S(1)}, u32[]{:S(2)}) copy-start(bf16[64,2048]{1,0:T(8,128)(2,1)S(1)} %collective-permute-done.14.refs_2_) | copy-start | bytes 786436
  161.7 12.3 %collective-permute-start.30 = (bf16[64,2048]{1,0:T(8,128)(2,1)}, bf16[64,2048]{1,0:T(8,128)(2,1)}, u32[]{:S(2)}, u32[]{:S(2)}) collective-permute-start(bf16[64,2048]{1,0:T(8,128)(2,1)} %get-tuple-element.100), channel_id=1, source_target_pairs={{0,16},{8,24},{16,0},{24,8},{1,17},{9,25},{17,1},{25,9},{2,18},{10... | collective-permute-start | bytes 786440 | tf_op jit(solution)/shard_map/ppermute | solution.py:467
  162.9 11.3 %collective-permute-start.31 = (bf16[64,2048]{1,0:T(8,128)(2,1)}, bf16[64,2048]{1,0:T(8,128)(2,1)}, u32[]{:S(2)}, u32[]{:S(2)}) collective-permute-start(bf16[64,2048]{1,0:T(8,128)(2,1)} %get-tuple-element.101), channel_id=1, source_target_pairs={{0,24},{8,16},{16,8},{24,0},{1,25},{9,17},{17,9},{25,1},{2,26},{10... | collective-permute-start | bytes 786440 | tf_op jit(solution)/shard_map/ppermute | solution.py:467
  167.1 1.6 collective-permute-start.5
  167.1 9.1 %copy-start.19 = (bf16[64,2048]{1,0:T(8,128)(2,1)S(1)}, bf16[64,2048]{1,0:T(8,128)(2,1)}, u32[]{:S(2)}) copy-start(bf16[64,2048]{1,0:T(8,128)(2,1)} %copy-done.18) | copy-start | bytes 786436
  168.7 10.1 %collective-permute-start.15 = (bf16[64,2048]{1,0:T(8,128)(2,1)}, bf16[64,2048]{1,0:T(8,128)(2,1)S(1)}, u32[]{:S(2)}, u32[]{:S(2)}) collective-permute-start(bf16[64,2048]{1,0:T(8,128)(2,1)} %copy-done.33), channel_id=1, source_target_pairs={{0,24},{8,16},{16,8},{24,0},{1,25},{9,17},{17,9},{25,1},{2,26},{10... | collective-permute-start | bytes 786440 | tf_op jit(solution)/shard_map/ppermute | solution.py:467
  171.7 8.7 %copy-start.9 = (bf16[128,2176]{1,0:T(8,128)(2,1)S(1)}, bf16[128,2176]{1,0:T(8,128)(2,1)}, u32[]{:S(2)}) copy-start(bf16[128,2176]{1,0:T(8,128)(2,1)} %get-tuple-element.71.meta_ref) | copy-start | bytes 1671172
  171.7 8.7 %copy-start.17 = (bf16[64,2048]{1,0:T(8,128)(2,1)S(1)}, bf16[64,2048]{1,0:T(8,128)(2,1)}, u32[]{:S(2)}) copy-start(bf16[64,2048]{1,0:T(8,128)(2,1)} %copy-done.16) | copy-start | bytes 786436
  174.0 9.1 %collective-permute-start.7 = (bf16[64,2048]{1,0:T(8,128)(2,1)S(1)}, bf16[64,2048]{1,0:T(8,128)(2,1)S(1)}, u32[]{:S(2)}, u32[]{:S(2)}) collective-permute-start(bf16[64,2048]{1,0:T(8,128)(2,1)S(1)} %get-tuple-element.68), channel_id=1, source_target_pairs={{0,6},{1,7},{2,0},{3,1},{4,2},{5,3},{6,4},{7,5},{8,14},{9,15},{10,... | collective-permute-start | bytes 786440 | tf_op jit(solution)/shard_map/ppermute | solution.py:464
  174.2 33.7 %collective-permute-start.8 = (bf16[64,2048]{1,0:T(8,128)(2,1)S(1)}, bf16[64,2048]{1,0:T(8,128)(2,1)S(1)}, u32[]{:S(2)}, u32[]{:S(2)}) collective-permute-start(bf16[64,2048]{1,0:T(8,128)(2,1)S(1)} %get-tuple-element.69), channel_id=1, source_target_pairs={{0,4},{1,5},{2,6},{3,7},{4,0},{5,1},{6,2},{7,3},{8,12},{9,13},{10,... | collective-permute-start | bytes 786440 | tf_op jit(solution)/shard_map/ppermute | solution.py:464
  174.2 33.7 %collective-permute-start.9 = (bf16[64,2048]{1,0:T(8,128)(2,1)S(1)}, bf16[64,2048]{1,0:T(8,128)(2,1)S(1)}, u32[]{:S(2)}, u32[]{:S(2)}) collective-permute-start(bf16[64,2048]{1,0:T(8,128)(2,1)S(1)} %get-tuple-element.70), channel_id=1, source_target_pairs={{0,2},{1,3},{2,4},{3,5},{4,6},{5,7},{6,0},{7,1},{8,10},{9,11},{10,... | collective-permute-start | bytes 786440 | tf_op jit(solution)/shard_map/ppermute | solution.py:464
  176.2 1.0 copy-start.15
  178.8 29.9 %collective-permute-start.39 = (bf16[128,2048]{1,0:T(8,128)(2,1)S(1)}, bf16[128,2048]{1,0:T(8,128)(2,1)S(1)}, u32[]{:S(2)}, u32[]{:S(2)}) collective-permute-start(bf16[128,2048]{1,0:T(8,128)(2,1)S(1)} %collect.7), channel_id=1, source_target_pairs={{0,2},{1,3},{2,4},{3,5},{4,6},{5,7},{6,0},{7,1},{8,10},{9,11},{10,... | collective-permute-start | bytes 1572872 | tf_op jit(solution)/shard_map/ppermute | solution.py:464
  (13 other events, 9.8 us)

commit v2 on v1

--- a/solution.py
+++ b/solution.py
@@ -113,7 +113,7 @@
         out = mm3(q[n] * grown[n], joint) + mm3(scores[n], update)
         joint = joint * jnp.exp(last[n]) + mm3(kt[n] * jnp.exp(last[n] - row[n]), update)
         local_ref[spans[n], :] = out[:, :DV]
-        proj_ref[spans[n], :] = out[:, DV:]
+        proj_ref[spans[n], :] = out[:, DV:].astype(BF16)
     for number, early_ref in enumerate(early_refs):
         joint_ref[number] = early_ref[0]
     joint_ref[len(early_refs)] = joint
@@ -132,7 +132,7 @@
         out_specs=[flat, flat, ends(1 + len(early))],
         out_shape=[
             jax.ShapeDtypeStruct((length, DV), F32),
-            jax.ShapeDtypeStruct((length, DK), F32),
+            jax.ShapeDtypeStruct((length, DK), BF16),
             jax.ShapeDtypeStruct((1 + len(early), DK, DV + DK), F32),
         ],
         cost_estimate=cost(length // CHUNK * 26 * 6 * 2 * 128**3, length * DK * 14),
@@ -172,13 +172,14 @@
     for h in range(heads):
         inner = inner_ref[h]
         state = mm3(inner[:, DV:], got_ref[h]) + inner[:, :DV]
-        states.append(jnp.where(late, state, inner[:, :DV]))
+        states.append(jnp.concatenate(halves(jnp.where(late, state, inner[:, :DV])), axis=1))
     depth, rows = mine_ref.shape[0], mine_ref.shape[1]
     for out_ref, shift in ((mine_ref, core_ref[0]), (other_ref, 1 - core_ref[0])):
         for z in range(depth):
             span = pl.ds(pl.multiple_of((z * CORES + shift) * rows, rows), rows)
             for h in range(heads):
-                out = local_refs[h][span, :] + mm3(proj_refs[h][span, :], states[h])
+                both = jnp.dot(proj_refs[h][span, :], states[h], preferred_element_type=F32)
+                out = local_refs[h][span, :] + both[:, :DV] + both[:, DV:]
                 out_ref[z, :, h * DV : (h + 1) * DV] = out.astype(BF16)
 
 

time: 210 us -> 213 us (1.014)
  local copies, waits for them, and re-layouts: 19.2 us -> 21.7 us
    unnamed x74 -> x76, local copies, waits for them, and re-layouts: 19.1 us -> 21.7 us
  transfers between devices with their start and end apart: 40 -> 40, of which waited for: 11 -> 11; matrix products, arithmetic and copies ran while one was open for 0% -> 0% of each run, Pallas kernels for 31% -> 30%
where the time goes in v2:
time: 213 us; the launch traced here: 212 us
  waiting for transfers between devices  83.2 us (39%)
  Pallas kernels  64.4 us (30%)
  starting transfers between devices  39.7 us (19%)
  local copies, waits for them, and re-layouts  21.7 us (10%)
    ppermute x9, waiting for transfers between devices, send(): lax.ppermute(x, 'tp', [(y, (y + chips * CORES) % tp) for y in range(tp)])  65.7 us
    pallas_call x4, Pallas kernels, expert_part(): pl.pallas_call(functools.partial(expert_kernel, moved, peers, slots), in_...  32 us
    ppermute x26, starting transfers between devices, trade(): return lax.ppermute(x, 'ep', [(y, y ^ distance) for y in range(ep)])  28.5 us
    unnamed x76, local copies, waits for them, and re-layouts  21.7 us
    ppermute x26, waiting for transfers between devices, trade(): return lax.ppermute(x, 'ep', [(y, y ^ distance) for y in range(ep)])  16 us
    pallas_call x2, Pallas kernels, mixer_local(): pl.pallas_call(functools.partial(mixer_kernel, head), grid=(1,), in_specs...  13 us
    ppermute x9, starting transfers between devices, send(): lax.ppermute(x, 'tp', [(y, (y + chips * CORES) % tp) for y in range(tp)])  10.1 us
    pallas_call x4, Pallas kernels, collect(): pl.pallas_call(functools.partial(collect_kernel, peers, slots), grid=(1,)...  6.38 us
  transfers between devices with their start and end apart: 40, of which 11 were waited for; matrix products, arithmetic and copies ran while one was open for 0% of the time, Pallas kernels for 30%

profile of v2, /device:TPU:0, one launch (start us, length us, event | category | flops | bytes accessed | tf_op | source)
XLA Modules:
  0.0 211.9 jit_solution(2208892633175232239)
XLA Ops:
  1.7 3.2 %prepare.1 = (bf16[128,2176]{1,0:T(8,128)(2,1)}, bf16[64,2176]{1,0:T(8,128)(2,1)}, bf16[64,2176]{1,0:T(8,128)(2,1)}, bf16[64,2176]{1,0:T(8,128)(2,1)}, bf16[64,2176]{1,0:T(8,128)(2,1)}) custom-call(s32[1]{0:T(128)} %bitcast.4.me_ref, bf16[128,2048]{1,0:T(8,128)(2,1)} %x_ref.1, f32[1,2048]{1,0:T(1,128)} %bitcast.9, s32[2,128]{1,0:T(2,128)} %bitcast.10, ...), custom_call_target="tpu_custom_call" | custom-call | flops 134217728 | bytes 2097152 | tf_op jit(solution)/shard_map/prepare/pallas_call | solution.py:286
  4.9 2.6 %collective-permute-start.16 = (bf16[128,2176]{1,0:T(8,128)(2,1)}, bf16[128,2176]{1,0:T(8,128)(2,1)S(1)}, u32[]{:S(2)}, u32[]{:S(2)}) collective-permute-start(bf16[128,2176]{1,0:T(8,128)(2,1)} %get-tuple-element.71.meta_ref), channel_id=1, source_target_pairs={{0,2},{1,3},{2,4},{3,5},{4,6},{5,7},{6,0},{7,1},{8,10},{9,11},{10,... | collective-permute-start | bytes 1671176 | tf_op jit(solution)/shard_map/ppermute | solution.py:465
  7.5 15.5 %collective-permute-done.16.block_ref.meta_ref = bf16[128,2176]{1,0:T(8,128)(2,1)S(1)} collective-permute-done((bf16[128,2176]{1,0:T(8,128)(2,1)}, bf16[128,2176]{1,0:T(8,128)(2,1)S(1)}, u32[]{:S(2)}, u32[]{:S(2)}) %collective-permute-start.16) | collective-permute-done | bytes 557088 | tf_op jit(solution)/shard_map/ppermute | solution.py:465
  23.0 16.3 %collective-permute-done.24.block_ref.meta_ref = bf16[128,2176]{1,0:T(8,128)(2,1)} collective-permute-done((bf16[128,2176]{1,0:T(8,128)(2,1)S(1)}, bf16[128,2176]{1,0:T(8,128)(2,1)}, u32[]{:S(2)}, u32[]{:S(2)}) %collective-permute-start.24) | collective-permute-done | bytes 557088 | tf_op jit(solution)/shard_map/ppermute | solution.py:465
  39.3 6.4 %mixer_local.2 = (f32[512,128]{1,0:T(8,128)}, bf16[512,128]{1,0:T(8,128)(2,1)}, f32[1,128,256]{2,1,0:T(8,128)}) custom-call(f32[2]{0:T(128)} %rate_ref.3, bf16[512,256]{1,0:T(8,128)(2,1)} %q_ref.3, bf16[512,256]{1,0:T(8,128)(2,1)} %k_ref.3, bf16[512,256]{1,0:T(8,128)(2,1)} %v_ref.3, bf16[2,512]{1,0:T(2,128)(2,1)} %write_ref.3, bf16[2,512]{1,0:T(2,128)(2,1)} %decay_ref.3, ...), custom_call_target="tpu_custom_call" | custom-call | flops 2617245696 | bytes 917504 | tf_op jit(solution)/shard_map/mixer_local/pallas_call | solution.py:128
  45.7 1.4 dispatch.3
  47.9 7.0 %collective-permute-done.25.block_ref.meta_ref = bf16[128,2176]{1,0:T(8,128)(2,1)S(1)} collective-permute-done((bf16[128,2176]{1,0:T(8,128)(2,1)}, bf16[128,2176]{1,0:T(8,128)(2,1)S(1)}, u32[]{:S(2)}, u32[]{:S(2)}) %collective-permute-start.25) | collective-permute-done | bytes 557088 | tf_op jit(solution)/shard_map/ppermute | solution.py:465
  54.8 1.0 collective-permute-start.17
  55.9 1.6 collective-permute-start.18
  57.4 0.9 collective-permute-start.19
  58.4 6.6 %mixer_local.3 = (f32[512,128]{1,0:T(8,128)}, bf16[512,128]{1,0:T(8,128)(2,1)}, f32[2,128,256]{2,1,0:T(8,128)}) custom-call(f32[2]{0:T(128)} %rate_ref.3, bf16[512,256]{1,0:T(8,128)(2,1)} %q_ref.3, bf16[512,256]{1,0:T(8,128)(2,1)} %k_ref.3, bf16[512,256]{1,0:T(8,128)(2,1)} %v_ref.3, bf16[2,512]{1,0:T(2,128)(2,1)} %write_ref.3, bf16[2,512]{1,0:T(2,128)(2,1)} %decay_ref.3, ...), custom_call_target="tpu_custom_call" | custom-call | flops 2617245696 | bytes 917504 | tf_op jit(solution)/shard_map/mixer_local/pallas_call | solution.py:128
  64.9 2.5 %dispatch.5 = (bf16[64,2176]{1,0:T(8,128)(2,1)S(1)}, bf16[64,2176]{1,0:T(8,128)(2,1)}, bf16[64,2176]{1,0:T(8,128)(2,1)}, bf16[64,2176]{1,0:T(8,128)(2,1)}) custom-call(s32[1]{0:T(128)} %bitcast.4.me_ref, bf16[128,2176]{1,0:T(8,128)(2,1)} %collective-permute-done.24.block_ref.meta_ref), custom_call_target="tpu_custom_call" | custom-call | flops 142606336 | bytes 1671168 | tf_op jit(solution)/shard_map/dispatch/pallas_call | solution.py:317
  70.9 1.0 collective-permute-start.10
  71.9 1.0 collective-permute-start.32
  73.0 1.1 collective-permute-start.33
  74.0 1.4 collective-permute-start.34
  75.4 8.8 %expert_part.5 = (bf16[64,2048]{1,0:T(8,128)(2,1)}, bf16[64,2048]{1,0:T(8,128)(2,1)}, bf16[64,2048]{1,0:T(8,128)(2,1)}, bf16[64,2048]{1,0:T(8,128)(2,1)}) custom-call(s32[1]{0:T(128)} %bitcast.4.me_ref, bf16[64,2176]{1,0:T(8,128)(2,1)} %copy-done.13, bf16[64,2176]{1,0:T(8,128)(2,1)} %collective-permute-done.17.refs_1_, ...), custom_call_target="tpu_custom_call" | custom-call | flops 3221225472 | bytes 14680064 | tf_op jit(solution)/shard_map/expert_part/pallas_call | solution.py:392
  84.3 2.5 %collective-permute-done.32.refs_1_ = bf16[64,2176]{1,0:T(8,128)(2,1)} collective-permute-done((bf16[64,2176]{1,0:T(8,128)(2,1)}, bf16[64,2176]{1,0:T(8,128)(2,1)}, u32[]{:S(2)}, u32[]{:S(2)}) %collective-permute-start.32) | collective-permute-done | bytes 278560 | tf_op jit(solution)/shard_map/ppermute | solution.py:468
  86.7 1.1 collective-permute-start.11
  87.8 1.4 collective-permute-start.12
  89.2 4.0 %collective-permute-done.34.refs_3_ = bf16[64,2176]{1,0:T(8,128)(2,1)} collective-permute-done((bf16[64,2176]{1,0:T(8,128)(2,1)}, bf16[64,2176]{1,0:T(8,128)(2,1)}, u32[]{:S(2)}, u32[]{:S(2)}) %collective-permute-start.34) | collective-permute-done | bytes 278560 | tf_op jit(solution)/shard_map/ppermute | solution.py:468
  93.2 1.5 collective-permute-start.26
  94.8 1.6 copy-done
  96.4 1.6 copy-done.2
  98.0 1.6 copy-done.4
  99.5 1.6 copy-done.7
  101.1 1.0 copy-done.12
  102.1 8.1 %expert_part.7 = (bf16[64,2048]{1,0:T(8,128)(2,1)S(1)}, bf16[64,2048]{1,0:T(8,128)(2,1)S(1)}, bf16[64,2048]{1,0:T(8,128)(2,1)S(1)}, bf16[64,2048]{1,0:T(8,128)(2,1)S(1)}) custom-call(s32[1]{0:T(128)} %bitcast.4.me_ref, bf16[64,2176]{1,0:T(8,128)(2,1)S(1)} %copy-done.12, bf16[64,2176]{1,0:T(8,128)(2,1)} %collective-permute-done.32.refs_1_, ...), custom_call_target="tpu_custom_call" | custom-call | flops 3221225472 | bytes 14680064 | tf_op jit(solution)/shard_map/expert_part/pallas_call | solution.py:392
  110.8 1.5 collective-permute-start.28
  112.3 1.5 collective-permute-start.35
  114.3 8.0 %expert_part.4 = (bf16[64,2048]{1,0:T(8,128)(2,1)S(1)}, bf16[64,2048]{1,0:T(8,128)(2,1)}, bf16[64,2048]{1,0:T(8,128)(2,1)}, bf16[64,2048]{1,0:T(8,128)(2,1)S(1)}) custom-call(s32[1]{0:T(128)} %bitcast.4.me_ref, bf16[64,2176]{1,0:T(8,128)(2,1)S(1)} %copy-done.10, bf16[64,2176]{1,0:T(8,128)(2,1)} %collective-permute-done.10.refs_1_, ...), custom_call_target="tpu_custom_call" | custom-call | flops 3221225472 | bytes 14680064 | tf_op jit(solution)/shard_map/expert_part/pallas_call | solution.py:392
  122.4 1.1 collective-permute-start.20
  123.4 1.1 collective-permute-start.21
  124.5 1.4 collective-permute-start.22
  125.9 0.8 collective-permute-done.35.refs_1_
  127.4 2.6 %collective-permute-done.36.refs_2_ = bf16[64,2048]{1,0:T(8,128)(2,1)S(1)} collective-permute-done((bf16[64,2048]{1,0:T(8,128)(2,1)S(1)}, bf16[64,2048]{1,0:T(8,128)(2,1)S(1)}, u32[]{:S(2)}, u32[]{:S(2)}) %collective-permute-start.36) | collective-permute-done | bytes 262176 | tf_op jit(solution)/shard_map/ppermute | solution.py:468
  130.0 7.1 %expert_part.6 = (bf16[64,2048]{1,0:T(8,128)(2,1)S(1)}, bf16[64,2048]{1,0:T(8,128)(2,1)}, bf16[64,2048]{1,0:T(8,128)(2,1)}, bf16[64,2048]{1,0:T(8,128)(2,1)}) custom-call(s32[1]{0:T(128)} %bitcast.4.me_ref, bf16[64,2176]{1,0:T(8,128)(2,1)S(1)} %get-tuple-element.94.refs_0_, bf16[64,2176]{1,0:T(8,128)(2,1)S(1)} %collective-permute-done.26.refs_1_, ...), custom_call_target="tpu_custom_call" | custom-call | flops 3221225472 | bytes 14680064 | tf_op jit(solution)/shard_map/expert_part/pallas_call | solution.py:392
  137.8 6.0 %collective-permute-done.37.refs_3_ = bf16[64,2048]{1,0:T(8,128)(2,1)S(1)} collective-permute-done((bf16[64,2048]{1,0:T(8,128)(2,1)S(1)}, bf16[64,2048]{1,0:T(8,128)(2,1)S(1)}, u32[]{:S(2)}, u32[]{:S(2)}) %collective-permute-start.37) | collective-permute-done | bytes 262176 | tf_op jit(solution)/shard_map/ppermute | solution.py:468
  144.3 2.0 collect.6
  147.0 1.0 collective-permute-start.14
  148.7 1.7 collective-permute-start.29
  151.2 0.9 copy-done.24
  152.2 0.9 copy-done.27
  154.5 0.9 collective-permute-start.4
  155.4 0.9 copy-done.18
  156.3 0.9 copy-done.20
  157.3 0.9 copy-done.22
  158.2 2.2 %collect.4 = bf16[128,2048]{1,0:T(8,128)(2,1)} custom-call(s32[1]{0:T(128)} %bitcast.4.me_ref, bf16[128,2176]{1,0:T(8,128)(2,1)S(1)} %collective-permute-done.16.block_ref.meta_ref, bf16[64,2048]{1,0:T(8,128)(2,1)S(1)} %copy-done.18, bf16[64,2048]{1,0:T(8,128)(2,1)S(1)} %copy-done.20, bf16[64,2048]{1,0:T(8,128)(2,1)S(1)} %copy-done.22, ...), custom_call_target="tpu_custom_call" | custom-call | flops 134217728 | bytes 2097152 | tf_op jit(solution)/shard_map/collect/pallas_call | solution.py:422
  160.4 3.8 %collective-permute-start.23 = (bf16[128,2048]{1,0:T(8,128)(2,1)}, bf16[128,2048]{1,0:T(8,128)(2,1)S(1)}, u32[]{:S(2)}, u32[]{:S(2)}) collective-permute-start(bf16[128,2048]{1,0:T(8,128)(2,1)} %collect.4), channel_id=1, source_target_pairs={{0,6},{1,7},{2,0},{3,1},{4,2},{5,3},{6,4},{7,5},{8,14},{9,15},{10,... | collective-permute-start | bytes 1572872 | tf_op jit(solution)/shard_map/ppermute | solution.py:465
  164.3 1.2 collective-permute-start.30
  166.1 0.8 collective-permute-start.31
  166.9 2.4 %attend.1 = (bf16[4,64,256]{2,1,0:T(8,128)(2,1)}, bf16[4,64,256]{2,1,0:T(8,128)(2,1)}) custom-call(s32[1]{0:T(128)} %bitcast.1.late_ref, s32[1]{0:T(128)} %bitcast.2.core_ref, f32[512,128]{1,0:T(8,128)} %get-tuple-element.56.refs_0_, f32[512,128]{1,0:T(8,128)} %get-tuple-element.58.refs_1_, bf16[512,128]{1,0:T(8,128)(2,1)} %get-tuple-element.59.refs_2_, ...), custom_call_target="tpu_custom_call" | custom-call | flops 201326592 | bytes 1310720 | tf_op jit(solution)/shard_map/attend/pallas_call | solution.py:191
  169.3 1.5 collective-permute-done.5.theirs_ref
  170.9 2.1 %collective-permute-start.15 = (bf16[64,2048]{1,0:T(8,128)(2,1)}, bf16[64,2048]{1,0:T(8,128)(2,1)S(1)}, u32[]{:S(2)}, u32[]{:S(2)}) collective-permute-start(bf16[64,2048]{1,0:T(8,128)(2,1)} %copy-done.34), channel_id=1, source_target_pairs={{0,24},{8,16},{16,8},{24,0},{1,25},{9,17},{17,9},{25,1},{2,26},{10... | collective-permute-start | bytes 786440 | tf_op jit(solution)/shard_map/ppermute | solution.py:468
  173.0 0.9 copy-done.28
  173.9 2.3 %project.1 = (bf16[64,2048]{1,0:T(8,128)(2,1)S(1)}, bf16[64,2048]{1,0:T(8,128)(2,1)S(1)}, bf16[64,2048]{1,0:T(8,128)(2,1)S(1)}, bf16[64,2048]{1,0:T(8,128)(2,1)S(1)}) custom-call(s32[1]{0:T(128)} %bitcast.level_ref, bf16[4,64,256]{2,1,0:T(8,128)(2,1)S(1)} %copy-done.28, bf16[4,64,256]{2,1,0:T(8,128)(2,1)S(1)} %collective-permute-done.5.theirs_ref, ...), custom_call_target="tpu_custom_call" | custom-call | flops 536870912 | bytes 3145728 | tf_op jit(solution)/shard_map/project/pallas_call | solution.py:235
  176.4 2.0 collective-permute-start.9
  178.4 0.9 copy-done.15
  179.3 1.7 collect.7
  181.1 1.5 collective-permute-start.39
  183.1 2.2 %collective-permute-done.7 = bf16[64,2048]{1,0:T(8,128)(2,1)S(1)} collective-permute-done((bf16[64,2048]{1,0:T(8,128)(2,1)S(1)}, bf16[64,2048]{1,0:T(8,128)(2,1)S(1)}, u32[]{:S(2)}, u32[]{:S(2)}) %collective-permute-start.7) | collective-permute-done | bytes 262176 | tf_op jit(solution)/shard_map/ppermute | solution.py:465
  185.3 24.8 %collective-permute-done.8 = bf16[64,2048]{1,0:T(8,128)(2,1)S(1)} collective-permute-done((bf16[64,2048]{1,0:T(8,128)(2,1)S(1)}, bf16[64,2048]{1,0:T(8,128)(2,1)S(1)}, u32[]{:S(2)}, u32[]{:S(2)}) %collective-permute-start.8) | collective-permute-done | bytes 262176 | tf_op jit(solution)/shard_map/ppermute | solution.py:465
  210.1 0.8 add_convert_fusion.1
  210.9 0.9 add_convert_fusion
  (115 shorter events, 13.1 us)
Async XLA Ops:
  0.6 55.2 %collective-permute-start = (bf16[4,128,2048]{2,1,0:T(8,128)(2,1)}, bf16[4,128,2048]{2,1,0:T(8,128)(2,1)S(1)}, u32[]{:S(2)}, u32[]{:S(2)}) collective-permute-start(bf16[4,128,2048]{2,1,0:T(8,128)(2,1)} %refs_4_.3), channel_id=1, source_target_pairs={{0,1},{1,0},{2,3},{3,2},{4,5},{5,4},{6,7},{7,6},{8,9},{9,8},{10,11... | collective-permute-start | bytes 6291464 | tf_op jit(solution)/shard_map/ppermute | solution.py:462
  1.2 56.2 %collective-permute-start.1 = (bf16[4,128,2048]{2,1,0:T(8,128)(2,1)}, bf16[4,128,2048]{2,1,0:T(8,128)(2,1)}, u32[]{:S(2)}, u32[]{:S(2)}) collective-permute-start(bf16[4,128,2048]{2,1,0:T(8,128)(2,1)} %refs_6_.3), channel_id=1, source_target_pairs={{0,1},{1,0},{2,3},{3,2},{4,5},{5,4},{6,7},{7,6},{8,9},{9,8},{10,11... | collective-permute-start | bytes 6291464 | tf_op jit(solution)/shard_map/ppermute | solution.py:462
  1.3 69.6 %collective-permute-start.2 = (bf16[4,128,2048]{2,1,0:T(8,128)(2,1)}, bf16[4,128,2048]{2,1,0:T(8,128)(2,1)}, u32[]{:S(2)}, u32[]{:S(2)}) collective-permute-start(bf16[4,128,2048]{2,1,0:T(8,128)(2,1)} %refs_8_.3), channel_id=1, source_target_pairs={{0,1},{1,0},{2,3},{3,2},{4,5},{5,4},{6,7},{7,6},{8,9},{9,8},{10,11... | collective-permute-start | bytes 6291464 | tf_op jit(solution)/shard_map/ppermute | solution.py:462
  4.9 18.1 %collective-permute-start.16 = (bf16[128,2176]{1,0:T(8,128)(2,1)}, bf16[128,2176]{1,0:T(8,128)(2,1)S(1)}, u32[]{:S(2)}, u32[]{:S(2)}) collective-permute-start(bf16[128,2176]{1,0:T(8,128)(2,1)} %get-tuple-element.71.meta_ref), channel_id=1, source_target_pairs={{0,2},{1,3},{2,4},{3,5},{4,6},{5,7},{6,0},{7,1},{8,10},{9,11},{10,... | collective-permute-start | bytes 1671176 | tf_op jit(solution)/shard_map/ppermute | solution.py:465
  23.0 16.3 %collective-permute-start.24 = (bf16[128,2176]{1,0:T(8,128)(2,1)S(1)}, bf16[128,2176]{1,0:T(8,128)(2,1)}, u32[]{:S(2)}, u32[]{:S(2)}) collective-permute-start(bf16[128,2176]{1,0:T(8,128)(2,1)S(1)} %collective-permute-done.16.block_ref.meta_ref), channel_id=1, source_target_pairs={{0,2},{1,3},{2,4},{3,5},{4,6},{5,7},{6,0},{7,1},{8,10},{9,11},{10,... | collective-permute-start | bytes 1671176 | tf_op jit(solution)/shard_map/ppermute | solution.py:465
  39.3 15.5 %collective-permute-start.25 = (bf16[128,2176]{1,0:T(8,128)(2,1)}, bf16[128,2176]{1,0:T(8,128)(2,1)S(1)}, u32[]{:S(2)}, u32[]{:S(2)}) collective-permute-start(bf16[128,2176]{1,0:T(8,128)(2,1)} %collective-permute-done.24.block_ref.meta_ref), channel_id=1, source_target_pairs={{0,2},{1,3},{2,4},{3,5},{4,6},{5,7},{6,0},{7,1},{8,10},{9,11},{10,... | collective-permute-start | bytes 1671176 | tf_op jit(solution)/shard_map/ppermute | solution.py:465
  39.3 74.5 %collective-permute-start.6 = (bf16[256,2048]{1,0:T(8,128)(2,1)}, bf16[256,2048]{1,0:T(8,128)(2,1)}, u32[]{:S(2)}, u32[]{:S(2)}) collective-permute-start(bf16[256,2048]{1,0:T(8,128)(2,1)} %own_ref.1), channel_id=1, source_target_pairs={{0,1},{1,0},{2,3},{3,2},{4,5},{5,4},{6,7},{7,6},{8,9},{9,8},{10,11... | collective-permute-start | bytes 3145736 | tf_op jit(solution)/shard_map/ppermute | solution.py:462
  54.8 17.1 %collective-permute-start.17 = (bf16[64,2176]{1,0:T(8,128)(2,1)}, bf16[64,2176]{1,0:T(8,128)(2,1)}, u32[]{:S(2)}, u32[]{:S(2)}) collective-permute-start(bf16[64,2176]{1,0:T(8,128)(2,1)} %get-tuple-element.87), channel_id=1, source_target_pairs={{0,8},{8,0},{16,24},{24,16},{1,9},{9,1},{17,25},{25,17},{2,10},{10... | collective-permute-start | bytes 835592 | tf_op jit(solution)/shard_map/ppermute | solution.py:468
  55.9 9.1 %copy-start.6 = (bf16[4,128,2048]{2,1,0:T(8,128)(2,1)}, bf16[4,128,2048]{2,1,0:T(8,128)(2,1)S(1)}, u32[]{:S(2)}) copy-start(bf16[4,128,2048]{2,1,0:T(8,128)(2,1)S(1)} %collective-permute-done.refs_5_) | copy-start | bytes 6291460
  55.9 17.1 %collective-permute-start.18 = (bf16[64,2176]{1,0:T(8,128)(2,1)}, bf16[64,2176]{1,0:T(8,128)(2,1)}, u32[]{:S(2)}, u32[]{:S(2)}) collective-permute-start(bf16[64,2176]{1,0:T(8,128)(2,1)} %get-tuple-element.88), channel_id=1, source_target_pairs={{0,16},{8,24},{16,0},{24,8},{1,17},{9,25},{17,1},{25,9},{2,18},{10... | collective-permute-start | bytes 835592 | tf_op jit(solution)/shard_map/ppermute | solution.py:468
  57.4 16.6 %collective-permute-start.19 = (bf16[64,2176]{1,0:T(8,128)(2,1)}, bf16[64,2176]{1,0:T(8,128)(2,1)}, u32[]{:S(2)}, u32[]{:S(2)}) collective-permute-start(bf16[64,2176]{1,0:T(8,128)(2,1)} %get-tuple-element.89), channel_id=1, source_target_pairs={{0,24},{8,16},{16,8},{24,0},{1,25},{9,17},{17,9},{25,1},{2,26},{10... | collective-permute-start | bytes 835592 | tf_op jit(solution)/shard_map/ppermute | solution.py:468
  70.9 39.3 %collective-permute-start.10 = (bf16[64,2176]{1,0:T(8,128)(2,1)}, bf16[64,2176]{1,0:T(8,128)(2,1)}, u32[]{:S(2)}, u32[]{:S(2)}) collective-permute-start(bf16[64,2176]{1,0:T(8,128)(2,1)} %get-tuple-element.73), channel_id=1, source_target_pairs={{0,8},{8,0},{16,24},{24,16},{1,9},{9,1},{17,25},{25,17},{2,10},{10... | collective-permute-start | bytes 835592 | tf_op jit(solution)/shard_map/ppermute | solution.py:468
  71.9 14.8 %collective-permute-start.32 = (bf16[64,2176]{1,0:T(8,128)(2,1)}, bf16[64,2176]{1,0:T(8,128)(2,1)}, u32[]{:S(2)}, u32[]{:S(2)}) collective-permute-start(bf16[64,2176]{1,0:T(8,128)(2,1)} %get-tuple-element.103), channel_id=1, source_target_pairs={{0,8},{8,0},{16,24},{24,16},{1,9},{9,1},{17,25},{25,17},{2,10},{10... | collective-permute-start | bytes 835592 | tf_op jit(solution)/shard_map/ppermute | solution.py:468
  73.0 14.8 %collective-permute-start.33 = (bf16[64,2176]{1,0:T(8,128)(2,1)}, bf16[64,2176]{1,0:T(8,128)(2,1)}, u32[]{:S(2)}, u32[]{:S(2)}) collective-permute-start(bf16[64,2176]{1,0:T(8,128)(2,1)} %get-tuple-element.104), channel_id=1, source_target_pairs={{0,16},{8,24},{16,0},{24,8},{1,17},{9,25},{17,1},{25,9},{2,18},{10... | collective-permute-start | bytes 835592 | tf_op jit(solution)/shard_map/ppermute | solution.py:468
  74.0 19.2 %collective-permute-start.34 = (bf16[64,2176]{1,0:T(8,128)(2,1)}, bf16[64,2176]{1,0:T(8,128)(2,1)}, u32[]{:S(2)}, u32[]{:S(2)}) collective-permute-start(bf16[64,2176]{1,0:T(8,128)(2,1)} %get-tuple-element.105), channel_id=1, source_target_pairs={{0,24},{8,16},{16,8},{24,0},{1,25},{9,17},{17,9},{25,1},{2,26},{10... | collective-permute-start | bytes 835592 | tf_op jit(solution)/shard_map/ppermute | solution.py:468
  86.7 24.1 %collective-permute-start.11 = (bf16[64,2176]{1,0:T(8,128)(2,1)}, bf16[64,2176]{1,0:T(8,128)(2,1)S(1)}, u32[]{:S(2)}, u32[]{:S(2)}) collective-permute-start(bf16[64,2176]{1,0:T(8,128)(2,1)} %get-tuple-element.74), channel_id=1, source_target_pairs={{0,16},{8,24},{16,0},{24,8},{1,17},{9,25},{17,1},{25,9},{2,18},{10... | collective-permute-start | bytes 835592 | tf_op jit(solution)/shard_map/ppermute | solution.py:468
  87.8 24.5 %collective-permute-start.12 = (bf16[64,2176]{1,0:T(8,128)(2,1)}, bf16[64,2176]{1,0:T(8,128)(2,1)S(1)}, u32[]{:S(2)}, u32[]{:S(2)}) collective-permute-start(bf16[64,2176]{1,0:T(8,128)(2,1)} %get-tuple-element.75), channel_id=1, source_target_pairs={{0,24},{8,16},{16,8},{24,0},{1,25},{9,17},{17,9},{25,1},{2,26},{10... | collective-permute-start | bytes 835592 | tf_op jit(solution)/shard_map/ppermute | solution.py:468
  93.2 29.1 %collective-permute-start.26 = (bf16[64,2176]{1,0:T(8,128)(2,1)}, bf16[64,2176]{1,0:T(8,128)(2,1)S(1)}, u32[]{:S(2)}, u32[]{:S(2)}) collective-permute-start(bf16[64,2176]{1,0:T(8,128)(2,1)} %copy-done.33), channel_id=1, source_target_pairs={{0,8},{8,0},{16,24},{24,16},{1,9},{9,1},{17,25},{25,17},{2,10},{10... | collective-permute-start | bytes 835592 | tf_op jit(solution)/shard_map/ppermute | solution.py:468
  94.8 1.6 copy-start
  96.4 1.6 copy-start.2
  98.0 1.6 copy-start.4
  99.5 1.6 copy-start.7
  101.1 1.0 copy-start.12
  102.1 8.2 %copy-start.32 = (bf16[64,2176]{1,0:T(8,128)(2,1)S(1)}, bf16[64,2176]{1,0:T(8,128)(2,1)}, u32[]{:S(2)}) copy-start(bf16[64,2176]{1,0:T(8,128)(2,1)} %copy-done.31) | copy-start | bytes 835588
  102.1 8.7 %copy-start.30 = (bf16[64,2176]{1,0:T(8,128)(2,1)S(1)}, bf16[64,2176]{1,0:T(8,128)(2,1)}, u32[]{:S(2)}) copy-start(bf16[64,2176]{1,0:T(8,128)(2,1)} %copy-done.29) | copy-start | bytes 835588
  102.1 12.2 %copy-start.1 = (bf16[4,128,2048]{2,1,0:T(8,128)(2,1)S(1)}, bf16[4,128,2048]{2,1,0:T(8,128)(2,1)}, u32[]{:S(2)}) copy-start(bf16[4,128,2048]{2,1,0:T(8,128)(2,1)} %refs_4_.3) | copy-start | bytes 6291460
  102.1 12.2 %copy-start.3 = (bf16[4,128,2048]{2,1,0:T(8,128)(2,1)S(1)}, bf16[4,128,2048]{2,1,0:T(8,128)(2,1)}, u32[]{:S(2)}) copy-start(bf16[4,128,2048]{2,1,0:T(8,128)(2,1)} %refs_6_.3) | copy-start | bytes 6291460
  102.1 12.2 %copy-start.5 = (bf16[4,128,2048]{2,1,0:T(8,128)(2,1)S(1)}, bf16[4,128,2048]{2,1,0:T(8,128)(2,1)}, u32[]{:S(2)}) copy-start(bf16[4,128,2048]{2,1,0:T(8,128)(2,1)} %refs_8_.3) | copy-start | bytes 6291460
  102.1 12.2 %copy-start.10 = (bf16[64,2176]{1,0:T(8,128)(2,1)S(1)}, bf16[64,2176]{1,0:T(8,128)(2,1)}, u32[]{:S(2)}) copy-start(bf16[64,2176]{1,0:T(8,128)(2,1)} %get-tuple-element.72.refs_0_) | copy-start | bytes 835588
  110.3 13.2 %collective-permute-start.27 = (bf16[64,2176]{1,0:T(8,128)(2,1)S(1)}, bf16[64,2176]{1,0:T(8,128)(2,1)S(1)}, u32[]{:S(2)}, u32[]{:S(2)}) collective-permute-start(bf16[64,2176]{1,0:T(8,128)(2,1)S(1)} %copy-done.32), channel_id=1, source_target_pairs={{0,16},{8,24},{16,0},{24,8},{1,17},{9,25},{17,1},{25,9},{2,18},{10... | collective-permute-start | bytes 835592 | tf_op jit(solution)/shard_map/ppermute | solution.py:468
  110.8 13.7 %collective-permute-start.28 = (bf16[64,2176]{1,0:T(8,128)(2,1)S(1)}, bf16[64,2176]{1,0:T(8,128)(2,1)S(1)}, u32[]{:S(2)}, u32[]{:S(2)}) collective-permute-start(bf16[64,2176]{1,0:T(8,128)(2,1)S(1)} %copy-done.30), channel_id=1, source_target_pairs={{0,24},{8,16},{16,8},{24,0},{1,25},{9,17},{17,9},{25,1},{2,26},{10... | collective-permute-start | bytes 835592 | tf_op jit(solution)/shard_map/ppermute | solution.py:468
  112.3 14.4 %collective-permute-start.35 = (bf16[64,2048]{1,0:T(8,128)(2,1)S(1)}, bf16[64,2048]{1,0:T(8,128)(2,1)S(1)}, u32[]{:S(2)}, u32[]{:S(2)}) collective-permute-start(bf16[64,2048]{1,0:T(8,128)(2,1)S(1)} %get-tuple-element.107), channel_id=1, source_target_pairs={{0,8},{8,0},{16,24},{24,16},{1,9},{9,1},{17,25},{25,17},{2,10},{10... | collective-permute-start | bytes 786440 | tf_op jit(solution)/shard_map/ppermute | solution.py:468
  113.8 16.2 %collective-permute-start.36 = (bf16[64,2048]{1,0:T(8,128)(2,1)S(1)}, bf16[64,2048]{1,0:T(8,128)(2,1)S(1)}, u32[]{:S(2)}, u32[]{:S(2)}) collective-permute-start(bf16[64,2048]{1,0:T(8,128)(2,1)S(1)} %get-tuple-element.108), channel_id=1, source_target_pairs={{0,16},{8,24},{16,0},{24,8},{1,17},{9,25},{17,1},{25,9},{2,18},{10... | collective-permute-start | bytes 786440 | tf_op jit(solution)/shard_map/ppermute | solution.py:468
  114.3 8.0 %copy-start.37 = (bf16[64,2048]{1,0:T(8,128)(2,1)S(1)}, bf16[64,2048]{1,0:T(8,128)(2,1)}, u32[]{:S(2)}) copy-start(bf16[64,2048]{1,0:T(8,128)(2,1)} %get-tuple-element.91) | copy-start | bytes 786436
  114.3 9.1 %copy-start.36 = (bf16[64,2048]{1,0:T(8,128)(2,1)S(1)}, bf16[64,2048]{1,0:T(8,128)(2,1)}, u32[]{:S(2)}) copy-start(bf16[64,2048]{1,0:T(8,128)(2,1)} %get-tuple-element.92) | copy-start | bytes 786436
  114.3 15.7 %copy-start.23 = (f32[2,128,256]{2,1,0:T(8,128)S(1)}, f32[2,128,256]{2,1,0:T(8,128)}, u32[]{:S(2)}) copy-start(f32[2,128,256]{2,1,0:T(8,128)} %get-tuple-element.62.own_ref) | copy-start | bytes 786436
  122.3 7.7 %copy-start.34 = (bf16[64,2048]{1,0:T(8,128)(2,1)}, bf16[64,2048]{1,0:T(8,128)(2,1)S(1)}, u32[]{:S(2)}) copy-start(bf16[64,2048]{1,0:T(8,128)(2,1)S(1)} %get-tuple-element.85) | copy-start | bytes 786436
  122.4 24.0 %collective-permute-start.20 = (bf16[64,2048]{1,0:T(8,128)(2,1)S(1)}, bf16[64,2048]{1,0:T(8,128)(2,1)S(1)}, u32[]{:S(2)}, u32[]{:S(2)}) collective-permute-start(bf16[64,2048]{1,0:T(8,128)(2,1)S(1)} %copy-done.37), channel_id=1, source_target_pairs={{0,8},{8,0},{16,24},{24,16},{1,9},{9,1},{17,25},{25,17},{2,10},{10... | collective-permute-start | bytes 786440 | tf_op jit(solution)/shard_map/ppermute | solution.py:468
  123.4 24.6 %collective-permute-start.21 = (bf16[64,2048]{1,0:T(8,128)(2,1)S(1)}, bf16[64,2048]{1,0:T(8,128)(2,1)S(1)}, u32[]{:S(2)}, u32[]{:S(2)}) collective-permute-start(bf16[64,2048]{1,0:T(8,128)(2,1)S(1)} %copy-done.36), channel_id=1, source_target_pairs={{0,16},{8,24},{16,0},{24,8},{1,17},{9,25},{17,1},{25,9},{2,18},{10... | collective-permute-start | bytes 786440 | tf_op jit(solution)/shard_map/ppermute | solution.py:468
  124.5 30.0 %collective-permute-start.22 = (bf16[64,2048]{1,0:T(8,128)(2,1)}, bf16[64,2048]{1,0:T(8,128)(2,1)}, u32[]{:S(2)}, u32[]{:S(2)}) collective-permute-start(bf16[64,2048]{1,0:T(8,128)(2,1)} %get-tuple-element.93), channel_id=1, source_target_pairs={{0,24},{8,16},{16,8},{24,0},{1,25},{9,17},{17,9},{25,1},{2,26},{10... | collective-permute-start | bytes 786440 | tf_op jit(solution)/shard_map/ppermute | solution.py:468
  126.7 17.1 %collective-permute-start.37 = (bf16[64,2048]{1,0:T(8,128)(2,1)S(1)}, bf16[64,2048]{1,0:T(8,128)(2,1)S(1)}, u32[]{:S(2)}, u32[]{:S(2)}) collective-permute-start(bf16[64,2048]{1,0:T(8,128)(2,1)S(1)} %get-tuple-element.109), channel_id=1, source_target_pairs={{0,24},{8,16},{16,8},{24,0},{1,25},{9,17},{17,9},{25,1},{2,26},{10... | collective-permute-start | bytes 786440 | tf_op jit(solution)/shard_map/ppermute | solution.py:468
  130.0 20.4 %collective-permute-start.3 = (f32[2,128,256]{2,1,0:T(8,128)S(1)}, f32[2,128,256]{2,1,0:T(8,128)S(1)}, u32[]{:S(2)}, u32[]{:S(2)}) collective-permute-start(f32[2,128,256]{2,1,0:T(8,128)S(1)} %copy-done.23), channel_id=1, source_target_pairs={{0,8},{8,0},{16,24},{24,16},{1,9},{9,1},{17,25},{25,17},{2,10},{10... | collective-permute-start | bytes 786440 | tf_op jit(solution)/shard_map/ppermute | solution.py:468
  143.8 16.6 %collective-permute-start.13 = (bf16[64,2048]{1,0:T(8,128)(2,1)}, bf16[64,2048]{1,0:T(8,128)(2,1)S(1)}, u32[]{:S(2)}, u32[]{:S(2)}) collective-permute-start(bf16[64,2048]{1,0:T(8,128)(2,1)} %get-tuple-element.83), channel_id=1, source_target_pairs={{0,8},{8,0},{16,24},{24,16},{1,9},{9,1},{17,25},{25,17},{2,10},{10... | collective-permute-start | bytes 786440 | tf_op jit(solution)/shard_map/ppermute | solution.py:468
  147.0 17.2 %collective-permute-start.14 = (bf16[64,2048]{1,0:T(8,128)(2,1)}, bf16[64,2048]{1,0:T(8,128)(2,1)S(1)}, u32[]{:S(2)}, u32[]{:S(2)}) collective-permute-start(bf16[64,2048]{1,0:T(8,128)(2,1)} %get-tuple-element.84), channel_id=1, source_target_pairs={{0,16},{8,24},{16,0},{24,8},{1,17},{9,25},{17,1},{25,9},{2,18},{10... | collective-permute-start | bytes 786440 | tf_op jit(solution)/shard_map/ppermute | solution.py:468
  148.7 20.6 %collective-permute-start.29 = (bf16[64,2048]{1,0:T(8,128)(2,1)}, bf16[64,2048]{1,0:T(8,128)(2,1)}, u32[]{:S(2)}, u32[]{:S(2)}) collective-permute-start(bf16[64,2048]{1,0:T(8,128)(2,1)} %get-tuple-element.99), channel_id=1, source_target_pairs={{0,8},{8,0},{16,24},{24,16},{1,9},{9,1},{17,25},{25,17},{2,10},{10... | collective-permute-start | bytes 786440 | tf_op jit(solution)/shard_map/ppermute | solution.py:468
  151.1 25.3 %collective-permute-start.38 = (bf16[128,2048]{1,0:T(8,128)(2,1)}, bf16[128,2048]{1,0:T(8,128)(2,1)}, u32[]{:S(2)}, u32[]{:S(2)}) collective-permute-start(bf16[128,2048]{1,0:T(8,128)(2,1)} %collect.6), channel_id=1, source_target_pairs={{0,2},{1,3},{2,4},{3,5},{4,6},{5,7},{6,0},{7,1},{8,10},{9,11},{10,... | collective-permute-start | bytes 1572872 | tf_op jit(solution)/shard_map/ppermute | solution.py:465
  151.2 1.0 copy-start.24
  152.2 0.9 copy-start.27
  153.1 19.9 %copy-start.8 = (bf16[256,2048]{1,0:T(8,128)(2,1)S(1)}, bf16[256,2048]{1,0:T(8,128)(2,1)}, u32[]{:S(2)}) copy-start(bf16[256,2048]{1,0:T(8,128)(2,1)} %own_ref.1) | copy-start | bytes 3145732
  154.5 11.0 %collective-permute-start.4 = (f32[2,128,128]{2,1,0:T(8,128)S(1)}, f32[2,128,128]{2,1,0:T(8,128)S(1)}, u32[]{:S(2)}, u32[]{:S(2)}) collective-permute-start(f32[2,128,128]{2,1,0:T(8,128)S(1)} %slice.3), channel_id=1, source_target_pairs={{0,16},{8,24},{16,0},{24,8},{1,17},{9,25},{17,1},{25,9},{2,18},{10... | collective-permute-start | bytes 393224 | tf_op jit(solution)/shard_map/ppermute | solution.py:468
  155.4 0.9 copy-start.18
  156.3 0.9 copy-start.20
  160.4 22.2 %collective-permute-start.23 = (bf16[128,2048]{1,0:T(8,128)(2,1)}, bf16[128,2048]{1,0:T(8,128)(2,1)S(1)}, u32[]{:S(2)}, u32[]{:S(2)}) collective-permute-start(bf16[128,2048]{1,0:T(8,128)(2,1)} %collect.4), channel_id=1, source_target_pairs={{0,6},{1,7},{2,0},{3,1},{4,2},{5,3},{6,4},{7,5},{8,14},{9,15},{10,... | collective-permute-start | bytes 1572872 | tf_op jit(solution)/shard_map/ppermute | solution.py:465
  164.3 8.7 %copy-start.16 = (bf16[64,2048]{1,0:T(8,128)(2,1)}, bf16[64,2048]{1,0:T(8,128)(2,1)S(1)}, u32[]{:S(2)}) copy-start(bf16[64,2048]{1,0:T(8,128)(2,1)S(1)} %collective-permute-done.14.refs_2_) | copy-start | bytes 786436
  164.3 12.0 %collective-permute-start.30 = (bf16[64,2048]{1,0:T(8,128)(2,1)}, bf16[64,2048]{1,0:T(8,128)(2,1)}, u32[]{:S(2)}, u32[]{:S(2)}) collective-permute-start(bf16[64,2048]{1,0:T(8,128)(2,1)} %get-tuple-element.100), channel_id=1, source_target_pairs={{0,16},{8,24},{16,0},{24,8},{1,17},{9,25},{17,1},{25,9},{2,18},{10... | collective-permute-start | bytes 786440 | tf_op jit(solution)/shard_map/ppermute | solution.py:468
  166.1 10.3 %collective-permute-start.31 = (bf16[64,2048]{1,0:T(8,128)(2,1)}, bf16[64,2048]{1,0:T(8,128)(2,1)}, u32[]{:S(2)}, u32[]{:S(2)}) collective-permute-start(bf16[64,2048]{1,0:T(8,128)(2,1)} %get-tuple-element.101), channel_id=1, source_target_pairs={{0,24},{8,16},{16,8},{24,0},{1,25},{9,17},{17,9},{25,1},{2,26},{10... | collective-permute-start | bytes 786440 | tf_op jit(solution)/shard_map/ppermute | solution.py:468
  169.3 1.6 collective-permute-start.5
  170.9 10.2 %collective-permute-start.15 = (bf16[64,2048]{1,0:T(8,128)(2,1)}, bf16[64,2048]{1,0:T(8,128)(2,1)S(1)}, u32[]{:S(2)}, u32[]{:S(2)}) collective-permute-start(bf16[64,2048]{1,0:T(8,128)(2,1)} %copy-done.34), channel_id=1, source_target_pairs={{0,24},{8,16},{16,8},{24,0},{1,25},{9,17},{17,9},{25,1},{2,26},{10... | collective-permute-start | bytes 786440 | tf_op jit(solution)/shard_map/ppermute | solution.py:468
  173.9 8.7 %copy-start.9 = (bf16[128,2176]{1,0:T(8,128)(2,1)S(1)}, bf16[128,2176]{1,0:T(8,128)(2,1)}, u32[]{:S(2)}) copy-start(bf16[128,2176]{1,0:T(8,128)(2,1)} %get-tuple-element.71.meta_ref) | copy-start | bytes 1671172
  173.9 8.7 %copy-start.17 = (bf16[64,2048]{1,0:T(8,128)(2,1)S(1)}, bf16[64,2048]{1,0:T(8,128)(2,1)}, u32[]{:S(2)}) copy-start(bf16[64,2048]{1,0:T(8,128)(2,1)} %copy-done.16) | copy-start | bytes 786436
  176.2 9.1 %collective-permute-start.7 = (bf16[64,2048]{1,0:T(8,128)(2,1)S(1)}, bf16[64,2048]{1,0:T(8,128)(2,1)S(1)}, u32[]{:S(2)}, u32[]{:S(2)}) collective-permute-start(bf16[64,2048]{1,0:T(8,128)(2,1)S(1)} %get-tuple-element.68), channel_id=1, source_target_pairs={{0,6},{1,7},{2,0},{3,1},{4,2},{5,3},{6,4},{7,5},{8,14},{9,15},{10,... | collective-permute-start | bytes 786440 | tf_op jit(solution)/shard_map/ppermute | solution.py:465
  176.4 33.7 %collective-permute-start.8 = (bf16[64,2048]{1,0:T(8,128)(2,1)S(1)}, bf16[64,2048]{1,0:T(8,128)(2,1)S(1)}, u32[]{:S(2)}, u32[]{:S(2)}) collective-permute-start(bf16[64,2048]{1,0:T(8,128)(2,1)S(1)} %get-tuple-element.69), channel_id=1, source_target_pairs={{0,4},{1,5},{2,6},{3,7},{4,0},{5,1},{6,2},{7,3},{8,12},{9,13},{10,... | collective-permute-start | bytes 786440 | tf_op jit(solution)/shard_map/ppermute | solution.py:465
  176.4 33.7 %collective-permute-start.9 = (bf16[64,2048]{1,0:T(8,128)(2,1)S(1)}, bf16[64,2048]{1,0:T(8,128)(2,1)S(1)}, u32[]{:S(2)}, u32[]{:S(2)}) collective-permute-start(bf16[64,2048]{1,0:T(8,128)(2,1)S(1)} %get-tuple-element.70), channel_id=1, source_target_pairs={{0,2},{1,3},{2,4},{3,5},{4,6},{5,7},{6,0},{7,1},{8,10},{9,11},{10,... | collective-permute-start | bytes 786440 | tf_op jit(solution)/shard_map/ppermute | solution.py:465
  181.1 29.9 %collective-permute-start.39 = (bf16[128,2048]{1,0:T(8,128)(2,1)S(1)}, bf16[128,2048]{1,0:T(8,128)(2,1)S(1)}, u32[]{:S(2)}, u32[]{:S(2)}) collective-permute-start(bf16[128,2048]{1,0:T(8,128)(2,1)S(1)} %collect.7), channel_id=1, source_target_pairs={{0,2},{1,3},{2,4},{3,5},{4,6},{5,7},{6,0},{7,1},{8,10},{9,11},{10,... | collective-permute-start | bytes 1572872 | tf_op jit(solution)/shard_map/ppermute | solution.py:465
  (14 other events, 10.5 us)

commit v3 on v2

--- a/solution.py
+++ b/solution.py
@@ -143,7 +143,7 @@
 def join_kernel(late_ref, own_ref, got_ref, inner_ref, own_out, inner_out):
     late = late_ref[0] > 0
     for h in range(own_ref.shape[0]):
-        own, got, inner = own_ref[h], got_ref[h], inner_ref[h]
+        own, got, inner = own_ref[h], got_ref[h].astype(F32), inner_ref[h]
         first, second = jnp.where(late, got, own), jnp.where(late, own, got)
         blank = jnp.zeros_like(own[:, DV:])
         keep = lambda x: jnp.concatenate([x[:, :DV], blank], axis=1)
@@ -171,7 +171,7 @@
     states = []
     for h in range(heads):
         inner = inner_ref[h]
-        state = mm3(inner[:, DV:], got_ref[h]) + inner[:, :DV]
+        state = mm3(inner[:, DV:], got_ref[h].astype(F32)) + inner[:, :DV]
         states.append(jnp.concatenate(halves(jnp.where(late, state, inner[:, :DV])), axis=1))
     depth, rows = mine_ref.shape[0], mine_ref.shape[1]
     for out_ref, shift in ((mine_ref, core_ref[0]), (other_ref, 1 - core_ref[0])):
@@ -533,7 +533,7 @@
     while True:
         late = scalar((me // span) % 2)
         final = 2 * span >= ep
-        got = trade(joint[..., :DV] if final else joint, span)
+        got = trade((joint[..., :DV] if final else joint).astype(BF16), span)
         if final:
             break
         joint, inner = join(late, joint, got, inner)

time: 213 us -> 226 us (1.061)
  waiting for transfers between devices: 83.2 us -> 90 us
  starting transfers between devices: 39.7 us -> 43.7 us
  other arithmetic: 1.79 us -> 4.06 us
    ppermute x26, waiting for transfers between devices: 16 us -> 23.4 us  [trade(): return lax.ppermute(x, 'ep', [(y, y ^ distance) for y in range(ep)])]
    ppermute x26, starting transfers between devices: 28.5 us -> 32.6 us  [trade(): return lax.ppermute(x, 'ep', [(y, y ^ distance) for y in range(ep)])]
    unnamed x76 -> x70, local copies, waits for them, and re-layouts: 21.7 us -> 21.5 us
  transfers between devices with their start and end apart: 40 -> 40, of which waited for: 11 -> 10; matrix products, arithmetic and copies ran while one was open for 0% -> 2% of each run, Pallas kernels for 30% -> 28%
where the time goes in v3:
time: 226 us; the launch traced here: 225 us
  waiting for transfers between devices  90 us (40%)
  Pallas kernels  63.9 us (28%)
  starting transfers between devices  43.7 us (19%)
  local copies, waits for them, and re-layouts  22.4 us (10%)
  other arithmetic  4.06 us (2%)
    ppermute x9, waiting for transfers between devices, send(): lax.ppermute(x, 'tp', [(y, (y + chips * CORES) % tp) for y in range(tp)])  66.5 us
    ppermute x26, starting transfers between devices, trade(): return lax.ppermute(x, 'ep', [(y, y ^ distance) for y in range(ep)])  32.6 us
    pallas_call x4, Pallas kernels, expert_part(): pl.pallas_call(functools.partial(expert_kernel, moved, peers, slots), in_...  31.1 us
    ppermute x26, waiting for transfers between devices, trade(): return lax.ppermute(x, 'ep', [(y, y ^ distance) for y in range(ep)])  23.4 us
    unnamed x70, local copies, waits for them, and re-layouts  21.5 us
    pallas_call x2, Pallas kernels, mixer_local(): pl.pallas_call(functools.partial(mixer_kernel, head), grid=(1,), in_specs...  13 us
    ppermute x9, starting transfers between devices, send(): lax.ppermute(x, 'tp', [(y, (y + chips * CORES) % tp) for y in range(tp)])  10 us
    pallas_call x4, Pallas kernels, collect(): pl.pallas_call(functools.partial(collect_kernel, peers, slots), grid=(1,)...  5.72 us
  transfers between devices with their start and end apart: 40, of which 10 were waited for; matrix products, arithmetic and copies ran while one was open for 2% of the time, Pallas kernels for 28%

profile of v3, /device:TPU:0, one launch (start us, length us, event | category | flops | bytes accessed | tf_op | source)
XLA Modules:
  0.0 225.0 jit_solution(7627737171403264665)
XLA Ops:
  1.7 3.2 %prepare.1 = (bf16[128,2176]{1,0:T(8,128)(2,1)}, bf16[64,2176]{1,0:T(8,128)(2,1)}, bf16[64,2176]{1,0:T(8,128)(2,1)}, bf16[64,2176]{1,0:T(8,128)(2,1)}, bf16[64,2176]{1,0:T(8,128)(2,1)}) custom-call(s32[1]{0:T(128)} %bitcast.4.me_ref, bf16[128,2048]{1,0:T(8,128)(2,1)} %x_ref.1, f32[1,2048]{1,0:T(1,128)} %bitcast.9, s32[2,128]{1,0:T(2,128)} %bitcast.10, ...), custom_call_target="tpu_custom_call" | custom-call | flops 134217728 | bytes 2097152 | tf_op jit(solution)/shard_map/prepare/pallas_call | solution.py:286
  4.9 2.6 %collective-permute-start.16 = (bf16[128,2176]{1,0:T(8,128)(2,1)}, bf16[128,2176]{1,0:T(8,128)(2,1)S(1)}, u32[]{:S(2)}, u32[]{:S(2)}) collective-permute-start(bf16[128,2176]{1,0:T(8,128)(2,1)} %get-tuple-element.71.meta_ref), channel_id=1, source_target_pairs={{0,2},{1,3},{2,4},{3,5},{4,6},{5,7},{6,0},{7,1},{8,10},{9,11},{10,... | collective-permute-start | bytes 1671176 | tf_op jit(solution)/shard_map/ppermute | solution.py:465
  7.6 15.5 %collective-permute-done.16.block_ref.meta_ref = bf16[128,2176]{1,0:T(8,128)(2,1)S(1)} collective-permute-done((bf16[128,2176]{1,0:T(8,128)(2,1)}, bf16[128,2176]{1,0:T(8,128)(2,1)S(1)}, u32[]{:S(2)}, u32[]{:S(2)}) %collective-permute-start.16) | collective-permute-done | bytes 557088 | tf_op jit(solution)/shard_map/ppermute | solution.py:465
  23.0 16.3 %collective-permute-done.24.block_ref.meta_ref = bf16[128,2176]{1,0:T(8,128)(2,1)} collective-permute-done((bf16[128,2176]{1,0:T(8,128)(2,1)S(1)}, bf16[128,2176]{1,0:T(8,128)(2,1)}, u32[]{:S(2)}, u32[]{:S(2)}) %collective-permute-start.24) | collective-permute-done | bytes 557088 | tf_op jit(solution)/shard_map/ppermute | solution.py:465
  39.3 6.4 %mixer_local.2 = (f32[512,128]{1,0:T(8,128)}, bf16[512,128]{1,0:T(8,128)(2,1)}, f32[1,128,256]{2,1,0:T(8,128)}) custom-call(f32[2]{0:T(128)} %rate_ref.3, bf16[512,256]{1,0:T(8,128)(2,1)} %q_ref.3, bf16[512,256]{1,0:T(8,128)(2,1)} %k_ref.3, bf16[512,256]{1,0:T(8,128)(2,1)} %v_ref.3, bf16[2,512]{1,0:T(2,128)(2,1)} %write_ref.3, bf16[2,512]{1,0:T(2,128)(2,1)} %decay_ref.3, ...), custom_call_target="tpu_custom_call" | custom-call | flops 2617245696 | bytes 917504 | tf_op jit(solution)/shard_map/mixer_local/pallas_call | solution.py:128
  45.8 1.4 dispatch.3
  47.9 6.9 %collective-permute-done.25.block_ref.meta_ref = bf16[128,2176]{1,0:T(8,128)(2,1)S(1)} collective-permute-done((bf16[128,2176]{1,0:T(8,128)(2,1)}, bf16[128,2176]{1,0:T(8,128)(2,1)S(1)}, u32[]{:S(2)}, u32[]{:S(2)}) %collective-permute-start.25) | collective-permute-done | bytes 557088 | tf_op jit(solution)/shard_map/ppermute | solution.py:465
  54.9 1.0 collective-permute-start.17
  55.9 1.6 collective-permute-start.18
  57.5 0.9 collective-permute-start.19
  59.0 6.6 %mixer_local.3 = (f32[512,128]{1,0:T(8,128)}, bf16[512,128]{1,0:T(8,128)(2,1)}, f32[2,128,256]{2,1,0:T(8,128)}) custom-call(f32[2]{0:T(128)} %rate_ref.3, bf16[512,256]{1,0:T(8,128)(2,1)} %q_ref.3, bf16[512,256]{1,0:T(8,128)(2,1)} %k_ref.3, bf16[512,256]{1,0:T(8,128)(2,1)} %v_ref.3, bf16[2,512]{1,0:T(2,128)(2,1)} %write_ref.3, bf16[2,512]{1,0:T(2,128)(2,1)} %decay_ref.3, ...), custom_call_target="tpu_custom_call" | custom-call | flops 2617245696 | bytes 917504 | tf_op jit(solution)/shard_map/mixer_local/pallas_call | solution.py:128
  65.6 2.5 %dispatch.5 = (bf16[64,2176]{1,0:T(8,128)(2,1)S(1)}, bf16[64,2176]{1,0:T(8,128)(2,1)}, bf16[64,2176]{1,0:T(8,128)(2,1)}, bf16[64,2176]{1,0:T(8,128)(2,1)}) custom-call(s32[1]{0:T(128)} %bitcast.4.me_ref, bf16[128,2176]{1,0:T(8,128)(2,1)} %collective-permute-done.24.block_ref.meta_ref), custom_call_target="tpu_custom_call" | custom-call | flops 142606336 | bytes 1671168 | tf_op jit(solution)/shard_map/dispatch/pallas_call | solution.py:317
  71.6 1.0 collective-permute-start.32
  72.6 1.6 convert_element_type.29
  74.3 1.5 collective-permute-start.33
  75.8 0.9 collective-permute-start.34
  76.7 1.0 collective-permute-start.3
  77.8 8.8 %expert_part.5 = (bf16[64,2048]{1,0:T(8,128)(2,1)}, bf16[64,2048]{1,0:T(8,128)(2,1)}, bf16[64,2048]{1,0:T(8,128)(2,1)}, bf16[64,2048]{1,0:T(8,128)(2,1)}) custom-call(s32[1]{0:T(128)} %bitcast.4.me_ref, bf16[64,2176]{1,0:T(8,128)(2,1)} %copy-done.16, bf16[64,2176]{1,0:T(8,128)(2,1)} %collective-permute-done.17.refs_1_, ...), custom_call_target="tpu_custom_call" | custom-call | flops 3221225472 | bytes 14680064 | tf_op jit(solution)/shard_map/expert_part/pallas_call | solution.py:392
  87.3 0.9 collective-permute-start.26
  88.2 0.9 broadcast_in_dim.4.inner_ref
  89.2 0.9 copy-done.25
  90.1 1.5 join.1
  92.4 1.1 collective-permute-start.27
  93.5 1.5 collective-permute-start.28
  95.0 1.0 collective-permute-start.4
  96.0 1.6 copy-done
  97.6 1.6 copy-done.2
  99.2 1.6 copy-done.5
  100.8 1.6 copy-done.9
  102.4 1.0 copy-done.15
  103.3 8.1 %expert_part.7 = (bf16[64,2048]{1,0:T(8,128)(2,1)S(1)}, bf16[64,2048]{1,0:T(8,128)(2,1)S(1)}, bf16[64,2048]{1,0:T(8,128)(2,1)S(1)}, bf16[64,2048]{1,0:T(8,128)(2,1)S(1)}) custom-call(s32[1]{0:T(128)} %bitcast.4.me_ref, bf16[64,2176]{1,0:T(8,128)(2,1)S(1)} %copy-done.15, bf16[64,2176]{1,0:T(8,128)(2,1)} %collective-permute-done.32.refs_1_, ...), custom_call_target="tpu_custom_call" | custom-call | flops 3221225472 | bytes 14680064 | tf_op jit(solution)/shard_map/expert_part/pallas_call | solution.py:392
  111.4 1.0 collective-permute-start.20
  112.5 1.0 collective-permute-start.21
  113.5 1.1 collective-permute-start.35
  114.6 1.0 collective-permute-start.36
  115.6 1.4 collective-permute-start.37
  117.0 6.9 %expert_part.6 = (bf16[64,2048]{1,0:T(8,128)(2,1)S(1)}, bf16[64,2048]{1,0:T(8,128)(2,1)}, bf16[64,2048]{1,0:T(8,128)(2,1)}, bf16[64,2048]{1,0:T(8,128)(2,1)S(1)}) custom-call(s32[1]{0:T(128)} %bitcast.4.me_ref, bf16[64,2176]{1,0:T(8,128)(2,1)S(1)} %get-tuple-element.94.refs_0_, bf16[64,2176]{1,0:T(8,128)(2,1)S(1)} %collective-permute-done.26.refs_1_, ...), custom_call_target="tpu_custom_call" | custom-call | flops 3221225472 | bytes 14680064 | tf_op jit(solution)/shard_map/expert_part/pallas_call | solution.py:392
  123.9 2.4 %collective-permute-done.35.refs_1_ = bf16[64,2048]{1,0:T(8,128)(2,1)S(1)} collective-permute-done((bf16[64,2048]{1,0:T(8,128)(2,1)S(1)}, bf16[64,2048]{1,0:T(8,128)(2,1)S(1)}, u32[]{:S(2)}, u32[]{:S(2)}) %collective-permute-start.35) | collective-permute-done | bytes 262176 | tf_op jit(solution)/shard_map/ppermute | solution.py:468
  126.3 1.4 collective-permute-start.22
  127.7 3.4 %collective-permute-done.36.refs_2_ = bf16[64,2048]{1,0:T(8,128)(2,1)S(1)} collective-permute-done((bf16[64,2048]{1,0:T(8,128)(2,1)S(1)}, bf16[64,2048]{1,0:T(8,128)(2,1)S(1)}, u32[]{:S(2)}, u32[]{:S(2)}) %collective-permute-start.36) | collective-permute-done | bytes 262176 | tf_op jit(solution)/shard_map/ppermute | solution.py:468
  131.1 5.5 %collective-permute-start.29 = (bf16[64,2048]{1,0:T(8,128)(2,1)}, bf16[64,2048]{1,0:T(8,128)(2,1)}, u32[]{:S(2)}, u32[]{:S(2)}) collective-permute-start(bf16[64,2048]{1,0:T(8,128)(2,1)} %get-tuple-element.99), channel_id=1, source_target_pairs={{0,8},{8,0},{16,24},{24,16},{1,9},{9,1},{17,25},{25,17},{2,10},{10... | collective-permute-start | bytes 786440 | tf_op jit(solution)/shard_map/ppermute | solution.py:468
  136.7 2.0 collect.6
  139.4 2.4 %attend.1 = (bf16[4,64,256]{2,1,0:T(8,128)(2,1)}, bf16[4,64,256]{2,1,0:T(8,128)(2,1)}) custom-call(s32[1]{0:T(128)} %bitcast.1.late_ref, s32[1]{0:T(128)} %bitcast.2.core_ref, f32[512,128]{1,0:T(8,128)} %get-tuple-element.56.refs_0_, f32[512,128]{1,0:T(8,128)} %get-tuple-element.58.refs_1_, bf16[512,128]{1,0:T(8,128)(2,1)} %get-tuple-element.59.refs_2_, ...), custom_call_target="tpu_custom_call" | custom-call | flops 201326592 | bytes 1310720 | tf_op jit(solution)/shard_map/attend/pallas_call | solution.py:191
  142.5 2.0 collective-permute-start.11
  144.5 1.5 collective-permute-start.12
  146.7 1.4 collective-permute-start.31
  148.1 0.9 copy-done.17
  149.1 0.9 copy-done.19
  150.0 0.9 copy-done.24
  151.0 1.5 collect.4
  152.5 1.2 copy-done.11
  155.6 2.4 %project.1 = (bf16[64,2048]{1,0:T(8,128)(2,1)S(1)}, bf16[64,2048]{1,0:T(8,128)(2,1)S(1)}, bf16[64,2048]{1,0:T(8,128)(2,1)S(1)}, bf16[64,2048]{1,0:T(8,128)(2,1)S(1)}) custom-call(s32[1]{0:T(128)} %bitcast.level_ref, bf16[4,64,256]{2,1,0:T(8,128)(2,1)S(1)} %copy-done.26, bf16[4,64,256]{2,1,0:T(8,128)(2,1)S(1)} %copy-done.28, ...), custom_call_target="tpu_custom_call" | custom-call | flops 536870912 | bytes 3145728 | tf_op jit(solution)/shard_map/project/pallas_call | solution.py:235
  158.0 6.9 %collective-permute-done.31.refs_3_ = bf16[64,2048]{1,0:T(8,128)(2,1)} collective-permute-done((bf16[64,2048]{1,0:T(8,128)(2,1)}, bf16[64,2048]{1,0:T(8,128)(2,1)}, u32[]{:S(2)}, u32[]{:S(2)}) %collective-permute-start.31) | collective-permute-done | bytes 262176 | tf_op jit(solution)/shard_map/ppermute | solution.py:468
  164.9 3.8 %collective-permute-start.23 = (bf16[128,2048]{1,0:T(8,128)(2,1)S(1)}, bf16[128,2048]{1,0:T(8,128)(2,1)S(1)}, u32[]{:S(2)}, u32[]{:S(2)}) collective-permute-start(bf16[128,2048]{1,0:T(8,128)(2,1)S(1)} %collect.4), channel_id=1, source_target_pairs={{0,6},{1,7},{2,0},{3,1},{4,2},{5,3},{6,4},{7,5},{8,14},{9,15},{10,... | collective-permute-start | bytes 1572872 | tf_op jit(solution)/shard_map/ppermute | solution.py:465
  168.8 0.9 copy-done.21
  169.7 1.7 collect.7
  171.5 2.1 collective-permute-start.9
  173.6 1.4 collective-permute-start.39
  175.0 7.3 %expert_part.4 = (bf16[64,2048]{1,0:T(8,128)(2,1)S(1)}, bf16[64,2048]{1,0:T(8,128)(2,1)S(1)}, bf16[64,2048]{1,0:T(8,128)(2,1)S(1)}, bf16[64,2048]{1,0:T(8,128)(2,1)S(1)}) custom-call(s32[1]{0:T(128)} %bitcast.4.me_ref, bf16[64,2176]{1,0:T(8,128)(2,1)S(1)} %copy-done.13, bf16[64,2176]{1,0:T(8,128)(2,1)S(1)} %collective-permute-done.10.refs_1_, ...), custom_call_target="tpu_custom_call" | custom-call | flops 3221225472 | bytes 14680064 | tf_op jit(solution)/shard_map/expert_part/pallas_call | solution.py:392
  182.3 5.2 %collective-permute-done.7 = bf16[64,2048]{1,0:T(8,128)(2,1)S(1)} collective-permute-done((bf16[64,2048]{1,0:T(8,128)(2,1)S(1)}, bf16[64,2048]{1,0:T(8,128)(2,1)S(1)}, u32[]{:S(2)}, u32[]{:S(2)}) %collective-permute-start.7) | collective-permute-done | bytes 262176 | tf_op jit(solution)/shard_map/ppermute | solution.py:465
  188.1 22.6 %collective-permute-done.8 = bf16[64,2048]{1,0:T(8,128)(2,1)S(1)} collective-permute-done((bf16[64,2048]{1,0:T(8,128)(2,1)S(1)}, bf16[64,2048]{1,0:T(8,128)(2,1)S(1)}, u32[]{:S(2)}, u32[]{:S(2)}) %collective-permute-start.8) | collective-permute-done | bytes 262176 | tf_op jit(solution)/shard_map/ppermute | solution.py:465
  210.8 2.0 collective-permute-start.15
  213.6 10.0 %collective-permute-done.14.refs_2_ = bf16[64,2048]{1,0:T(8,128)(2,1)S(1)} collective-permute-done((bf16[64,2048]{1,0:T(8,128)(2,1)S(1)}, bf16[64,2048]{1,0:T(8,128)(2,1)S(1)}, u32[]{:S(2)}, u32[]{:S(2)}) %collective-permute-start.14) | collective-permute-done | bytes 262176 | tf_op jit(solution)/shard_map/ppermute | solution.py:468
  224.1 0.9 add_convert_fusion
  (110 shorter events, 13.5 us)
Async XLA Ops:
  0.6 55.3 %collective-permute-start = (bf16[4,128,2048]{2,1,0:T(8,128)(2,1)}, bf16[4,128,2048]{2,1,0:T(8,128)(2,1)S(1)}, u32[]{:S(2)}, u32[]{:S(2)}) collective-permute-start(bf16[4,128,2048]{2,1,0:T(8,128)(2,1)} %refs_4_.3), channel_id=1, source_target_pairs={{0,1},{1,0},{2,3},{3,2},{4,5},{5,4},{6,7},{7,6},{8,9},{9,8},{10,11... | collective-permute-start | bytes 6291464 | tf_op jit(solution)/shard_map/ppermute | solution.py:462
  1.2 56.3 %collective-permute-start.1 = (bf16[4,128,2048]{2,1,0:T(8,128)(2,1)}, bf16[4,128,2048]{2,1,0:T(8,128)(2,1)}, u32[]{:S(2)}, u32[]{:S(2)}) collective-permute-start(bf16[4,128,2048]{2,1,0:T(8,128)(2,1)} %refs_6_.3), channel_id=1, source_target_pairs={{0,1},{1,0},{2,3},{3,2},{4,5},{5,4},{6,7},{7,6},{8,9},{9,8},{10,11... | collective-permute-start | bytes 6291464 | tf_op jit(solution)/shard_map/ppermute | solution.py:462
  1.3 70.4 %collective-permute-start.2 = (bf16[4,128,2048]{2,1,0:T(8,128)(2,1)}, bf16[4,128,2048]{2,1,0:T(8,128)(2,1)}, u32[]{:S(2)}, u32[]{:S(2)}) collective-permute-start(bf16[4,128,2048]{2,1,0:T(8,128)(2,1)} %refs_8_.3), channel_id=1, source_target_pairs={{0,1},{1,0},{2,3},{3,2},{4,5},{5,4},{6,7},{7,6},{8,9},{9,8},{10,11... | collective-permute-start | bytes 6291464 | tf_op jit(solution)/shard_map/ppermute | solution.py:462
  4.9 18.1 %collective-permute-start.16 = (bf16[128,2176]{1,0:T(8,128)(2,1)}, bf16[128,2176]{1,0:T(8,128)(2,1)S(1)}, u32[]{:S(2)}, u32[]{:S(2)}) collective-permute-start(bf16[128,2176]{1,0:T(8,128)(2,1)} %get-tuple-element.71.meta_ref), channel_id=1, source_target_pairs={{0,2},{1,3},{2,4},{3,5},{4,6},{5,7},{6,0},{7,1},{8,10},{9,11},{10,... | collective-permute-start | bytes 1671176 | tf_op jit(solution)/shard_map/ppermute | solution.py:465
  23.0 16.3 %collective-permute-start.24 = (bf16[128,2176]{1,0:T(8,128)(2,1)S(1)}, bf16[128,2176]{1,0:T(8,128)(2,1)}, u32[]{:S(2)}, u32[]{:S(2)}) collective-permute-start(bf16[128,2176]{1,0:T(8,128)(2,1)S(1)} %collective-permute-done.16.block_ref.meta_ref), channel_id=1, source_target_pairs={{0,2},{1,3},{2,4},{3,5},{4,6},{5,7},{6,0},{7,1},{8,10},{9,11},{10,... | collective-permute-start | bytes 1671176 | tf_op jit(solution)/shard_map/ppermute | solution.py:465
  39.3 15.5 %collective-permute-start.25 = (bf16[128,2176]{1,0:T(8,128)(2,1)}, bf16[128,2176]{1,0:T(8,128)(2,1)S(1)}, u32[]{:S(2)}, u32[]{:S(2)}) collective-permute-start(bf16[128,2176]{1,0:T(8,128)(2,1)} %collective-permute-done.24.block_ref.meta_ref), channel_id=1, source_target_pairs={{0,2},{1,3},{2,4},{3,5},{4,6},{5,7},{6,0},{7,1},{8,10},{9,11},{10,... | collective-permute-start | bytes 1671176 | tf_op jit(solution)/shard_map/ppermute | solution.py:465
  39.3 72.1 %collective-permute-start.6 = (bf16[256,2048]{1,0:T(8,128)(2,1)}, bf16[256,2048]{1,0:T(8,128)(2,1)}, u32[]{:S(2)}, u32[]{:S(2)}) collective-permute-start(bf16[256,2048]{1,0:T(8,128)(2,1)} %own_ref.1), channel_id=1, source_target_pairs={{0,1},{1,0},{2,3},{3,2},{4,5},{5,4},{6,7},{7,6},{8,9},{9,8},{10,11... | collective-permute-start | bytes 3145736 | tf_op jit(solution)/shard_map/ppermute | solution.py:462
  54.9 19.4 %collective-permute-start.17 = (bf16[64,2176]{1,0:T(8,128)(2,1)}, bf16[64,2176]{1,0:T(8,128)(2,1)}, u32[]{:S(2)}, u32[]{:S(2)}) collective-permute-start(bf16[64,2176]{1,0:T(8,128)(2,1)} %get-tuple-element.87), channel_id=1, source_target_pairs={{0,8},{8,0},{16,24},{24,16},{1,9},{9,1},{17,25},{25,17},{2,10},{10... | collective-permute-start | bytes 835592 | tf_op jit(solution)/shard_map/ppermute | solution.py:468
  55.9 9.8 %copy-start.8 = (bf16[4,128,2048]{2,1,0:T(8,128)(2,1)}, bf16[4,128,2048]{2,1,0:T(8,128)(2,1)S(1)}, u32[]{:S(2)}) copy-start(bf16[4,128,2048]{2,1,0:T(8,128)(2,1)S(1)} %collective-permute-done.refs_5_) | copy-start | bytes 6291460
  55.9 19.9 %collective-permute-start.18 = (bf16[64,2176]{1,0:T(8,128)(2,1)}, bf16[64,2176]{1,0:T(8,128)(2,1)}, u32[]{:S(2)}, u32[]{:S(2)}) collective-permute-start(bf16[64,2176]{1,0:T(8,128)(2,1)} %get-tuple-element.88), channel_id=1, source_target_pairs={{0,16},{8,24},{16,0},{24,8},{1,17},{9,25},{17,1},{25,9},{2,18},{10... | collective-permute-start | bytes 835592 | tf_op jit(solution)/shard_map/ppermute | solution.py:468
  57.5 19.3 %collective-permute-start.19 = (bf16[64,2176]{1,0:T(8,128)(2,1)}, bf16[64,2176]{1,0:T(8,128)(2,1)}, u32[]{:S(2)}, u32[]{:S(2)}) collective-permute-start(bf16[64,2176]{1,0:T(8,128)(2,1)} %get-tuple-element.89), channel_id=1, source_target_pairs={{0,24},{8,16},{16,8},{24,0},{1,25},{9,17},{17,9},{25,1},{2,26},{10... | collective-permute-start | bytes 835592 | tf_op jit(solution)/shard_map/ppermute | solution.py:468
  71.6 20.7 %collective-permute-start.32 = (bf16[64,2176]{1,0:T(8,128)(2,1)}, bf16[64,2176]{1,0:T(8,128)(2,1)}, u32[]{:S(2)}, u32[]{:S(2)}) collective-permute-start(bf16[64,2176]{1,0:T(8,128)(2,1)} %get-tuple-element.103), channel_id=1, source_target_pairs={{0,8},{8,0},{16,24},{24,16},{1,9},{9,1},{17,25},{25,17},{2,10},{10... | collective-permute-start | bytes 835592 | tf_op jit(solution)/shard_map/ppermute | solution.py:468
  74.3 19.2 %collective-permute-start.33 = (bf16[64,2176]{1,0:T(8,128)(2,1)}, bf16[64,2176]{1,0:T(8,128)(2,1)}, u32[]{:S(2)}, u32[]{:S(2)}) collective-permute-start(bf16[64,2176]{1,0:T(8,128)(2,1)} %get-tuple-element.104), channel_id=1, source_target_pairs={{0,16},{8,24},{16,0},{24,8},{1,17},{9,25},{17,1},{25,9},{2,18},{10... | collective-permute-start | bytes 835592 | tf_op jit(solution)/shard_map/ppermute | solution.py:468
  75.8 19.2 %collective-permute-start.34 = (bf16[64,2176]{1,0:T(8,128)(2,1)}, bf16[64,2176]{1,0:T(8,128)(2,1)}, u32[]{:S(2)}, u32[]{:S(2)}) collective-permute-start(bf16[64,2176]{1,0:T(8,128)(2,1)} %get-tuple-element.105), channel_id=1, source_target_pairs={{0,24},{8,16},{16,8},{24,0},{1,25},{9,17},{17,9},{25,1},{2,26},{10... | collective-permute-start | bytes 835592 | tf_op jit(solution)/shard_map/ppermute | solution.py:468
  76.7 10.6 %collective-permute-start.3 = (bf16[2,128,256]{2,1,0:T(8,128)(2,1)}, bf16[2,128,256]{2,1,0:T(8,128)(2,1)}, u32[]{:S(2)}, u32[]{:S(2)}) collective-permute-start(bf16[2,128,256]{2,1,0:T(8,128)(2,1)} %convert_element_type.29), channel_id=1, source_target_pairs={{0,8},{8,0},{16,24},{24,16},{1,9},{9,1},{17,25},{25,17},{2,10},{10... | collective-permute-start | bytes 393224 | tf_op jit(solution)/shard_map/ppermute | solution.py:468
  87.3 25.1 %collective-permute-start.26 = (bf16[64,2176]{1,0:T(8,128)(2,1)}, bf16[64,2176]{1,0:T(8,128)(2,1)S(1)}, u32[]{:S(2)}, u32[]{:S(2)}) collective-permute-start(bf16[64,2176]{1,0:T(8,128)(2,1)} %copy-done.31), channel_id=1, source_target_pairs={{0,8},{8,0},{16,24},{24,16},{1,9},{9,1},{17,25},{25,17},{2,10},{10... | collective-permute-start | bytes 835592 | tf_op jit(solution)/shard_map/ppermute | solution.py:468
  89.2 1.0 copy-start.25
  92.4 21.1 %collective-permute-start.27 = (bf16[64,2176]{1,0:T(8,128)(2,1)}, bf16[64,2176]{1,0:T(8,128)(2,1)S(1)}, u32[]{:S(2)}, u32[]{:S(2)}) collective-permute-start(bf16[64,2176]{1,0:T(8,128)(2,1)} %copy-done.30), channel_id=1, source_target_pairs={{0,16},{8,24},{16,0},{24,8},{1,17},{9,25},{17,1},{25,9},{2,18},{10... | collective-permute-start | bytes 835592 | tf_op jit(solution)/shard_map/ppermute | solution.py:468
  93.5 21.1 %collective-permute-start.28 = (bf16[64,2176]{1,0:T(8,128)(2,1)}, bf16[64,2176]{1,0:T(8,128)(2,1)S(1)}, u32[]{:S(2)}, u32[]{:S(2)}) collective-permute-start(bf16[64,2176]{1,0:T(8,128)(2,1)} %copy-done.29), channel_id=1, source_target_pairs={{0,24},{8,16},{16,8},{24,0},{1,25},{9,17},{17,9},{25,1},{2,26},{10... | collective-permute-start | bytes 835592 | tf_op jit(solution)/shard_map/ppermute | solution.py:468
  95.0 20.6 %collective-permute-start.4 = (bf16[2,128,128]{2,1,0:T(8,128)(2,1)S(1)}, bf16[2,128,128]{2,1,0:T(8,128)(2,1)S(1)}, u32[]{:S(2)}, u32[]{:S(2)}) collective-permute-start(bf16[2,128,128]{2,1,0:T(8,128)(2,1)S(1)} %slice.7), channel_id=1, source_target_pairs={{0,16},{8,24},{16,0},{24,8},{1,17},{9,25},{17,1},{25,9},{2,18},{10... | collective-permute-start | bytes 196616 | tf_op jit(solution)/shard_map/ppermute | solution.py:468
  96.0 1.6 copy-start
  97.6 1.6 copy-start.2
  99.2 1.6 copy-start.5
  100.8 1.6 copy-start.9
  102.4 1.0 copy-start.15
  103.3 8.1 %copy-start.34 = (bf16[64,2048]{1,0:T(8,128)(2,1)S(1)}, bf16[64,2048]{1,0:T(8,128)(2,1)}, u32[]{:S(2)}) copy-start(bf16[64,2048]{1,0:T(8,128)(2,1)} %get-tuple-element.91) | copy-start | bytes 786436
  103.3 13.6 %copy-start.1 = (bf16[4,128,2048]{2,1,0:T(8,128)(2,1)S(1)}, bf16[4,128,2048]{2,1,0:T(8,128)(2,1)}, u32[]{:S(2)}) copy-start(bf16[4,128,2048]{2,1,0:T(8,128)(2,1)} %refs_4_.3) | copy-start | bytes 6291460
  103.3 13.6 %copy-start.3 = (bf16[4,128,2048]{2,1,0:T(8,128)(2,1)S(1)}, bf16[4,128,2048]{2,1,0:T(8,128)(2,1)}, u32[]{:S(2)}) copy-start(bf16[4,128,2048]{2,1,0:T(8,128)(2,1)} %refs_6_.3) | copy-start | bytes 6291460
  103.3 13.6 %copy-start.6 = (bf16[4,128,2048]{2,1,0:T(8,128)(2,1)S(1)}, bf16[4,128,2048]{2,1,0:T(8,128)(2,1)}, u32[]{:S(2)}) copy-start(bf16[4,128,2048]{2,1,0:T(8,128)(2,1)} %refs_8_.3) | copy-start | bytes 6291460
  111.4 27.2 %collective-permute-start.20 = (bf16[64,2048]{1,0:T(8,128)(2,1)S(1)}, bf16[64,2048]{1,0:T(8,128)(2,1)S(1)}, u32[]{:S(2)}, u32[]{:S(2)}) collective-permute-start(bf16[64,2048]{1,0:T(8,128)(2,1)S(1)} %copy-done.34), channel_id=1, source_target_pairs={{0,8},{8,0},{16,24},{24,16},{1,9},{9,1},{17,25},{25,17},{2,10},{10... | collective-permute-start | bytes 786440 | tf_op jit(solution)/shard_map/ppermute | solution.py:468
  112.5 29.3 %collective-permute-start.21 = (bf16[64,2048]{1,0:T(8,128)(2,1)}, bf16[64,2048]{1,0:T(8,128)(2,1)}, u32[]{:S(2)}, u32[]{:S(2)}) collective-permute-start(bf16[64,2048]{1,0:T(8,128)(2,1)} %get-tuple-element.92), channel_id=1, source_target_pairs={{0,16},{8,24},{16,0},{24,8},{1,17},{9,25},{17,1},{25,9},{2,18},{10... | collective-permute-start | bytes 786440 | tf_op jit(solution)/shard_map/ppermute | solution.py:468
  113.5 12.8 %collective-permute-start.35 = (bf16[64,2048]{1,0:T(8,128)(2,1)S(1)}, bf16[64,2048]{1,0:T(8,128)(2,1)S(1)}, u32[]{:S(2)}, u32[]{:S(2)}) collective-permute-start(bf16[64,2048]{1,0:T(8,128)(2,1)S(1)} %get-tuple-element.107), channel_id=1, source_target_pairs={{0,8},{8,0},{16,24},{24,16},{1,9},{9,1},{17,25},{25,17},{2,10},{10... | collective-permute-start | bytes 786440 | tf_op jit(solution)/shard_map/ppermute | solution.py:468
  114.6 16.5 %collective-permute-start.36 = (bf16[64,2048]{1,0:T(8,128)(2,1)S(1)}, bf16[64,2048]{1,0:T(8,128)(2,1)S(1)}, u32[]{:S(2)}, u32[]{:S(2)}) collective-permute-start(bf16[64,2048]{1,0:T(8,128)(2,1)S(1)} %get-tuple-element.108), channel_id=1, source_target_pairs={{0,16},{8,24},{16,0},{24,8},{1,17},{9,25},{17,1},{25,9},{2,18},{10... | collective-permute-start | bytes 786440 | tf_op jit(solution)/shard_map/ppermute | solution.py:468
  115.6 8.3 %copy-start.33 = (bf16[2,128,128]{2,1,0:T(8,128)(2,1)}, bf16[2,128,128]{2,1,0:T(8,128)(2,1)S(1)}, u32[]{:S(2)}) copy-start(bf16[2,128,128]{2,1,0:T(8,128)(2,1)S(1)} %collective-permute-done.4.refs_4_) | copy-start | bytes 196612
  115.6 21.1 %collective-permute-start.37 = (bf16[64,2048]{1,0:T(8,128)(2,1)S(1)}, bf16[64,2048]{1,0:T(8,128)(2,1)S(1)}, u32[]{:S(2)}, u32[]{:S(2)}) collective-permute-start(bf16[64,2048]{1,0:T(8,128)(2,1)S(1)} %get-tuple-element.109), channel_id=1, source_target_pairs={{0,24},{8,16},{16,8},{24,0},{1,25},{9,17},{17,9},{25,1},{2,26},{10... | collective-permute-start | bytes 786440 | tf_op jit(solution)/shard_map/ppermute | solution.py:468
  123.9 14.7 %copy-start.20 = (bf16[64,2048]{1,0:T(8,128)(2,1)}, bf16[64,2048]{1,0:T(8,128)(2,1)S(1)}, u32[]{:S(2)}) copy-start(bf16[64,2048]{1,0:T(8,128)(2,1)S(1)} %get-tuple-element.98.refs_0_) | copy-start | bytes 786436
  123.9 14.7 %copy-start.32 = (bf16[64,2048]{1,0:T(8,128)(2,1)}, bf16[64,2048]{1,0:T(8,128)(2,1)S(1)}, u32[]{:S(2)}) copy-start(bf16[64,2048]{1,0:T(8,128)(2,1)S(1)} %get-tuple-element.101) | copy-start | bytes 786436
  126.3 15.5 %collective-permute-start.22 = (bf16[64,2048]{1,0:T(8,128)(2,1)}, bf16[64,2048]{1,0:T(8,128)(2,1)S(1)}, u32[]{:S(2)}, u32[]{:S(2)}) collective-permute-start(bf16[64,2048]{1,0:T(8,128)(2,1)} %get-tuple-element.93), channel_id=1, source_target_pairs={{0,24},{8,16},{16,8},{24,0},{1,25},{9,17},{17,9},{25,1},{2,26},{10... | collective-permute-start | bytes 786440 | tf_op jit(solution)/shard_map/ppermute | solution.py:468
  131.1 11.4 %collective-permute-start.29 = (bf16[64,2048]{1,0:T(8,128)(2,1)}, bf16[64,2048]{1,0:T(8,128)(2,1)}, u32[]{:S(2)}, u32[]{:S(2)}) collective-permute-start(bf16[64,2048]{1,0:T(8,128)(2,1)} %get-tuple-element.99), channel_id=1, source_target_pairs={{0,8},{8,0},{16,24},{24,16},{1,9},{9,1},{17,25},{25,17},{2,10},{10... | collective-permute-start | bytes 786440 | tf_op jit(solution)/shard_map/ppermute | solution.py:468
  136.7 7.9 %collective-permute-start.30 = (bf16[64,2048]{1,0:T(8,128)(2,1)}, bf16[64,2048]{1,0:T(8,128)(2,1)}, u32[]{:S(2)}, u32[]{:S(2)}) collective-permute-start(bf16[64,2048]{1,0:T(8,128)(2,1)} %get-tuple-element.100), channel_id=1, source_target_pairs={{0,16},{8,24},{16,0},{24,8},{1,17},{9,25},{17,1},{25,9},{2,18},{10... | collective-permute-start | bytes 786440 | tf_op jit(solution)/shard_map/ppermute | solution.py:468
  139.4 29.3 %collective-permute-start.38 = (bf16[128,2048]{1,0:T(8,128)(2,1)}, bf16[128,2048]{1,0:T(8,128)(2,1)}, u32[]{:S(2)}, u32[]{:S(2)}) collective-permute-start(bf16[128,2048]{1,0:T(8,128)(2,1)} %collect.6), channel_id=1, source_target_pairs={{0,2},{1,3},{2,4},{3,5},{4,6},{5,7},{6,0},{7,1},{8,10},{9,11},{10,... | collective-permute-start | bytes 1572872 | tf_op jit(solution)/shard_map/ppermute | solution.py:465
  141.8 4.3 %collective-permute-start.5 = (bf16[4,64,256]{2,1,0:T(8,128)(2,1)}, bf16[4,64,256]{2,1,0:T(8,128)(2,1)S(1)}, u32[]{:S(2)}, u32[]{:S(2)}) collective-permute-start(bf16[4,64,256]{2,1,0:T(8,128)(2,1)} %get-tuple-element.66), channel_id=1, source_target_pairs={{0,1},{1,0},{2,3},{3,2},{4,5},{5,4},{6,7},{7,6},{8,9},{9,8},{10,11... | collective-permute-start | bytes 393224 | tf_op jit(solution)/shard_map/ppermute | solution.py:462
  142.5 29.0 %collective-permute-start.10 = (bf16[64,2176]{1,0:T(8,128)(2,1)}, bf16[64,2176]{1,0:T(8,128)(2,1)S(1)}, u32[]{:S(2)}, u32[]{:S(2)}) collective-permute-start(bf16[64,2176]{1,0:T(8,128)(2,1)} %get-tuple-element.73), channel_id=1, source_target_pairs={{0,8},{8,0},{16,24},{24,16},{1,9},{9,1},{17,25},{25,17},{2,10},{10... | collective-permute-start | bytes 835592 | tf_op jit(solution)/shard_map/ppermute | solution.py:468
  142.5 29.0 %collective-permute-start.11 = (bf16[64,2176]{1,0:T(8,128)(2,1)}, bf16[64,2176]{1,0:T(8,128)(2,1)}, u32[]{:S(2)}, u32[]{:S(2)}) collective-permute-start(bf16[64,2176]{1,0:T(8,128)(2,1)} %get-tuple-element.74), channel_id=1, source_target_pairs={{0,16},{8,24},{16,0},{24,8},{1,17},{9,25},{17,1},{25,9},{2,18},{10... | collective-permute-start | bytes 835592 | tf_op jit(solution)/shard_map/ppermute | solution.py:468
  144.5 29.1 %collective-permute-start.12 = (bf16[64,2176]{1,0:T(8,128)(2,1)}, bf16[64,2176]{1,0:T(8,128)(2,1)}, u32[]{:S(2)}, u32[]{:S(2)}) collective-permute-start(bf16[64,2176]{1,0:T(8,128)(2,1)} %get-tuple-element.75), channel_id=1, source_target_pairs={{0,24},{8,16},{16,8},{24,0},{1,25},{9,17},{17,9},{25,1},{2,26},{10... | collective-permute-start | bytes 835592 | tf_op jit(solution)/shard_map/ppermute | solution.py:468
  146.7 18.2 %collective-permute-start.31 = (bf16[64,2048]{1,0:T(8,128)(2,1)}, bf16[64,2048]{1,0:T(8,128)(2,1)}, u32[]{:S(2)}, u32[]{:S(2)}) collective-permute-start(bf16[64,2048]{1,0:T(8,128)(2,1)} %copy-done.32), channel_id=1, source_target_pairs={{0,24},{8,16},{16,8},{24,0},{1,25},{9,17},{17,9},{25,1},{2,26},{10... | collective-permute-start | bytes 786440 | tf_op jit(solution)/shard_map/ppermute | solution.py:468
  148.1 0.9 copy-start.17
  149.1 0.9 copy-start.19
  150.0 0.9 copy-start.24
  151.0 24.0 %copy-start.10 = (bf16[4,128,2048]{2,1,0:T(8,128)(2,1)S(1)}, bf16[4,128,2048]{2,1,0:T(8,128)(2,1)}, u32[]{:S(2)}) copy-start(bf16[4,128,2048]{2,1,0:T(8,128)(2,1)} %copy-done.8) | copy-start | bytes 6291460
  152.5 1.2 copy-start.11
  155.6 19.5 %copy-start.4 = (bf16[4,128,2048]{2,1,0:T(8,128)(2,1)S(1)}, bf16[4,128,2048]{2,1,0:T(8,128)(2,1)}, u32[]{:S(2)}) copy-start(bf16[4,128,2048]{2,1,0:T(8,128)(2,1)} %refs_6_.3) | copy-start | bytes 6291460
  155.6 19.5 %copy-start.7 = (bf16[4,128,2048]{2,1,0:T(8,128)(2,1)S(1)}, bf16[4,128,2048]{2,1,0:T(8,128)(2,1)}, u32[]{:S(2)}) copy-start(bf16[4,128,2048]{2,1,0:T(8,128)(2,1)} %refs_8_.3) | copy-start | bytes 6291460
  155.6 19.5 %copy-start.13 = (bf16[64,2176]{1,0:T(8,128)(2,1)S(1)}, bf16[64,2176]{1,0:T(8,128)(2,1)}, u32[]{:S(2)}) copy-start(bf16[64,2176]{1,0:T(8,128)(2,1)} %get-tuple-element.72.refs_0_) | copy-start | bytes 835588
  164.9 58.7 %collective-permute-start.23 = (bf16[128,2048]{1,0:T(8,128)(2,1)S(1)}, bf16[128,2048]{1,0:T(8,128)(2,1)S(1)}, u32[]{:S(2)}, u32[]{:S(2)}) collective-permute-start(bf16[128,2048]{1,0:T(8,128)(2,1)S(1)} %collect.4), channel_id=1, source_target_pairs={{0,6},{1,7},{2,0},{3,1},{4,2},{5,3},{6,4},{7,5},{8,14},{9,15},{10,... | collective-permute-start | bytes 1572872 | tf_op jit(solution)/shard_map/ppermute | solution.py:465
  168.7 18.8 %collective-permute-start.7 = (bf16[64,2048]{1,0:T(8,128)(2,1)S(1)}, bf16[64,2048]{1,0:T(8,128)(2,1)S(1)}, u32[]{:S(2)}, u32[]{:S(2)}) collective-permute-start(bf16[64,2048]{1,0:T(8,128)(2,1)S(1)} %get-tuple-element.68), channel_id=1, source_target_pairs={{0,6},{1,7},{2,0},{3,1},{4,2},{5,3},{6,4},{7,5},{8,14},{9,15},{10,... | collective-permute-start | bytes 786440 | tf_op jit(solution)/shard_map/ppermute | solution.py:465
  168.8 0.9 copy-start.21
  171.4 39.3 %collective-permute-start.8 = (bf16[64,2048]{1,0:T(8,128)(2,1)S(1)}, bf16[64,2048]{1,0:T(8,128)(2,1)S(1)}, u32[]{:S(2)}, u32[]{:S(2)}) collective-permute-start(bf16[64,2048]{1,0:T(8,128)(2,1)S(1)} %get-tuple-element.69), channel_id=1, source_target_pairs={{0,4},{1,5},{2,6},{3,7},{4,0},{5,1},{6,2},{7,3},{8,12},{9,13},{10,... | collective-permute-start | bytes 786440 | tf_op jit(solution)/shard_map/ppermute | solution.py:465
  171.5 39.2 %collective-permute-start.9 = (bf16[64,2048]{1,0:T(8,128)(2,1)S(1)}, bf16[64,2048]{1,0:T(8,128)(2,1)S(1)}, u32[]{:S(2)}, u32[]{:S(2)}) collective-permute-start(bf16[64,2048]{1,0:T(8,128)(2,1)S(1)} %get-tuple-element.70), channel_id=1, source_target_pairs={{0,2},{1,3},{2,4},{3,5},{4,6},{5,7},{6,0},{7,1},{8,10},{9,11},{10,... | collective-permute-start | bytes 786440 | tf_op jit(solution)/shard_map/ppermute | solution.py:465
  173.6 50.5 %collective-permute-start.39 = (bf16[128,2048]{1,0:T(8,128)(2,1)S(1)}, bf16[128,2048]{1,0:T(8,128)(2,1)S(1)}, u32[]{:S(2)}, u32[]{:S(2)}) collective-permute-start(bf16[128,2048]{1,0:T(8,128)(2,1)S(1)} %collect.7), channel_id=1, source_target_pairs={{0,2},{1,3},{2,4},{3,5},{4,6},{5,7},{6,0},{7,1},{8,10},{9,11},{10,... | collective-permute-start | bytes 1572872 | tf_op jit(solution)/shard_map/ppermute | solution.py:465
  175.0 48.6 %copy-start.12 = (bf16[128,2176]{1,0:T(8,128)(2,1)S(1)}, bf16[128,2176]{1,0:T(8,128)(2,1)}, u32[]{:S(2)}) copy-start(bf16[128,2176]{1,0:T(8,128)(2,1)} %get-tuple-element.71.meta_ref) | copy-start | bytes 1671172
  187.5 26.1 %collective-permute-start.13 = (bf16[64,2048]{1,0:T(8,128)(2,1)S(1)}, bf16[64,2048]{1,0:T(8,128)(2,1)S(1)}, u32[]{:S(2)}, u32[]{:S(2)}) collective-permute-start(bf16[64,2048]{1,0:T(8,128)(2,1)S(1)} %get-tuple-element.83), channel_id=1, source_target_pairs={{0,8},{8,0},{16,24},{24,16},{1,9},{9,1},{17,25},{25,17},{2,10},{10... | collective-permute-start | bytes 786440 | tf_op jit(solution)/shard_map/ppermute | solution.py:468
  210.7 12.9 %collective-permute-start.14 = (bf16[64,2048]{1,0:T(8,128)(2,1)S(1)}, bf16[64,2048]{1,0:T(8,128)(2,1)S(1)}, u32[]{:S(2)}, u32[]{:S(2)}) collective-permute-start(bf16[64,2048]{1,0:T(8,128)(2,1)S(1)} %get-tuple-element.84), channel_id=1, source_target_pairs={{0,16},{8,24},{16,0},{24,8},{1,17},{9,25},{17,1},{25,9},{2,18},{10... | collective-permute-start | bytes 786440 | tf_op jit(solution)/shard_map/ppermute | solution.py:468
  210.8 12.8 %collective-permute-start.15 = (bf16[64,2048]{1,0:T(8,128)(2,1)S(1)}, bf16[64,2048]{1,0:T(8,128)(2,1)S(1)}, u32[]{:S(2)}, u32[]{:S(2)}) collective-permute-start(bf16[64,2048]{1,0:T(8,128)(2,1)S(1)} %get-tuple-element.85), channel_id=1, source_target_pairs={{0,24},{8,16},{16,8},{24,0},{1,25},{9,17},{17,9},{25,1},{2,26},{10... | collective-permute-start | bytes 786440 | tf_op jit(solution)/shard_map/ppermute | solution.py:468
  (11 other events, 8.2 us)
